TPU v7x, 512 devices: a whole 4x4x16 slice. The times are simulated.
512 devices in a mesh: kv: 32 (over z, core), tp: 16 (over y, x).
Axes of the slice: x: 4, y: 4, z: 16, core: 2. Of those that a mesh axis runs over, the one named last changes fastest.
Arguments:
- tokens: bfloat16 [256, 4096], P('tp', 'kv'), may hold values from -64 to 64
- first_norm_gain: float32 [4096], P('kv'), may hold values from 0.1 to 1.9
- first_gate_weight: bfloat16 [4096, 10240], P('kv', 'tp'), may hold values from -0.09375 to 0.09375
- first_up_weight: bfloat16 [4096, 10240], P('kv', 'tp'), may hold values from -0.09375 to 0.09375
- first_down_weight: bfloat16 [10240, 4096], P('tp', 'kv'), may hold values from -0.0625 to 0.0625
- mixer_norm_gain: float32 [4096], P('kv'), may hold values from 0.1 to 1.9
- query_weight_matrix: bfloat16 [4096, 2048], P('kv', 'tp'), may hold values from -0.09375 to 0.09375
- key_weight_matrix: bfloat16 [4096, 2048], P('kv', 'tp'), may hold values from -0.09375 to 0.09375
- value_weight_matrix: bfloat16 [4096, 2048], P('kv', 'tp'), may hold values from -0.09375 to 0.09375
- output_gate_weight: bfloat16 [4096, 2048], P('kv', 'tp'), may hold values from -0.09375 to 0.09375
- strength_weight: bfloat16 [4096, 16], replicated, may hold values from -0.375 to 0.375
- decay_weight: bfloat16 [4096, 16], replicated, may hold values from -0.75 to 0.75
- head_decay_speed: float32 [16], P('tp'), may hold values from 0.003 to 0.15
- head_decay_offset: float32 [16], P('tp'), may hold values from -4 to 4
- head_norm_gain: float32 [128], replicated, may hold values from 0.1 to 1.9
- mixer_out_weight: bfloat16 [2048, 4096], P('tp', 'kv'), may hold values from -0.125 to 0.125
- second_norm_gain: float32 [4096], P('kv'), may hold values from 0.1 to 1.9
- second_gate_weight: bfloat16 [4096, 10240], P('kv', 'tp'), may hold values from -0.09375 to 0.09375
- second_up_weight: bfloat16 [4096, 10240], P('kv', 'tp'), may hold values from -0.09375 to 0.09375
- second_down_weight: bfloat16 [10240, 4096], P('tp', 'kv'), may hold values from -0.0625 to 0.0625
- recurrent: float32 [256, 16, 128, 128], P('kv', 'tp'), may hold values from -1.25 to 1.25
- earlier_key_cache: bfloat16 [256, 64, 2048], P('kv', None, 'tp'), may hold values from -6 to 6
- earlier_value_cache: bfloat16 [256, 64, 2048], P('kv', None, 'tp'), may hold values from -6 to 6
- strength_logit_history: float32 [16, 256, 64], P('tp', 'kv'), may hold values from -6 to 6
- decay_input_history: float32 [16, 256, 64], P('tp', 'kv'), may hold values from -8 to 8
- position_decay_extra: float32 [16, 256, 64], P('tp', 'kv'), may hold values from -1 to 0
- lengths: int32 [256], P('kv'), may hold values from 1 to 64, 4096 in all
Outputs:
- layer_output: bfloat16 [256, 4096], P('tp', 'kv')
Inputs may be any that keep to these rules, and one draw needn't show every extreme that they name: `lengths`: positions at or beyond a sequence's length in its caches take no part; the new token sits at position length - 1.
All inputs are finite; a program needn't handle non-finite values. No bound on the sum of `lengths` on one device may be relied on, other than what follows from the above.
Results may differ from a plain program's by a relative error of at most 0.008.
Values may be sent and summed in bfloat16 or wider, within the bound.
No kernel may reach another device: no remote copies, remote signals or barrier semaphores. Data moves between devices by JAX's collectives and lax.ppermute only.
A program may use at most 64 MiB of HBM per device.

v0:
```python
import jax
import jax.numpy as jnp
from jax import lax
from jax.sharding import PartitionSpec as P

D = 4096


def cut_along(x, dim, count):
    before, after = (x.shape[:dim], x.shape[dim + 1 :])
    return jnp.moveaxis(x.reshape(*before, count, -1, *after), dim, 0)


def sent_and_summed(x, axis, dim):
    count = lax.axis_size(axis)
    parts = lax.all_to_all(cut_along(x, dim, count), axis, 0, 0, tiled=True)
    return jnp.sum(parts.astype(jnp.float32), axis=0)


def in_one_piece(arrays, axis, dim, along):
    columns = [a.reshape(*a.shape[:along], -1) for a in arrays]
    both = jnp.concatenate(columns, axis=along)
    result, at, outs = (sent_and_summed(both, axis, dim), 0, [])
    for a, column in zip(arrays, columns):
        share = result[..., at : at + column.shape[along]]
        outs.append(share.reshape(*share.shape[:along], *a.shape[along:]))
        at += column.shape[along]
    return tuple(outs)


def from_everyone(x, axis):
    count = lax.axis_size(axis)
    return lax.all_to_all(jnp.broadcast_to(x[None], (count, *x.shape)), axis, 0, 0, tiled=True)


def in_order(parts, dim):
    parts = jnp.moveaxis(parts, 0, dim)
    shape = parts.shape
    return parts.reshape(*shape[:dim], shape[dim] * shape[dim + 1], *shape[dim + 2 :])


def gather_directly(x, axis, dim):
    parts = from_everyone(x, axis)
    return in_order(parts, dim)


def over_copies(x, axis):
    return from_everyone(x, axis).sum(axis=0)


def sent_and_summed_2(x, axis, dim):
    parts = cut_along(x, dim, lax.axis_size(axis))
    arrived = lax.all_to_all(parts, axis, split_axis=0, concat_axis=0, tiled=True)
    return arrived.sum(axis=0)


def side_by_side(arrays, axis, dim, along):
    columns = [a.reshape(*a.shape[:along], -1) for a in arrays]
    both = jnp.concatenate(columns, axis=along)
    result, at, outs = (sent_and_summed_2(both, axis, dim), 0, [])
    for a, column in zip(arrays, columns):
        share = result[..., at : at + column.shape[along]]
        outs.append(share.reshape(*share.shape[:along], *a.shape[along:]))
        at += column.shape[along]
    return tuple(outs)


def taken_together(x, axis):
    return from_everyone(x, axis).astype(jnp.float32).sum(axis=0)


def delta_rule_block(
    current_query,
    current_key,
    current_value,
    output_gate_rows,
    strength_logit_current,
    decay_input_current,
    recurrent,
    earlier_key_cache,
    earlier_value_cache,
    strength_logit_history,
    decay_input_history,
    position_decay_extra,
    lengths,
    head_decay_speed,
    head_decay_offset,
    head_norm_gain,
):
    batch, heads, width = current_query.shape
    depth = current_value.shape[2]
    span = earlier_key_cache.shape[1]
    position = jnp.arange(span, dtype=jnp.int32)
    current = (lengths - 1)[:, None, None]
    is_new = position[None, None, :] == current
    live = position[None, None, :] <= current
    keys = (
        earlier_key_cache.astype(jnp.float32)
        .reshape(batch, span, heads, width)
        .transpose(0, 2, 1, 3)
    )
    keys = jnp.where(is_new[..., None], current_key[:, :, None, :], keys)
    keys = jnp.where(live[..., None], keys, 0.0)
    keys = keys * lax.rsqrt(jnp.sum(keys * keys, -1, keepdims=True) + 1e-06)
    values = (
        earlier_value_cache.astype(jnp.float32)
        .reshape(batch, span, heads, depth)
        .transpose(0, 2, 1, 3)
    )
    values = jnp.where(is_new[..., None], current_value[:, :, None, :], values)
    values = jnp.where(live[..., None], values, 0.0)
    beta = jax.nn.sigmoid(
        jnp.where(
            is_new, strength_logit_current[:, :, None], strength_logit_history.transpose(1, 0, 2)
        )
    )
    beta = jnp.where(live, beta, 0.0)
    block_record = jnp.where(
        is_new, decay_input_current[:, :, None], decay_input_history.transpose(1, 0, 2)
    )
    log_decay_amount = -head_decay_speed[None, :, None] * jax.nn.softplus(
        block_record + head_decay_offset[None, :, None]
    ) + position_decay_extra.transpose(1, 0, 2)
    log_decay_amount = jnp.where(live, log_decay_amount, 0.0)
    cumul = jnp.cumsum(log_decay_amount, -1)
    earlier = position[:, None] > position[None, :]
    within = position[:, None] >= position[None, :]
    gaps = jnp.exp(jnp.where(within, cumul[..., :, None] - cumul[..., None, :], -jnp.inf))
    gram = jnp.einsum("bhpk,bhsk->bhps", keys, keys, precision=lax.Precision.HIGHEST)
    coupling = jnp.where(earlier, beta[..., :, None] * gram * gaps, 0.0)
    system = coupling + jnp.eye(span, dtype=jnp.float32)
    right_side = jnp.concatenate(
        [values * beta[..., None], keys * (beta * jnp.exp(cumul))[..., None]], -1
    )
    solved = jax.scipy.linalg.solve_triangular(system, right_side, lower=True, unit_diagonal=True)
    updates = solved[..., :depth] - jnp.einsum(
        "bhpk,bhkv->bhpv", solved[..., depth:], recurrent, precision=lax.Precision.HIGHEST
    )
    query = (
        current_query
        * lax.rsqrt(jnp.sum(current_query * current_query, -1, keepdims=True) + 1e-06)
        * width ** (-0.5)
    )
    latest = jnp.sum(jnp.where(is_new, cumul, 0.0), -1)
    scores = jnp.einsum("bhk,bhsk->bhs", query, keys, precision=lax.Precision.HIGHEST)
    scores = scores * jnp.exp(jnp.where(live, latest[..., None] - cumul, -jnp.inf))
    carried = jnp.exp(latest)[..., None] * jnp.einsum(
        "bhk,bhkv->bhv", query, recurrent, precision=lax.Precision.HIGHEST
    )
    head_out = carried + jnp.einsum(
        "bhs,bhsv->bhv", scores, updates, precision=lax.Precision.HIGHEST
    )
    normed = head_out * lax.rsqrt(jnp.mean(head_out * head_out, -1, keepdims=True) + 1e-06)
    normed = normed * head_norm_gain[None, None, :] * jax.nn.silu(output_gate_rows)
    return normed.reshape(batch, heads * depth).astype(jnp.bfloat16)


def rounded(values):
    return lax.optimization_barrier(values.astype(jnp.bfloat16)).astype(jnp.float32)


def branch_partial(wide, gain, gate_w, up_w, down_w):
    scaled = (wide * gain[None, :]).astype(jnp.bfloat16)
    squares = jnp.sum(wide * wide, -1)
    gate_part = jnp.dot(scaled, gate_w, preferred_element_type=jnp.float32)
    up_part = jnp.dot(scaled, up_w, preferred_element_type=jnp.float32)
    gate_share, up_share, square_share = in_one_piece(
        (
            gate_part.astype(jnp.bfloat16),
            up_part.astype(jnp.bfloat16),
            squares.astype(jnp.bfloat16),
        ),
        "kv",
        0,
        1,
    )
    factor = lax.rsqrt(square_share / D + 1e-06)[:, None]
    hidden = (jax.nn.silu(gate_share * factor) * (up_share * factor)).astype(jnp.bfloat16)
    return jnp.dot(gather_directly(hidden, "kv", 0), down_w, preferred_element_type=jnp.float32)


def body(
    tokens,
    first_norm_gain,
    first_gate_weight,
    first_up_weight,
    first_down_weight,
    mixer_norm_gain,
    query_weight_matrix,
    key_weight_matrix,
    value_weight_matrix,
    output_gate_weight,
    strength_weight,
    decay_weight,
    head_decay_speed,
    head_decay_offset,
    head_norm_gain,
    mixer_out_weight,
    second_norm_gain,
    second_gate_weight,
    second_up_weight,
    second_down_weight,
    recurrent,
    earlier_key_cache,
    earlier_value_cache,
    strength_logit_history,
    decay_input_history,
    position_decay_extra,
    lengths,
):
    whole = gather_directly(tokens, "tp", 0)
    first_wide = whole.astype(jnp.float32)
    first_part = branch_partial(
        first_wide, first_norm_gain, first_gate_weight, first_up_weight, first_down_weight
    )
    first_branch = over_copies(first_part, "tp")
    middle = rounded(first_wide + 0.5 * first_branch)
    mix_input = (middle * mixer_norm_gain[None, :]).astype(jnp.bfloat16)
    heads = head_decay_speed.shape[0]
    slice_rows = mix_input.shape[1]
    corner = (lax.axis_index("kv") * slice_rows, lax.axis_index("tp") * heads)
    small_cols = jnp.concatenate(
        [
            lax.dynamic_slice(strength_weight, corner, (slice_rows, heads)),
            lax.dynamic_slice(decay_weight, corner, (slice_rows, heads)),
        ],
        1,
    )
    query_part = jnp.dot(mix_input, query_weight_matrix, preferred_element_type=jnp.float32)
    key_part = jnp.dot(mix_input, key_weight_matrix, preferred_element_type=jnp.float32)
    value_part = jnp.dot(mix_input, value_weight_matrix, preferred_element_type=jnp.float32)
    gate_part = jnp.dot(mix_input, output_gate_weight, preferred_element_type=jnp.float32)
    logit_part = jnp.dot(mix_input, small_cols, preferred_element_type=jnp.float32)
    squares = jnp.sum(middle * middle, -1)
    query_rows, key_rows, value_rows, gate_rows, logit_rows, square_rows = side_by_side(
        (query_part, key_part, value_part, gate_part, logit_part, squares), "kv", 0, 1
    )
    factor = lax.rsqrt(square_rows / D + 1e-06)[:, None]
    local = query_rows.shape[0]
    current_query = (query_rows * factor).reshape(local, heads, -1)
    current_key = (key_rows * factor).reshape(local, heads, -1)
    current_value = (value_rows * factor).reshape(local, heads, -1)
    output_gate_rows = (gate_rows * factor).reshape(local, heads, -1)
    logits = logit_rows * factor
    mixed = delta_rule_block(
        current_query,
        current_key,
        current_value,
        output_gate_rows,
        logits[:, :heads],
        logits[:, heads:],
        recurrent,
        earlier_key_cache,
        earlier_value_cache,
        strength_logit_history,
        decay_input_history,
        position_decay_extra,
        lengths,
        head_decay_speed,
        head_decay_offset,
        head_norm_gain,
    )
    mixer_part = jnp.dot(
        gather_directly(mixed, "kv", 0), mixer_out_weight, preferred_element_type=jnp.float32
    )
    mixer_branch = taken_together(mixer_part.astype(jnp.bfloat16), "tp").astype(jnp.float32)
    second = rounded(middle + mixer_branch)
    last_part = branch_partial(
        second, second_norm_gain, second_gate_weight, second_up_weight, second_down_weight
    )
    last_branch = sent_and_summed(last_part.astype(jnp.bfloat16), "tp", 0)
    count = tokens.shape[0]
    own_rows = lax.dynamic_slice_in_dim(second, lax.axis_index("tp") * count, count, 0)
    return (own_rows + 0.5 * last_branch).astype(jnp.bfloat16)


def solution(mesh):
    return jax.shard_map(
        body,
        mesh=mesh,
        in_specs=(
            P("tp", "kv"),
            P("kv"),
            P("kv", "tp"),
            P("kv", "tp"),
            P("tp", "kv"),
            P("kv"),
            P("kv", "tp"),
            P("kv", "tp"),
            P("kv", "tp"),
            P("kv", "tp"),
            P(),
            P(),
            P("tp"),
            P("tp"),
            P(),
            P("tp", "kv"),
            P("kv"),
            P("kv", "tp"),
            P("kv", "tp"),
            P("tp", "kv"),
            P("kv", "tp", None, None),
            P("kv", None, "tp"),
            P("kv", None, "tp"),
            P("tp", "kv", None),
            P("tp", "kv", None),
            P("tp", "kv", None),
            P("kv"),
        ),
        out_specs=P("tp", "kv"),
        check_vma=False,
    )
```

profile of v0, /device:TPU:1, one launch (start us, length us, event | category | flops | bytes accessed | tf_op | source)
XLA Modules:
  0.0 359.3 jit_solution(14318786925854877529)
XLA Ops:
  0.0 0.8 broadcast_in_dim.149
  0.8 13.9 %all_to_all.50 = bf16[16,16,128]{2,1,0:T(8,128)(2,1)S(1)} all-to-all(bf16[16,16,128]{2,1,0:T(8,128)(2,1)S(1)} %broadcast_in_dim.149), channel_id=1, replica_groups=mesh['kv'=32,'tp'=16] {'tp'}, dimensions={0} | all-to-all | bytes 131072 | tf_op jit(solution)/shard_map/all_to_all | solution.py:33
  15.3 1.1 fusion
  16.5 1.1 fusion.1
  18.0 59.1 %all_to_all.51 = bf16[32,8,1281]{2,1,0:T(8,128)(2,1)S(1)} all-to-all(bf16[32,8,1281]{2,1,0:T(8,128)(2,1)S(1)} %pad_maximum_fusion), channel_id=1, replica_groups=mesh['kv'=32,'tp'=16] {'kv'}, dimensions={0} | all-to-all | bytes 1311744 | tf_op jit(solution)/shard_map/all_to_all | solution.py:16
  77.4 28.2 %all_to_all.52 = bf16[32,8,640]{2,1,0:T(8,128)(2,1)S(1)} all-to-all(bf16[32,8,640]{2,1,0:T(8,128)(2,1)S(1)} %broadcast_in_dim.150), channel_id=1, replica_groups=mesh['kv'=32,'tp'=16] {'kv'}, dimensions={0} | all-to-all | bytes 655360 | tf_op jit(solution)/shard_map/all_to_all | solution.py:33
  105.8 1.6 broadcast_in_dim.151
  107.4 3.7 %all-to-all-start.3 = ((f32[16,256,128]{2,1,0:T(8,128)}), f32[16,256,128]{2,1,0:T(8,128)S(1)}, u32[]{:S(2)}, u32[]{:S(2)}) async-start(f32[16,256,128]{2,1,0:T(8,128)} %broadcast_in_dim.151), calls=%async_computation.3 | async-start | bytes 4194304 | tf_op jit(solution)/shard_map/all_to_all | solution.py:33
  111.1 0.8 dynamic_slice.10
  111.9 0.8 dynamic_slice.9
  112.7 29.5 %all-to-all-done.3 = f32[16,256,128]{2,1,0:T(8,128)S(1)} async-done(((f32[16,256,128]{2,1,0:T(8,128)}), f32[16,256,128]{2,1,0:T(8,128)S(1)}, u32[]{:S(2)}, u32[]{:S(2)}) %all-to-all-start.3) | async-done | bytes 2097184 | tf_op jit(solution)/shard_map/all_to_all | solution.py:33
  143.4 0.9 concatenate.48
  144.3 5.9 %all-to-all-start.4 = ((f32[32,8,515]{2,1,0:T(8,128)}), f32[32,8,515]{2,1,0:T(8,128)S(1)}, u32[]{:S(2)}, u32[]{:S(2)}) async-start(f32[32,8,515]{2,1,0:T(8,128)} %concatenate.48), calls=%async_computation.4 | async-start | bytes 1310720 | tf_op jit(solution)/shard_map/all_to_all | solution.py:53
  151.7 37.5 %all-to-all-done.4 = f32[32,8,515]{2,1,0:T(8,128)S(1)} async-done(((f32[32,8,515]{2,1,0:T(8,128)}), f32[32,8,515]{2,1,0:T(8,128)S(1)}, u32[]{:S(2)}, u32[]{:S(2)}) %all-to-all-start.4) | async-done | bytes 527392 | tf_op jit(solution)/shard_map/all_to_all | solution.py:53
  190.8 0.7 fusion.23
  191.6 1.0 fusion.11
  192.6 39.3 %custom-call.4 = f32[8,1,64,64]{2,3,1,0:T(8,128)S(1)} custom-call(f32[8,1,64,64]{3,2,1,0:T(8,128)S(1)} %fusion.11), custom_call_target="InvertDiagBlocksLowerTriangular" | custom-call | tf_op jit(solution)/shard_map/jit(_solve_triangular)/vmap()/triangular_solve | solution.py:135
  234.8 16.3 %all_to_all.53 = bf16[32,8,128]{2,1,0:T(8,128)(2,1)S(1)} all-to-all(bf16[32,8,128]{2,1,0:T(8,128)(2,1)S(1)} %broadcast_in_dim.166), channel_id=1, replica_groups=mesh['kv'=32,'tp'=16] {'kv'}, dimensions={0} | all-to-all | bytes 131072 | tf_op jit(solution)/shard_map/all_to_all | solution.py:33
  251.5 18.7 %all_to_all.54 = bf16[16,256,128]{2,1,0:T(8,128)(2,1)S(1)} all-to-all(bf16[16,256,128]{2,1,0:T(8,128)(2,1)S(1)} %broadcast_in_dim.167), channel_id=1, replica_groups=mesh['kv'=32,'tp'=16] {'tp'}, dimensions={0} | all-to-all | bytes 2097152 | tf_op jit(solution)/shard_map/all_to_all | solution.py:33
  271.6 47.7 %all_to_all.55 = bf16[32,8,1281]{2,1,0:T(8,128)(2,1)S(1)} all-to-all(bf16[32,8,1281]{2,1,0:T(8,128)(2,1)S(1)} %pad_maximum_fusion.1), channel_id=1, replica_groups=mesh['kv'=32,'tp'=16] {'kv'}, dimensions={0} | all-to-all | bytes 1311744 | tf_op jit(solution)/shard_map/all_to_all | solution.py:16
  319.6 28.2 %all_to_all.56 = bf16[32,8,640]{2,1,0:T(8,128)(2,1)S(1)} all-to-all(bf16[32,8,640]{2,1,0:T(8,128)(2,1)S(1)} %broadcast_in_dim.168), channel_id=1, replica_groups=mesh['kv'=32,'tp'=16] {'kv'}, dimensions={0} | all-to-all | bytes 655360 | tf_op jit(solution)/shard_map/all_to_all | solution.py:33
  347.8 0.9 convolution_convert_fusion.4
  348.7 3.5 all-to-all-start.9
  352.2 6.5 %all-to-all-done.9 = bf16[16,16,128]{2,1,0:T(8,128)(2,1)S(1)} async-done(((bf16[16,16,128]{2,1,0:T(8,128)(2,1)}), bf16[16,16,128]{2,1,0:T(8,128)(2,1)S(1)}, u32[]{:S(2)}, u32[]{:S(2)}) %all-to-all-start.9) | async-done | bytes 65568 | tf_op jit(solution)/shard_map/all_to_all | solution.py:16
  (101 shorter events, 10.1 us)
Async XLA Ops:
  0.0 231.9 %copy-start = (f32[8,1,128,128]{3,2,1,0:T(8,128)S(1)}, f32[8,1,128,128]{3,2,1,0:T(8,128)}, u32[]{:S(2)}) copy-start(f32[8,1,128,128]{3,2,1,0:T(8,128)} %param.47) | copy-start | bytes 1572868
  17.9 87.6 %copy-start.4 = (bf16[640,128]{1,0:T(8,128)(2,1)S(1)}, bf16[640,128]{1,0:T(8,128)(2,1)}, u32[]{:S(2)}) copy-start(bf16[640,128]{1,0:T(8,128)(2,1)} %param.31) | copy-start | bytes 491524
  107.4 34.7 %all-to-all-start.3 = ((f32[16,256,128]{2,1,0:T(8,128)}), f32[16,256,128]{2,1,0:T(8,128)S(1)}, u32[]{:S(2)}, u32[]{:S(2)}) async-start(f32[16,256,128]{2,1,0:T(8,128)} %broadcast_in_dim.151), calls=%async_computation.3 | async-start | bytes 4194304 | tf_op jit(solution)/shard_map/all_to_all | solution.py:33
  111.1 31.5 %copy-start.7 = (bf16[128,128]{1,0:T(8,128)(2,1)S(1)}, bf16[128,128]{1,0:T(8,128)(2,1)}, u32[]{:S(2)}) copy-start(bf16[128,128]{1,0:T(8,128)(2,1)} %param.36) | copy-start | bytes 98308
  111.1 31.5 %copy-start.12 = (f32[128]{0:T(128)S(1)}, f32[128]{0:T(128)}, u32[]{:S(2)}) copy-start(f32[128]{0:T(128)} %param.32) | copy-start | bytes 1540
  112.7 30.1 %copy-start.8 = (bf16[128,128]{1,0:T(8,128)(2,1)S(1)}, bf16[128,128]{1,0:T(8,128)(2,1)}, u32[]{:S(2)}) copy-start(bf16[128,128]{1,0:T(8,128)(2,1)} %param.35) | copy-start | bytes 98308
  112.7 30.3 %copy-start.9 = (bf16[128,128]{1,0:T(8,128)(2,1)S(1)}, bf16[128,128]{1,0:T(8,128)(2,1)}, u32[]{:S(2)}) copy-start(bf16[128,128]{1,0:T(8,128)(2,1)} %param.34) | copy-start | bytes 98308
  112.7 30.4 %copy-start.10 = (bf16[128,128]{1,0:T(8,128)(2,1)S(1)}, bf16[128,128]{1,0:T(8,128)(2,1)}, u32[]{:S(2)}) copy-start(bf16[128,128]{1,0:T(8,128)(2,1)} %param.33) | copy-start | bytes 98308
  143.4 8.2 %copy-start.18 = (s32[8]{0:T(128)S(1)}, s32[8]{0:T(128)}, u32[]{:S(2)}) copy-start(s32[8]{0:T(128)} %param.53) | copy-start | bytes 100
  143.4 46.4 %copy-start.1 = (bf16[8,64,128]{2,1,0:T(8,128)(2,1)S(1)}, bf16[8,64,128]{2,1,0:T(8,128)(2,1)}, u32[]{:S(2)}) copy-start(bf16[8,64,128]{2,1,0:T(8,128)(2,1)} %param.48) | copy-start | bytes 393220
  144.3 46.0 %copy-start.13 = (f32[1,8,64]{2,1,0:T(8,128)S(1)}, f32[1,8,64]{2,1,0:T(8,128)}, u32[]{:S(2)}) copy-start(f32[1,8,64]{2,1,0:T(8,128)} %param.52) | copy-start | bytes 6148
  144.3 46.0 %copy-start.14 = (f32[1,8,64]{2,1,0:T(8,128)S(1)}, f32[1,8,64]{2,1,0:T(8,128)}, u32[]{:S(2)}) copy-start(f32[1,8,64]{2,1,0:T(8,128)} %param.51) | copy-start | bytes 6148
  144.3 47.2 %copy-start.15 = (f32[1,8,64]{2,1,0:T(8,128)S(1)}, f32[1,8,64]{2,1,0:T(8,128)}, u32[]{:S(2)}) copy-start(f32[1,8,64]{2,1,0:T(8,128)} %param.50) | copy-start | bytes 6148
  144.3 44.8 %all-to-all-start.4 = ((f32[32,8,515]{2,1,0:T(8,128)}), f32[32,8,515]{2,1,0:T(8,128)S(1)}, u32[]{:S(2)}, u32[]{:S(2)}) async-start(f32[32,8,515]{2,1,0:T(8,128)} %concatenate.48), calls=%async_computation.4 | async-start | bytes 1310720 | tf_op jit(solution)/shard_map/all_to_all | solution.py:53
  189.2 43.3 %copy-start.6 = (bf16[8,64,128]{2,1,0:T(8,128)(2,1)S(1)}, bf16[8,64,128]{2,1,0:T(8,128)(2,1)}, u32[]{:S(2)}) copy-start(bf16[8,64,128]{2,1,0:T(8,128)(2,1)} %param.49) | copy-start | bytes 393220
  232.9 1.8 copy-start.17
  232.9 18.2 %copy-start.11 = (bf16[128,128]{1,0:T(8,128)(2,1)S(1)}, bf16[128,128]{1,0:T(8,128)(2,1)}, u32[]{:S(2)}) copy-start(bf16[128,128]{1,0:T(8,128)(2,1)} %param.42) | copy-start | bytes 98308
  251.4 19.0 %copy-start.2 = (bf16[128,640]{1,0:T(8,128)(2,1)S(1)}, bf16[128,640]{1,0:T(8,128)(2,1)}, u32[]{:S(2)}) copy-start(bf16[128,640]{1,0:T(8,128)(2,1)} %param.44) | copy-start | bytes 491524
  251.4 19.0 %copy-start.16 = (f32[128]{0:T(128)S(1)}, f32[128]{0:T(128)}, u32[]{:S(2)}) copy-start(f32[128]{0:T(128)} %param.43) | copy-start | bytes 1540
  270.1 0.9 copy-start.3
  271.6 76.2 %copy-start.5 = (bf16[640,128]{1,0:T(8,128)(2,1)S(1)}, bf16[640,128]{1,0:T(8,128)(2,1)}, u32[]{:S(2)}) copy-start(bf16[640,128]{1,0:T(8,128)(2,1)} %param.46) | copy-start | bytes 491524
  348.7 10.0 %all-to-all-start.9 = ((bf16[16,16,128]{2,1,0:T(8,128)(2,1)}), bf16[16,16,128]{2,1,0:T(8,128)(2,1)S(1)}, u32[]{:S(2)}, u32[]{:S(2)}) async-start(bf16[16,16,128]{2,1,0:T(8,128)(2,1)} %bitcast.40), calls=%async_computation.9 | async-start | bytes 131072 | tf_op jit(solution)/shard_map/all_to_all | solution.py:16
where the time goes:
time: 360 us; the launch traced here: 359 us
  blocking collectives  212 us (59%)
  waiting for transfers between devices  73.4 us (20%)
  other arithmetic  44.4 us (12%)
  starting transfers between devices  13.1 us (4%)
  matrix products  8.43 us (2%)
  local copies, waits for them, and re-layouts  6.25 us (2%)
    all_to_all x2, blocking collectives, sent_and_summed(): parts = lax.all_to_all(cut_along(x, dim, count), axis, 0, 0, tiled=True)  107 us
    all_to_all x5, blocking collectives, from_everyone(): lax.all_to_all(jnp.broadcast_to(x[None], (count, *x.shape)), axis, 0, 0,...  105 us
    another operation x4, other arithmetic, delta_rule_block(): jax.scipy.linalg.solve_triangular(system, right_side, lower=True, unit_di...  39.4 us
    all_to_all x1, waiting for transfers between devices, sent_and_summed_2(): lax.all_to_all(parts, axis, split_axis=0, concat_axis=0, tiled=True)  37.5 us
    all_to_all x1, waiting for transfers between devices, from_everyone(): lax.all_to_all(jnp.broadcast_to(x[None], (count, *x.shape)), axis, 0, 0,...  29.5 us
  transfers between devices with their start and end apart: 3, of which 3 were waited for; matrix products, arithmetic and copies ran while one was open for 0% of the time, Pallas kernels for 0%

commit v1 on v0

v1 whole, which is shorter than its diff:
```python
import jax
import jax.numpy as jnp
from jax import lax
from jax.sharding import Mesh, PartitionSpec as P

D = 4096
HIGHEST = lax.Precision.HIGHEST
f32 = jnp.float32
bf16 = jnp.bfloat16


def swap(x):
    return lax.ppermute(x, "c", [(0, 1), (1, 0)])


def to_all(x, axis):
    count = lax.axis_size(axis)
    return lax.all_to_all(jnp.broadcast_to(x[None], (count, *x.shape)), axis, 0, 0, tiled=True)


def summed(x, axis):
    count = lax.axis_size(axis)
    parts = lax.all_to_all(x.reshape(count, -1, *x.shape[1:]), axis, 0, 0, tiled=True)
    return jnp.sum(parts.astype(f32), axis=0)


def dot(x, w):
    return jnp.dot(x, w, preferred_element_type=f32)


def hi_lo(x):
    hi = x.astype(bf16)
    lo = (x - hi.astype(f32)).astype(bf16)
    return [hi, lo]


def columns(parts, width):
    used = sum(p.shape[1] for p in parts)
    fill = jnp.zeros((parts[0].shape[0], width - used), bf16)
    return jnp.concatenate([*parts, fill], axis=1)


def branch(wide, gain, gates, ups, downs):
    half = wide.shape[1] // 2
    scaled = (wide * gain).astype(bf16)
    squares = jnp.sum(wide * wide, -1, keepdims=True)
    own, other = scaled[:, :half], scaled[:, half:]
    gate = dot(own, gates[0]) + dot(other, gates[1])
    up = dot(own, ups[0]) + dot(other, ups[1])
    n = gate.shape[1]
    sent = columns([gate.astype(bf16), up.astype(bf16), *hi_lo(squares)], 2 * n + 128)
    got = summed(sent, "z")
    square = got[:, 2 * n : 2 * n + 1] + got[:, 2 * n + 1 : 2 * n + 2]
    factor = lax.rsqrt(square / D + 1e-06)
    hidden = (jax.nn.silu(got[:, :n] * factor) * (got[:, n : 2 * n] * factor)).astype(bf16)
    hidden = to_all(hidden, "z").reshape(-1, n)
    return [dot(hidden, down) for down in downs]


def earlier_state(
    recurrent, key_cache, value_cache, strength, decay, extra, lengths, speed, offset
):
    span = key_cache.shape[1]
    position = jnp.arange(span, dtype=jnp.int32)
    before = position[None, :] < (lengths - 1)[:, None]
    keys = jnp.where(before[..., None], key_cache.astype(f32), 0.0)
    keys = keys * lax.rsqrt(jnp.sum(keys * keys, -1, keepdims=True) + 1e-06)
    values = jnp.where(before[..., None], value_cache.astype(f32), 0.0)
    beta = jnp.where(before, jax.nn.sigmoid(strength), 0.0)
    amount = jnp.where(before, -speed * jax.nn.softplus(decay + offset) + extra, 0.0)
    upto = (position[:, None] <= position[None, :]).astype(f32)
    cumul = jnp.dot(amount, upto, precision=HIGHEST)
    last = cumul[:, -1:]
    earlier = position[:, None] > position[None, :]
    gaps = jnp.exp(jnp.where(earlier, cumul[:, :, None] - cumul[:, None, :], -jnp.inf))
    gram = jnp.einsum("bpk,bsk->bps", keys, keys, precision=HIGHEST)
    coupling = beta[:, :, None] * gram * gaps

    def mm(a, b):
        return jnp.einsum("bps,bsr->bpr", a, b, precision=HIGHEST)

    eye = jnp.eye(span, dtype=f32)

    def same(size):
        return (position[:, None] // size) == (position[None, :] // size)

    first = jnp.where(same(8), coupling, 0.0)
    second = mm(first, first)
    fourth = mm(second, second)
    inverse = mm(mm(eye - first, eye + second), eye + fourth)
    size = 8
    while size < span:
        below = jnp.where(same(2 * size) & ~same(size), coupling, 0.0)
        inverse = inverse - mm(mm(inverse, below), inverse)
        size *= 2
    carried = jnp.einsum("bpk,bkv->bpv", keys, recurrent, precision=HIGHEST)
    right = beta[..., None] * (values - jnp.exp(cumul)[..., None] * carried)
    updates = mm(inverse, right) * jnp.exp(last - cumul)[..., None]
    return jnp.exp(last)[..., None] * recurrent + jnp.einsum(
        "bpk,bpv->bkv", keys, updates, precision=HIGHEST
    )


def body(
    tokens,
    first_norm_gain,
    first_gate_weight,
    first_up_weight,
    first_down_weight,
    mixer_norm_gain,
    query_weight_matrix,
    key_weight_matrix,
    value_weight_matrix,
    output_gate_weight,
    strength_weight,
    decay_weight,
    head_decay_speed,
    head_decay_offset,
    head_norm_gain,
    mixer_out_weight,
    second_norm_gain,
    second_gate_weight,
    second_up_weight,
    second_down_weight,
    recurrent,
    earlier_key_cache,
    earlier_value_cache,
    strength_logit_history,
    decay_input_history,
    position_decay_extra,
    lengths,
):
    core, tp, z = lax.axis_index("c"), lax.axis_index("tp"), lax.axis_index("z")
    plane = lax.axis_size("tp")
    count, width = tokens.shape
    rows = count // 2

    def pair(x):
        return x, swap(x)

    gate1, up1, down1 = pair(first_gate_weight), pair(first_up_weight), pair(first_down_weight)
    gate2, up2, down2 = pair(second_gate_weight), pair(second_up_weight), pair(second_down_weight)
    projections = pair(
        jnp.concatenate(
            [query_weight_matrix, key_weight_matrix, value_weight_matrix, output_gate_weight], 1
        )
    )
    outs = pair(mixer_out_weight)
    gains = jnp.stack([first_norm_gain, mixer_norm_gain, second_norm_gain])
    gains = jnp.concatenate(pair(gains), axis=1)

    def small(which):
        corner = ((z * 2 + which) * width, tp)
        return jnp.concatenate(
            [lax.dynamic_slice(w, corner, (width, 1)) for w in (strength_weight, decay_weight)], 1
        )

    smalls = small(core), small(1 - core)

    state = earlier_state(
        recurrent[:, 0],
        earlier_key_cache,
        earlier_value_cache,
        strength_logit_history[0],
        decay_input_history[0],
        position_decay_extra[0],
        lengths,
        head_decay_speed[0],
        head_decay_offset[0],
    )

    blocks = jnp.broadcast_to(tokens.reshape(2, 1, rows, width), (2, plane, rows, width))
    got = lax.all_to_all(
        blocks.reshape(2 * plane, rows, width), ("c", "tp"), 0, 0, tiled=True
    ).reshape(2, plane * rows, width)
    wide = jnp.where(
        core == 0,
        jnp.concatenate([got[0], got[1]], 1),
        jnp.concatenate([got[1], got[0]], 1),
    ).astype(f32)

    part = branch(wide, gains[0], gate1, up1, down1)
    first_sum = summed(jnp.concatenate([p.astype(bf16) for p in part], 1), "tp")
    wide_own = lax.dynamic_slice_in_dim(wide, tp * rows, rows, 0)
    middle_own = (wide_own + 0.5 * first_sum).astype(bf16)
    middle = to_all(middle_own, "tp").reshape(-1, 2 * width).astype(f32)

    mix = (middle * gains[1]).astype(bf16)
    own, other = mix[:, :width], mix[:, width:]
    main = dot(own, projections[0]) + dot(other, projections[1])
    logit = dot(own, smalls[0]) + dot(other, smalls[1])
    squares = jnp.sum(middle * middle, -1, keepdims=True)
    n = main.shape[1]
    tail = hi_lo(jnp.concatenate([logit, squares], 1))
    got = summed(columns([main.astype(bf16), *tail], n + 128), "z")
    small_sums = got[:, n : n + 3] + got[:, n + 3 : n + 6]
    factor = lax.rsqrt(small_sums[:, 2:3] / D + 1e-06)
    dk = n // 4
    new_query, new_key, new_value, out_gate = [
        got[:, i * dk : (i + 1) * dk] * factor for i in range(4)
    ]
    beta = jax.nn.sigmoid(small_sums[:, 0:1] * factor)
    span = earlier_key_cache.shape[1]
    position = jnp.arange(span, dtype=jnp.int32)
    extra_new = jnp.sum(
        jnp.where(position[None, :] == (lengths - 1)[:, None], position_decay_extra[0], 0.0),
        -1,
        keepdims=True,
    )
    amount = (
        -head_decay_speed * jax.nn.softplus(small_sums[:, 1:2] * factor + head_decay_offset)
        + extra_new
    )
    query = new_query * lax.rsqrt(jnp.sum(new_query * new_query, -1, keepdims=True) + 1e-06)
    query = query * dk ** (-0.5)
    key = new_key * lax.rsqrt(jnp.sum(new_key * new_key, -1, keepdims=True) + 1e-06)
    score = jnp.sum(query * key, -1, keepdims=True)
    reduced = query - (score * beta) * key
    head_out = jnp.exp(amount) * jnp.einsum(
        "bk,bkv->bv", reduced, state, precision=HIGHEST
    ) + (score * beta) * new_value
    normed = head_out * lax.rsqrt(jnp.mean(head_out * head_out, -1, keepdims=True) + 1e-06)
    mixed = (normed * head_norm_gain[None, :] * jax.nn.silu(out_gate)).astype(bf16)

    mixed = to_all(mixed, "z").reshape(-1, dk)
    part = [dot(mixed, w) for w in outs]
    mixer_sum = summed(jnp.concatenate([p.astype(bf16) for p in part], 1), "tp")
    second_own = (middle_own.astype(f32) + mixer_sum).astype(bf16)
    got = to_all(second_own, ("c", "tp")).reshape(2, plane, rows, 2 * width)
    second = lax.dynamic_index_in_dim(got, core, 0, keepdims=False)
    second = second.reshape(-1, 2 * width).astype(f32)

    part = [p.astype(bf16) for p in branch(second, gains[2], gate2, up2, down2)]
    ordered = jnp.where(core == 0, jnp.stack(part), jnp.stack(part[::-1]))
    last = lax.all_to_all(
        ordered.reshape(2 * plane, rows, width), ("c", "tp"), 0, 0, tiled=True
    ).reshape(2, plane, rows, width)
    last = jnp.sum(last.astype(f32), axis=1).reshape(count, width)
    mine = lax.dynamic_index_in_dim(got, tp, 1, keepdims=False)
    flip = (lax.broadcasted_iota(jnp.int32, (2, 1, 1), 0) == core)
    mine = jnp.where(flip, mine[..., :width], mine[..., width:]).reshape(count, width)
    return (mine.astype(f32) + 0.5 * last).astype(bf16)


def solution(mesh):
    kv, tp = mesh.shape["kv"], mesh.shape["tp"]
    split = Mesh(mesh.devices.reshape(kv // 2, 2, tp), ("z", "c", "tp"))
    kv = ("z", "c")
    return jax.shard_map(
        body,
        mesh=split,
        in_specs=(
            P("tp", kv),
            P(kv),
            P(kv, "tp"),
            P(kv, "tp"),
            P("tp", kv),
            P(kv),
            P(kv, "tp"),
            P(kv, "tp"),
            P(kv, "tp"),
            P(kv, "tp"),
            P(),
            P(),
            P("tp"),
            P("tp"),
            P(),
            P("tp", kv),
            P(kv),
            P(kv, "tp"),
            P(kv, "tp"),
            P("tp", kv),
            P(kv, "tp", None, None),
            P(kv, None, "tp"),
            P(kv, None, "tp"),
            P("tp", kv, None),
            P("tp", kv, None),
            P("tp", kv, None),
            P(kv),
        ),
        out_specs=P("tp", kv),
        check_vma=False,
    )
```

time: 360 us -> 249 us (0.69)
  blocking collectives: 212 us -> 28.6 us
  starting transfers between devices: 13.1 us -> 114 us
  other arithmetic: 44.4 us -> 5.86 us
  local copies, waits for them, and re-layouts: 6.25 us -> 14.2 us
    all_to_all x7 -> x2, blocking collectives: 212 us -> 28.6 us  [summed(): lax.all_to_all(x.reshape(count, -1, *x.shape[1:]), axis, 0, 0, tiled=True)]
    all_to_all x3 -> x10, starting transfers between devices: 13.1 us -> 83.6 us  [the longest x5 43.7 us: to_all(): lax.all_to_all(jnp.broadcast_to(x[None], (count, *x.shape)), axis, 0, 0,...]
    another operation x5 -> x1, other arithmetic: 39.6 us -> 0.73 us  [body(): gains = jnp.stack([first_norm_gain, mixer_norm_gain, second_norm_gain])]
    ppermute x0 -> x9, starting transfers between devices: none -> 30.8 us  [swap(): return lax.ppermute(x, 'c', [(0, 1), (1, 0)])]
    unnamed x38 -> x47, local copies, waits for them, and re-layouts: 0.49 us -> 5.32 us
    dot_general x16 -> x34, matrix products: 7.65 us -> 11.2 us  [the longest x11 4.26 us: mm(): return jnp.einsum('bps,bsr->bpr', a, b, precision=HIGHEST)]
    all_to_all x3 -> x10, waiting for transfers between devices: 73.4 us -> 70.4 us  [the longest x5 33.1 us: to_all(): lax.all_to_all(jnp.broadcast_to(x[None], (count, *x.shape)), axis, 0, 0,...]
  transfers between devices with their start and end apart: 3 -> 19, of which waited for: 3 -> 9; matrix products, arithmetic and copies ran while one was open for 0% -> 7% of each run, Pallas kernels for 0% -> 0%
where the time goes in v1:
time: 249 us; the launch traced here: 247 us
  starting transfers between devices  114 us (46%)
  waiting for transfers between devices  70.5 us (28%)
  blocking collectives  28.6 us (11%)
  local copies, waits for them, and re-layouts  14.2 us (6%)
  matrix products  11.2 us (4%)
  other arithmetic  5.86 us (2%)
    all_to_all x5, starting transfers between devices, to_all(): lax.all_to_all(jnp.broadcast_to(x[None], (count, *x.shape)), axis, 0, 0,...  43.7 us
    all_to_all x5, waiting for transfers between devices, to_all(): lax.all_to_all(jnp.broadcast_to(x[None], (count, *x.shape)), axis, 0, 0,...  33.1 us
    ppermute x9, starting transfers between devices, swap(): return lax.ppermute(x, 'c', [(0, 1), (1, 0)])  30.8 us
    all_to_all x3, waiting for transfers between devices, summed(): lax.all_to_all(x.reshape(count, -1, *x.shape[1:]), axis, 0, 0, tiled=True)  30.3 us
    all_to_all x2, blocking collectives, summed(): lax.all_to_all(x.reshape(count, -1, *x.shape[1:]), axis, 0, 0, tiled=True)  28.6 us
    all_to_all x3, starting transfers between devices, summed(): lax.all_to_all(x.reshape(count, -1, *x.shape[1:]), axis, 0, 0, tiled=True)  27.6 us
    all_to_all x1, starting transfers between devices, body(): lax.all_to_all(ordered.reshape(2 * plane, rows, width), ('c', 'tp'), 0, 0...  8.07 us
    all_to_all x1, waiting for transfers between devices, body(): lax.all_to_all(ordered.reshape(2 * plane, rows, width), ('c', 'tp'), 0, 0...  7.08 us
  transfers between devices with their start and end apart: 19, of which 9 were waited for; matrix products, arithmetic and copies ran while one was open for 7% of the time, Pallas kernels for 0%

profile of v1, /device:TPU:1, one launch (start us, length us, event | category | flops | bytes accessed | tf_op | source)
XLA Modules:
  0.0 247.0 jit_solution(2650534391322852380)
XLA Ops:
  0.7 8.7 %collective-permute-start = (f32[3,128]{1,0:T(4,128)S(1)}, f32[3,128]{1,0:T(4,128)S(1)}, u32[]{:S(2)}, u32[]{:S(2)}) collective-permute-start(f32[3,128]{1,0:T(4,128)S(1)} %pad_maximum_fusion.2), channel_id=1, source_target_pairs={{0,16},{16,0},{1,17},{17,1},{2,18},{18,2},{3,19},{19,3},{4,20},{20... | collective-permute-start | bytes 4616 | tf_op jit(solution)/shard_map/ppermute | solution.py:13
  12.7 4.2 %all-to-all-start = ((bf16[32,8,128]{2,1,0:T(8,128)(2,1)}), bf16[32,8,128]{2,1,0:T(8,128)(2,1)S(1)}, u32[]{:S(2)}, u32[]{:S(2)}) async-start(bf16[32,8,128]{2,1,0:T(8,128)(2,1)} %bitcast.1), calls=%async_computation | async-start | bytes 131072 | tf_op jit(solution)/shard_map/all_to_all | solution.py:173
  33.6 13.0 %all-to-all-start.1 = ((bf16[16,8,1408]{2,1,0:T(8,128)(2,1)}), bf16[16,8,1408]{2,1,0:T(8,128)(2,1)S(1)}, u32[]{:S(2)}, u32[]{:S(2)}) async-start(bf16[16,8,1408]{2,1,0:T(8,128)(2,1)} %concatenate.54), calls=%async_computation.1 | async-start | bytes 720896 | tf_op jit(solution)/shard_map/all_to_all | solution.py:23
  49.0 13.7 %all-to-all-done.1 = bf16[16,8,1408]{2,1,0:T(8,128)(2,1)S(1)} async-done(((bf16[16,8,1408]{2,1,0:T(8,128)(2,1)}), bf16[16,8,1408]{2,1,0:T(8,128)(2,1)S(1)}, u32[]{:S(2)}, u32[]{:S(2)}) %all-to-all-start.1) | async-done | bytes 360480 | tf_op jit(solution)/shard_map/all_to_all | solution.py:23
  63.7 12.4 %all-to-all-start.2 = ((bf16[16,8,640]{2,1,0:T(8,128)(2,1)}), bf16[16,8,640]{2,1,0:T(8,128)(2,1)S(1)}, u32[]{:S(2)}, u32[]{:S(2)}) async-start(bf16[16,8,640]{2,1,0:T(8,128)(2,1)} %broadcast_in_dim.78), calls=%async_computation.2 | async-start | bytes 327680 | tf_op jit(solution)/shard_map/all_to_all | solution.py:18
  78.5 9.9 %all-to-all-done.2 = bf16[16,8,640]{2,1,0:T(8,128)(2,1)S(1)} async-done(((bf16[16,8,640]{2,1,0:T(8,128)(2,1)}), bf16[16,8,640]{2,1,0:T(8,128)(2,1)S(1)}, u32[]{:S(2)}, u32[]{:S(2)}) %all-to-all-start.2) | async-done | bytes 163872 | tf_op jit(solution)/shard_map/all_to_all | solution.py:18
  89.7 6.8 %all-to-all-start.3 = ((bf16[16,8,256]{2,1,0:T(8,128)(2,1)}), bf16[16,8,256]{2,1,0:T(8,128)(2,1)S(1)}, u32[]{:S(2)}, u32[]{:S(2)}) async-start(bf16[16,8,256]{2,1,0:T(8,128)(2,1)} %bitcast.11), calls=%async_computation.3 | async-start | bytes 131072 | tf_op jit(solution)/shard_map/all_to_all | solution.py:23
  96.6 6.5 %all-to-all-done.3 = bf16[16,8,256]{2,1,0:T(8,128)(2,1)S(1)} async-done(((bf16[16,8,256]{2,1,0:T(8,128)(2,1)}), bf16[16,8,256]{2,1,0:T(8,128)(2,1)S(1)}, u32[]{:S(2)}, u32[]{:S(2)}) %all-to-all-start.3) | async-done | bytes 65568 | tf_op jit(solution)/shard_map/all_to_all | solution.py:23
  103.8 3.5 %all-to-all-start.4 = ((bf16[16,8,256]{2,1,0:T(8,128)(2,1)}), bf16[16,8,256]{2,1,0:T(8,128)(2,1)S(1)}, u32[]{:S(2)}, u32[]{:S(2)}) async-start(bf16[16,8,256]{2,1,0:T(8,128)(2,1)} %broadcast_in_dim.79), calls=%async_computation.4 | async-start | bytes 131072 | tf_op jit(solution)/shard_map/all_to_all | solution.py:18
  108.1 5.6 %all-to-all-done.4 = bf16[16,8,256]{2,1,0:T(8,128)(2,1)S(1)} async-done(((bf16[16,8,256]{2,1,0:T(8,128)(2,1)}), bf16[16,8,256]{2,1,0:T(8,128)(2,1)S(1)}, u32[]{:S(2)}, u32[]{:S(2)}) %all-to-all-start.4) | async-done | bytes 65568 | tf_op jit(solution)/shard_map/all_to_all | solution.py:18
  115.6 7.7 %all-to-all-start.5 = ((bf16[16,8,640]{2,1,0:T(8,128)(2,1)}), bf16[16,8,640]{2,1,0:T(8,128)(2,1)S(1)}, u32[]{:S(2)}, u32[]{:S(2)}) async-start(bf16[16,8,640]{2,1,0:T(8,128)(2,1)} %maximum_bitcast_fusion), calls=%async_computation.5 | async-start | bytes 327680 | tf_op jit(solution)/shard_map/all_to_all | solution.py:23
  125.4 10.1 %all-to-all-done.5 = bf16[16,8,640]{2,1,0:T(8,128)(2,1)S(1)} async-done(((bf16[16,8,640]{2,1,0:T(8,128)(2,1)}), bf16[16,8,640]{2,1,0:T(8,128)(2,1)S(1)}, u32[]{:S(2)}, u32[]{:S(2)}) %all-to-all-start.5) | async-done | bytes 163872 | tf_op jit(solution)/shard_map/all_to_all | solution.py:23
  138.7 4.7 %all-to-all-start.6 = ((bf16[16,8,128]{2,1,0:T(8,128)(2,1)}), bf16[16,8,128]{2,1,0:T(8,128)(2,1)S(1)}, u32[]{:S(2)}, u32[]{:S(2)}) async-start(bf16[16,8,128]{2,1,0:T(8,128)(2,1)} %broadcast_in_dim.167), calls=%async_computation.6 | async-start | bytes 65536 | tf_op jit(solution)/shard_map/all_to_all | solution.py:18
  143.4 6.7 %collective-permute-start.5 = (bf16[128,128]{1,0:T(8,128)(2,1)S(1)}, bf16[128,128]{1,0:T(8,128)(2,1)S(1)}, u32[]{:S(2)}, u32[]{:S(2)}) collective-permute-start(bf16[128,128]{1,0:T(8,128)(2,1)S(1)} %copy-done.9), channel_id=1, source_target_pairs={{0,16},{16,0},{1,17},{17,1},{2,18},{18,2},{3,19},{19,3},{4,20},{20... | collective-permute-start | bytes 98312 | tf_op jit(solution)/shard_map/ppermute | solution.py:13
  150.1 4.8 %all-to-all-done.6 = bf16[16,8,128]{2,1,0:T(8,128)(2,1)S(1)} async-done(((bf16[16,8,128]{2,1,0:T(8,128)(2,1)}), bf16[16,8,128]{2,1,0:T(8,128)(2,1)S(1)}, u32[]{:S(2)}, u32[]{:S(2)}) %all-to-all-start.6) | async-done | bytes 32800 | tf_op jit(solution)/shard_map/all_to_all | solution.py:18
  155.5 9.8 %all_to_all.60 = bf16[16,8,256]{2,1,0:T(8,128)(2,1)S(1)} all-to-all(bf16[16,8,256]{2,1,0:T(8,128)(2,1)S(1)} %bitcast.155), channel_id=1, replica_groups=mesh['z'=16,'c'=2,'tp'=16] {'tp'}, dimensions={0} | all-to-all | bytes 131072 | tf_op jit(solution)/shard_map/all_to_all | solution.py:23
  166.0 10.6 %all-to-all-start.8 = ((bf16[32,8,256]{2,1,0:T(8,128)(2,1)}), bf16[32,8,256]{2,1,0:T(8,128)(2,1)S(1)}, u32[]{:S(2)}, u32[]{:S(2)}) async-start(bf16[32,8,256]{2,1,0:T(8,128)(2,1)} %broadcast_in_dim.168), calls=%async_computation.8 | async-start | bytes 262144 | tf_op jit(solution)/shard_map/all_to_all | solution.py:18
  181.0 3.2 %all-to-all-done.8 = bf16[32,8,256]{2,1,0:T(8,128)(2,1)S(1)} async-done(((bf16[32,8,256]{2,1,0:T(8,128)(2,1)}), bf16[32,8,256]{2,1,0:T(8,128)(2,1)S(1)}, u32[]{:S(2)}, u32[]{:S(2)}) %all-to-all-start.8) | async-done | bytes 131104 | tf_op jit(solution)/shard_map/all_to_all | solution.py:18
  185.5 18.7 %all_to_all.61 = bf16[16,8,1408]{2,1,0:T(8,128)(2,1)S(1)} all-to-all(bf16[16,8,1408]{2,1,0:T(8,128)(2,1)S(1)} %concatenate.64), channel_id=1, replica_groups=mesh['z'=16,'c'=2,'tp'=16] {'z'}, dimensions={0} | all-to-all | bytes 720896 | tf_op jit(solution)/shard_map/all_to_all | solution.py:23
  205.3 12.5 %all-to-all-start.10 = ((bf16[16,8,640]{2,1,0:T(8,128)(2,1)}), bf16[16,8,640]{2,1,0:T(8,128)(2,1)S(1)}, u32[]{:S(2)}, u32[]{:S(2)}) async-start(bf16[16,8,640]{2,1,0:T(8,128)(2,1)} %broadcast_in_dim.169), calls=%async_computation.10 | async-start | bytes 327680 | tf_op jit(solution)/shard_map/all_to_all | solution.py:18
  217.8 2.7 %collective-permute-start.8 = (bf16[640,128]{1,0:T(8,128)(2,1)S(1)}, bf16[640,128]{1,0:T(8,128)(2,1)S(1)}, u32[]{:S(2)}, u32[]{:S(2)}) collective-permute-start(bf16[640,128]{1,0:T(8,128)(2,1)S(1)} %copy-done.7), channel_id=1, source_target_pairs={{0,16},{16,0},{1,17},{17,1},{2,18},{18,2},{3,19},{19,3},{4,20},{20... | collective-permute-start | bytes 491528 | tf_op jit(solution)/shard_map/ppermute | solution.py:13
  220.5 9.6 %all-to-all-done.10 = bf16[16,8,640]{2,1,0:T(8,128)(2,1)S(1)} async-done(((bf16[16,8,640]{2,1,0:T(8,128)(2,1)}), bf16[16,8,640]{2,1,0:T(8,128)(2,1)S(1)}, u32[]{:S(2)}, u32[]{:S(2)}) %all-to-all-start.10) | async-done | bytes 163872 | tf_op jit(solution)/shard_map/all_to_all | solution.py:18
  231.1 8.1 %all-to-all-start.11 = ((bf16[32,8,128]{2,1,0:T(8,128)(2,1)}), bf16[32,8,128]{2,1,0:T(8,128)(2,1)S(1)}, u32[]{:S(2)}, u32[]{:S(2)}) async-start(bf16[32,8,128]{2,1,0:T(8,128)(2,1)} %bitcast.39), calls=%async_computation.11 | async-start | bytes 131072 | tf_op jit(solution)/shard_map/all_to_all | solution.py:235
  239.2 7.1 %all-to-all-done.11 = bf16[32,8,128]{2,1,0:T(8,128)(2,1)S(1)} async-done(((bf16[32,8,128]{2,1,0:T(8,128)(2,1)}), bf16[32,8,128]{2,1,0:T(8,128)(2,1)S(1)}, u32[]{:S(2)}, u32[]{:S(2)}) %all-to-all-start.11) | async-done | bytes 65568 | tf_op jit(solution)/shard_map/all_to_all | solution.py:235
  (178 shorter events, 44.0 us)
Async XLA Ops:
  0.0 17.0 %copy-start.2 = (bf16[128,640]{1,0:T(8,128)(2,1)S(1)}, bf16[128,640]{1,0:T(8,128)(2,1)}, u32[]{:S(2)}) copy-start(bf16[128,640]{1,0:T(8,128)(2,1)} %param.29) | copy-start | bytes 491524
  0.7 29.2 %collective-permute-start = (f32[3,128]{1,0:T(4,128)S(1)}, f32[3,128]{1,0:T(4,128)S(1)}, u32[]{:S(2)}, u32[]{:S(2)}) collective-permute-start(f32[3,128]{1,0:T(4,128)S(1)} %pad_maximum_fusion.2), channel_id=1, source_target_pairs={{0,16},{16,0},{1,17},{17,1},{2,18},{18,2},{3,19},{19,3},{4,20},{20... | collective-permute-start | bytes 4616 | tf_op jit(solution)/shard_map/ppermute | solution.py:13
  9.5 79.2 %collective-permute-start.3 = (bf16[640,128]{1,0:T(8,128)(2,1)}, bf16[640,128]{1,0:T(8,128)(2,1)S(1)}, u32[]{:S(2)}, u32[]{:S(2)}) collective-permute-start(bf16[640,128]{1,0:T(8,128)(2,1)} %param.31), channel_id=1, source_target_pairs={{0,16},{16,0},{1,17},{17,1},{2,18},{18,2},{3,19},{19,3},{4,20},{20... | collective-permute-start | bytes 491528 | tf_op jit(solution)/shard_map/ppermute | solution.py:13
  12.7 17.9 %all-to-all-start = ((bf16[32,8,128]{2,1,0:T(8,128)(2,1)}), bf16[32,8,128]{2,1,0:T(8,128)(2,1)S(1)}, u32[]{:S(2)}, u32[]{:S(2)}) async-start(bf16[32,8,128]{2,1,0:T(8,128)(2,1)} %bitcast.1), calls=%async_computation | async-start | bytes 131072 | tf_op jit(solution)/shard_map/all_to_all | solution.py:173
  17.0 15.3 %collective-permute-start.1 = (bf16[128,640]{1,0:T(8,128)(2,1)S(1)}, bf16[128,640]{1,0:T(8,128)(2,1)S(1)}, u32[]{:S(2)}, u32[]{:S(2)}) collective-permute-start(bf16[128,640]{1,0:T(8,128)(2,1)S(1)} %copy-done.2), channel_id=1, source_target_pairs={{0,16},{16,0},{1,17},{17,1},{2,18},{18,2},{3,19},{19,3},{4,20},{20... | collective-permute-start | bytes 491528 | tf_op jit(solution)/shard_map/ppermute | solution.py:13
  19.2 13.4 %collective-permute-start.2 = (bf16[128,640]{1,0:T(8,128)(2,1)}, bf16[128,640]{1,0:T(8,128)(2,1)S(1)}, u32[]{:S(2)}, u32[]{:S(2)}) collective-permute-start(bf16[128,640]{1,0:T(8,128)(2,1)} %param.30), channel_id=1, source_target_pairs={{0,16},{16,0},{1,17},{17,1},{2,18},{18,2},{3,19},{19,3},{4,20},{20... | collective-permute-start | bytes 491528 | tf_op jit(solution)/shard_map/ppermute | solution.py:13
  22.2 92.5 %collective-permute-start.4 = (bf16[128,512]{1,0:T(8,128)(2,1)S(1)}, bf16[128,512]{1,0:T(8,128)(2,1)S(1)}, u32[]{:S(2)}, u32[]{:S(2)}) collective-permute-start(bf16[128,512]{1,0:T(8,128)(2,1)S(1)} %constant_dynamic-update-slice_fusion), channel_id=1, source_target_pairs={{0,16},{16,0},{1,17},{17,1},{2,18},{18,2},{3,19},{19,3},{4,20},{20... | collective-permute-start | bytes 393224 | tf_op jit(solution)/shard_map/ppermute | solution.py:13
  33.6 29.1 %all-to-all-start.1 = ((bf16[16,8,1408]{2,1,0:T(8,128)(2,1)}), bf16[16,8,1408]{2,1,0:T(8,128)(2,1)S(1)}, u32[]{:S(2)}, u32[]{:S(2)}) async-start(bf16[16,8,1408]{2,1,0:T(8,128)(2,1)} %concatenate.54), calls=%async_computation.1 | async-start | bytes 720896 | tf_op jit(solution)/shard_map/all_to_all | solution.py:23
  63.7 24.7 %all-to-all-start.2 = ((bf16[16,8,640]{2,1,0:T(8,128)(2,1)}), bf16[16,8,640]{2,1,0:T(8,128)(2,1)S(1)}, u32[]{:S(2)}, u32[]{:S(2)}) async-start(bf16[16,8,640]{2,1,0:T(8,128)(2,1)} %broadcast_in_dim.78), calls=%async_computation.2 | async-start | bytes 327680 | tf_op jit(solution)/shard_map/all_to_all | solution.py:18
  77.6 10.8 %copy-start.4 = (bf16[640,128]{1,0:T(8,128)(2,1)S(1)}, bf16[640,128]{1,0:T(8,128)(2,1)}, u32[]{:S(2)}) copy-start(bf16[640,128]{1,0:T(8,128)(2,1)} %param.31) | copy-start | bytes 491524
  89.7 13.4 %all-to-all-start.3 = ((bf16[16,8,256]{2,1,0:T(8,128)(2,1)}), bf16[16,8,256]{2,1,0:T(8,128)(2,1)S(1)}, u32[]{:S(2)}, u32[]{:S(2)}) async-start(bf16[16,8,256]{2,1,0:T(8,128)(2,1)} %bitcast.11), calls=%async_computation.3 | async-start | bytes 131072 | tf_op jit(solution)/shard_map/all_to_all | solution.py:23
  103.8 10.0 %all-to-all-start.4 = ((bf16[16,8,256]{2,1,0:T(8,128)(2,1)}), bf16[16,8,256]{2,1,0:T(8,128)(2,1)S(1)}, u32[]{:S(2)}, u32[]{:S(2)}) async-start(bf16[16,8,256]{2,1,0:T(8,128)(2,1)} %broadcast_in_dim.79), calls=%async_computation.4 | async-start | bytes 131072 | tf_op jit(solution)/shard_map/all_to_all | solution.py:18
  115.6 19.9 %all-to-all-start.5 = ((bf16[16,8,640]{2,1,0:T(8,128)(2,1)}), bf16[16,8,640]{2,1,0:T(8,128)(2,1)S(1)}, u32[]{:S(2)}, u32[]{:S(2)}) async-start(bf16[16,8,640]{2,1,0:T(8,128)(2,1)} %maximum_bitcast_fusion), calls=%async_computation.5 | async-start | bytes 327680 | tf_op jit(solution)/shard_map/all_to_all | solution.py:23
  138.7 16.2 %all-to-all-start.6 = ((bf16[16,8,128]{2,1,0:T(8,128)(2,1)}), bf16[16,8,128]{2,1,0:T(8,128)(2,1)S(1)}, u32[]{:S(2)}, u32[]{:S(2)}) async-start(bf16[16,8,128]{2,1,0:T(8,128)(2,1)} %broadcast_in_dim.167), calls=%async_computation.6 | async-start | bytes 65536 | tf_op jit(solution)/shard_map/all_to_all | solution.py:18
  143.4 11.7 %collective-permute-start.5 = (bf16[128,128]{1,0:T(8,128)(2,1)S(1)}, bf16[128,128]{1,0:T(8,128)(2,1)S(1)}, u32[]{:S(2)}, u32[]{:S(2)}) collective-permute-start(bf16[128,128]{1,0:T(8,128)(2,1)S(1)} %copy-done.9), channel_id=1, source_target_pairs={{0,16},{16,0},{1,17},{17,1},{2,18},{18,2},{3,19},{19,3},{4,20},{20... | collective-permute-start | bytes 98312 | tf_op jit(solution)/shard_map/ppermute | solution.py:13
  155.5 23.3 %copy-start.6 = (bf16[128,640]{1,0:T(8,128)(2,1)S(1)}, bf16[128,640]{1,0:T(8,128)(2,1)}, u32[]{:S(2)}) copy-start(bf16[128,640]{1,0:T(8,128)(2,1)} %param.45) | copy-start | bytes 491524
  166.0 10.6 %copy-start.5 = (bf16[128,640]{1,0:T(8,128)(2,1)S(1)}, bf16[128,640]{1,0:T(8,128)(2,1)}, u32[]{:S(2)}) copy-start(bf16[128,640]{1,0:T(8,128)(2,1)} %param.44) | copy-start | bytes 491524
  166.0 18.2 %all-to-all-start.8 = ((bf16[32,8,256]{2,1,0:T(8,128)(2,1)}), bf16[32,8,256]{2,1,0:T(8,128)(2,1)S(1)}, u32[]{:S(2)}, u32[]{:S(2)}) async-start(bf16[32,8,256]{2,1,0:T(8,128)(2,1)} %broadcast_in_dim.168), calls=%async_computation.8 | async-start | bytes 262144 | tf_op jit(solution)/shard_map/all_to_all | solution.py:18
  176.6 8.4 %collective-permute-start.6 = (bf16[128,640]{1,0:T(8,128)(2,1)S(1)}, bf16[128,640]{1,0:T(8,128)(2,1)S(1)}, u32[]{:S(2)}, u32[]{:S(2)}) collective-permute-start(bf16[128,640]{1,0:T(8,128)(2,1)S(1)} %copy-done.5), channel_id=1, source_target_pairs={{0,16},{16,0},{1,17},{17,1},{2,18},{18,2},{3,19},{19,3},{4,20},{20... | collective-permute-start | bytes 491528 | tf_op jit(solution)/shard_map/ppermute | solution.py:13
  178.8 6.4 %collective-permute-start.7 = (bf16[128,640]{1,0:T(8,128)(2,1)S(1)}, bf16[128,640]{1,0:T(8,128)(2,1)S(1)}, u32[]{:S(2)}, u32[]{:S(2)}) collective-permute-start(bf16[128,640]{1,0:T(8,128)(2,1)S(1)} %copy-done.6), channel_id=1, source_target_pairs={{0,16},{16,0},{1,17},{17,1},{2,18},{18,2},{3,19},{19,3},{4,20},{20... | collective-permute-start | bytes 491528 | tf_op jit(solution)/shard_map/ppermute | solution.py:13
  205.3 12.5 %copy-start.7 = (bf16[640,128]{1,0:T(8,128)(2,1)S(1)}, bf16[640,128]{1,0:T(8,128)(2,1)}, u32[]{:S(2)}) copy-start(bf16[640,128]{1,0:T(8,128)(2,1)} %param.46) | copy-start | bytes 491524
  205.3 24.8 %all-to-all-start.10 = ((bf16[16,8,640]{2,1,0:T(8,128)(2,1)}), bf16[16,8,640]{2,1,0:T(8,128)(2,1)S(1)}, u32[]{:S(2)}, u32[]{:S(2)}) async-start(bf16[16,8,640]{2,1,0:T(8,128)(2,1)} %broadcast_in_dim.169), calls=%async_computation.10 | async-start | bytes 327680 | tf_op jit(solution)/shard_map/all_to_all | solution.py:18
  217.8 12.5 %collective-permute-start.8 = (bf16[640,128]{1,0:T(8,128)(2,1)S(1)}, bf16[640,128]{1,0:T(8,128)(2,1)S(1)}, u32[]{:S(2)}, u32[]{:S(2)}) collective-permute-start(bf16[640,128]{1,0:T(8,128)(2,1)S(1)} %copy-done.7), channel_id=1, source_target_pairs={{0,16},{16,0},{1,17},{17,1},{2,18},{18,2},{3,19},{19,3},{4,20},{20... | collective-permute-start | bytes 491528 | tf_op jit(solution)/shard_map/ppermute | solution.py:13
  231.1 15.2 %all-to-all-start.11 = ((bf16[32,8,128]{2,1,0:T(8,128)(2,1)}), bf16[32,8,128]{2,1,0:T(8,128)(2,1)S(1)}, u32[]{:S(2)}, u32[]{:S(2)}) async-start(bf16[32,8,128]{2,1,0:T(8,128)(2,1)} %bitcast.39), calls=%async_computation.11 | async-start | bytes 131072 | tf_op jit(solution)/shard_map/all_to_all | solution.py:235
  (17 other events, 33.7 us)

commit v2 on v1

v2 whole, which is shorter than its diff:
```python
import functools

import jax
import jax.numpy as jnp
from jax import lax
from jax.experimental import pallas as pl
from jax.experimental.pallas import tpu as pltpu
from jax.sharding import Mesh, PartitionSpec as P

HIGHEST = lax.Precision.HIGHEST
f32 = jnp.float32
bf16 = jnp.bfloat16
LANES = 128
EPS = 1e-06


def kernel(fn, out, *args, scalars=0, flops=1 << 20, limit=12 << 20, **static):
    outs = out if isinstance(out, list) else [out]
    smem = pl.BlockSpec(memory_space=pltpu.SMEM)
    vmem = pl.BlockSpec(memory_space=pltpu.VMEM)
    shapes = [jax.ShapeDtypeStruct(s, d) for s, d in outs]
    size = sum(a.size * a.dtype.itemsize for a in args)
    got = pl.pallas_call(
        functools.partial(fn, **static),
        out_shape=shapes,
        in_specs=[smem] * scalars + [vmem] * (len(args) - scalars),
        out_specs=[vmem] * len(outs),
        compiler_params=pltpu.CompilerParams(vmem_limit_bytes=limit),
        cost_estimate=pl.CostEstimate(flops=flops, bytes_accessed=size, transcendentals=0),
        name=fn.__name__,
    )(*args)
    return got if isinstance(out, list) else got[0]


def dot(x, w):
    return jnp.dot(x, w, preferred_element_type=f32)


def dot_t(x, w):
    return lax.dot_general(x, w, (((1,), (1,)), ((), ())), preferred_element_type=f32)


def exact(x, y, contract=((1,), (0,))):
    return lax.dot_general(
        x, y, (contract, ((), ())), precision=HIGHEST, preferred_element_type=f32
    )


def flat(x):
    x = x.astype(f32)
    return x.reshape(-1, x.shape[-1])


def blocked(x, count):
    return x.reshape(count, -1, x.shape[-1])


def lane_tile(rows, columns):
    lane = lax.broadcasted_iota(jnp.int32, (rows, LANES), 1)
    tile = jnp.zeros((rows, LANES), f32)
    for i, column in enumerate(columns):
        high = column.astype(bf16).astype(f32)
        tile = jnp.where(lane == i, high, tile)
        tile = jnp.where(lane == i + len(columns), column - high, tile)
    return tile


def column_of(sums, start, i, count):
    at = start + i
    return sums[:, at : at + 1] + sums[:, at + count : at + count + 1]


def silu(x):
    return x * jax.nn.sigmoid(x)


def softplus(x):
    return jnp.maximum(x, 0.0) + jnp.log1p(jnp.exp(-jnp.abs(x)))


def gate_up(own, other, gain, gain_x, gates, ups, out):
    n = gates[0].shape[1]
    count = out.shape[0]
    scaled, scaled_x = (own * gain).astype(bf16), (other * gain_x).astype(bf16)
    for at, pair in ((0, gates), (n, ups)):
        part = dot(scaled, pair[0][...]) + dot(scaled_x, pair[1][...])
        out[:, :, at : at + n] = blocked(part, count).astype(bf16)
    square = jnp.sum(own * own + other * other, -1, keepdims=True)
    out[:, :, 2 * n :] = blocked(lane_tile(own.shape[0], [square]), count).astype(bf16)


def first_products(ids, got, gains, gains_x, gate, gate_x, up, up_x, out):
    core = ids[0]
    gate_up(
        flat(got[core]),
        flat(got[1 - core]),
        gains[0:1],
        gains_x[0:1],
        (gate, gate_x),
        (up, up_x),
        out,
    )


def second_products(ids, got, gains, gains_x, gate, gate_x, up, up_x, out):
    wide = flat(got[ids[0]])
    half = wide.shape[1] // 2
    gate_up(
        wide[:, :half],
        wide[:, half:],
        gains[2:3],
        gains_x[2:3],
        (gate, gate_x),
        (up, up_x),
        out,
    )


def activate(parts, out, *, features):
    sums = jnp.sum(parts[...].astype(f32), axis=0)
    n = (sums.shape[1] - LANES) // 2
    factor = lax.rsqrt(column_of(sums, 2 * n, 0, 1) / features + EPS)
    hidden = silu(sums[:, :n] * factor) * (sums[:, n : 2 * n] * factor)
    out[...] = jnp.broadcast_to(hidden[None], out.shape).astype(bf16)


def down(hidden, weight, weight_x, out):
    rows = flat(hidden[...]).astype(bf16)
    half = weight.shape[1]
    out[:, :, :half] = blocked(dot(rows, weight[...]), out.shape[0]).astype(bf16)
    out[:, :, half:] = blocked(dot(rows, weight_x[...]), out.shape[0]).astype(bf16)


def last_down(ids, hidden, weight, weight_x, out):
    rows = flat(hidden[...]).astype(bf16)
    out[ids[0]] = blocked(dot(rows, weight[...]), out.shape[1]).astype(bf16)
    out[1 - ids[0]] = blocked(dot(rows, weight_x[...]), out.shape[1]).astype(bf16)


def add_first(ids, parts, got, out):
    sums = jnp.sum(parts[...].astype(f32), axis=0)
    core, block = ids[0], ids[1]
    own, other = got[core, block].astype(f32), got[1 - core, block].astype(f32)
    rows = jnp.concatenate([own, other], 1) + 0.5 * sums
    out[...] = jnp.broadcast_to(rows[None], out.shape).astype(bf16)


def add_mixer(ids, parts, middle, out):
    sums = jnp.sum(parts[...].astype(f32), axis=0)
    rows = middle[ids[1]].astype(f32) + sums
    out[...] = jnp.broadcast_to(rows[None], out.shape).astype(bf16)


def project(ids, middle, gains, gains_x, main, main_x, ws, ws_x, wd, wd_x, out):
    wide = flat(middle[...])
    half = wide.shape[1] // 2
    own, other = wide[:, :half], wide[:, half:]
    scaled, scaled_x = (own * gains[1:2]).astype(bf16), (other * gains_x[1:2]).astype(bf16)
    n, count = main.shape[1], out.shape[0]
    part = dot(scaled, main[...]) + dot(scaled_x, main_x[...])
    out[:, :, :n] = blocked(part, count).astype(bf16)
    heads = ws.shape[0]
    mine = lax.broadcasted_iota(jnp.int32, (wide.shape[0], heads), 1) == ids[1]
    columns = []
    for w, w_x in ((ws, ws_x), (wd, wd_x)):
        logit = dot_t(scaled, w[...]) + dot_t(scaled_x, w_x[...])
        columns.append(jnp.sum(jnp.where(mine, logit, 0.0), -1, keepdims=True))
    columns.append(jnp.sum(own * own + other * other, -1, keepdims=True))
    out[:, :, n:] = blocked(lane_tile(wide.shape[0], columns), count).astype(bf16)


def earlier_state(lengths, head, recurrent, keys, values, strength, decay, extra, state, new):
    count, span = strength.shape
    sequence = lax.broadcasted_iota(jnp.int32, (count, span), 0)
    lane = lax.broadcasted_iota(jnp.int32, (count, span), 1)
    latest = jnp.zeros((count, span), jnp.int32)
    for b in range(count):
        latest = jnp.where(sequence == b, lengths[b] - 1, latest)
    before = lane < latest
    beta = jnp.where(before, jax.nn.sigmoid(strength[...]), 0.0)
    amount = extra[...] - head[0] * softplus(decay[...] + head[1])
    amount = jnp.where(before, amount, 0.0)
    new_extra = jnp.sum(jnp.where(lane == latest, extra[...], 0.0), -1, keepdims=True)
    new[...] = jnp.broadcast_to(new_extra, new.shape)
    row = lax.broadcasted_iota(jnp.int32, (span, span), 0)
    col = lax.broadcasted_iota(jnp.int32, (span, span), 1)
    cumul = exact(amount, (row <= col).astype(f32))
    last = cumul[:, span - 1 : span]
    eye = (row == col).astype(f32)
    stacked = jnp.concatenate(
        [beta, cumul, jnp.exp(cumul), jnp.exp(last - cumul), before.astype(f32)], 0
    )
    upright = exact(eye, stacked, ((1,), (1,)))

    def upright_column(which, b):
        at = which * count + b
        return upright[:, at : at + 1]

    every = range(count)
    ks, couplings = [], []
    for b in every:
        k = keys[b].astype(f32) * upright_column(4, b)
        k = k * lax.rsqrt(jnp.sum(k * k, -1, keepdims=True) + EPS)
        gap = upright_column(1, b) - cumul[b : b + 1]
        gap = jnp.exp(jnp.where(row > col, gap, -jnp.inf))
        ks.append(k)
        couplings.append(upright_column(0, b) * exact(k, k, ((1,), (1,))) * gap)

    def same(size):
        return (row // size) == (col // size)

    first = [jnp.where(same(8), c, 0.0) for c in couplings]
    second = [exact(a, a) for a in first]
    fourth = [exact(a, a) for a in second]
    inverse = [exact(eye - a, eye + b) for a, b in zip(first, second)]
    inverse = [exact(a, eye + b) for a, b in zip(inverse, fourth)]
    size = 8
    while size < span:
        inside = same(2 * size) & ~same(size)
        right = [exact(jnp.where(inside, c, 0.0), a) for c, a in zip(couplings, inverse)]
        inverse = [a - exact(a, r) for a, r in zip(inverse, right)]
        size *= 2
    for b in every:
        carried = exact(ks[b], recurrent[b])
        value = values[b].astype(f32) * upright_column(4, b)
        side = upright_column(0, b) * (value - upright_column(2, b) * carried)
        update = exact(inverse[b], side) * upright_column(3, b)
        kept = jnp.exp(last[b : b + 1]) * recurrent[b]
        state[b] = kept + exact(ks[b], update, ((0,), (0,)))


def new_token(head, parts, state, new_extra, norm_gain, out, *, features):
    sums = jnp.sum(parts[...].astype(f32), axis=0)
    dk = (sums.shape[1] - LANES) // 4
    strength, decay, square = (column_of(sums, 4 * dk, i, 3) for i in range(3))
    factor = lax.rsqrt(square / features + EPS)
    query, key, value, gate = (sums[:, i * dk : (i + 1) * dk] * factor for i in range(4))
    beta = jax.nn.sigmoid(strength * factor)
    amount = new_extra[:, 0:1] - head[0] * softplus(decay * factor + head[1])
    query = query * lax.rsqrt(jnp.sum(query * query, -1, keepdims=True) + EPS) * dk**-0.5
    key = key * lax.rsqrt(jnp.sum(key * key, -1, keepdims=True) + EPS)
    score = jnp.sum(query * key, -1, keepdims=True)
    reduced = jnp.transpose(query - (score * beta) * key)
    sequence = lax.broadcasted_iota(jnp.int32, value.shape, 0)
    read = jnp.zeros(value.shape, f32)
    for b in range(value.shape[0]):
        one = jnp.sum(reduced[:, b : b + 1] * state[b], axis=0, keepdims=True)
        read = jnp.where(sequence == b, one, read)
    rows = jnp.exp(amount) * read + (score * beta) * value
    rows = rows * lax.rsqrt(jnp.mean(rows * rows, -1, keepdims=True) + EPS)
    rows = rows * norm_gain[...] * silu(gate)
    out[...] = jnp.broadcast_to(rows[None], out.shape).astype(bf16)


def finish(ids, parts, got, out):
    core, block = ids[0], ids[1]
    sums = jnp.sum(parts[...].astype(f32), axis=1)
    half = sums.shape[-1]
    rows = []
    for c in range(2):
        wide = got[c, block].astype(f32)
        mine = jnp.where(core == c, wide[:, :half], wide[:, half:])
        rows.append(mine + 0.5 * sums[c])
    out[...] = jnp.concatenate(rows, 0).astype(bf16)


def exchange(x, axis):
    return lax.all_to_all(x, axis, 0, 0, tiled=True)


def swap(x):
    return lax.ppermute(x, "c", [(0, 1), (1, 0)])


def together(*trees):
    return lax.optimization_barrier(trees)


def body(
    tokens,
    first_norm_gain,
    first_gate_weight,
    first_up_weight,
    first_down_weight,
    mixer_norm_gain,
    query_weight_matrix,
    key_weight_matrix,
    value_weight_matrix,
    output_gate_weight,
    strength_weight,
    decay_weight,
    head_decay_speed,
    head_decay_offset,
    head_norm_gain,
    mixer_out_weight,
    second_norm_gain,
    second_gate_weight,
    second_up_weight,
    second_down_weight,
    recurrent,
    earlier_key_cache,
    earlier_value_cache,
    strength_logit_history,
    decay_input_history,
    position_decay_extra,
    lengths,
):
    core, tp, z = lax.axis_index("c"), lax.axis_index("tp"), lax.axis_index("z")
    plane, ring = lax.axis_size("tp"), lax.axis_size("z")
    count, width = tokens.shape
    rows = count // 2
    features = 2 * ring * width
    hidden_units = first_gate_weight.shape[1]
    dk = query_weight_matrix.shape[1]
    ids = jnp.stack([core, tp]).astype(jnp.int32)
    head = jnp.concatenate([head_decay_speed, head_decay_offset])

    blocks = jnp.broadcast_to(tokens.reshape(2, 1, rows, width), (2, plane, rows, width))
    with jax.named_scope("tokens"):
        got = exchange(blocks.reshape(2 * plane, rows, width), ("c", "tp"))
    got = got.reshape(2, plane, rows, width)

    gains = jnp.stack([first_norm_gain, mixer_norm_gain, second_norm_gain])
    with jax.named_scope("early"):
        gains_x, gate_x, up_x = swap(gains), swap(first_gate_weight), swap(first_up_weight)
    sent = kernel(
        first_products,
        ((ring, rows, 2 * hidden_units + LANES), bf16),
        ids,
        got,
        gains,
        gains_x,
        first_gate_weight,
        gate_x,
        first_up_weight,
        up_x,
        scalars=1,
    )

    sent, later = together(
        sent,
        (
            first_down_weight,
            query_weight_matrix,
            key_weight_matrix,
            value_weight_matrix,
            output_gate_weight,
            strength_weight,
            decay_weight,
            recurrent,
            earlier_key_cache,
            earlier_value_cache,
            strength_logit_history,
            decay_input_history,
            position_decay_extra,
            lengths,
            mixer_out_weight,
            second_gate_weight,
            second_up_weight,
            second_down_weight,
        ),
    )
    (
        first_down_weight,
        query_weight_matrix,
        key_weight_matrix,
        value_weight_matrix,
        output_gate_weight,
        strength_weight,
        decay_weight,
        recurrent,
        earlier_key_cache,
        earlier_value_cache,
        strength_logit_history,
        decay_input_history,
        position_decay_extra,
        lengths,
        mixer_out_weight,
        second_gate_weight,
        second_up_weight,
        second_down_weight,
    ) = later
    parts = exchange(sent, "z")
    down_x = swap(first_down_weight)
    main = jnp.concatenate(
        [query_weight_matrix, key_weight_matrix, value_weight_matrix, output_gate_weight], 1
    )
    main_x = swap(main)

    def small(w, which):
        return lax.dynamic_slice_in_dim(w.T, (z * 2 + which) * width, width, 1)

    ws, ws_x = small(strength_weight, core), small(strength_weight, 1 - core)
    wd, wd_x = small(decay_weight, core), small(decay_weight, 1 - core)
    local = lengths.shape[0]
    state, new_extra = kernel(
        earlier_state,
        [((local, dk, recurrent.shape[-1]), f32), ((local, LANES), f32)],
        lengths,
        head,
        recurrent[:, 0],
        earlier_key_cache,
        earlier_value_cache,
        strength_logit_history[0],
        decay_input_history[0],
        position_decay_extra[0],
        scalars=2,
        flops=1 << 28,
    )
    parts, down_x, main, main_x, ws, ws_x, wd, wd_x, state, new_extra = together(
        parts, down_x, main, main_x, ws, ws_x, wd, wd_x, state, new_extra
    )

    hidden = kernel(
        activate, ((ring, rows, hidden_units), bf16), parts, features=features
    )
    hidden, later = together(
        hidden, (mixer_out_weight, second_gate_weight, second_up_weight, second_down_weight)
    )
    mixer_out_weight, second_gate_weight, second_up_weight, second_down_weight = later
    hidden = exchange(hidden, "z")
    out_x, gate2_x = swap(mixer_out_weight), swap(second_gate_weight)
    up2_x, down2_x = swap(second_up_weight), swap(second_down_weight)
    hidden, out_x, gate2_x, up2_x, down2_x = together(hidden, out_x, gate2_x, up2_x, down2_x)

    parts = kernel(down, ((plane, rows, 2 * width), bf16), hidden, first_down_weight, down_x)
    parts = exchange(parts, "tp")
    middle = kernel(add_first, ((plane, rows, 2 * width), bf16), ids, parts, got, scalars=1)
    middle = exchange(middle, "tp")

    parts = kernel(
        project,
        ((ring, rows, 4 * dk + LANES), bf16),
        ids,
        middle,
        gains,
        gains_x,
        main,
        main_x,
        ws,
        ws_x,
        wd,
        wd_x,
        scalars=1,
    )
    parts = exchange(parts, "z")
    mixed = kernel(
        new_token,
        ((ring, rows, dk), bf16),
        head,
        parts,
        state,
        new_extra,
        head_norm_gain[None],
        scalars=1,
        features=features,
    )
    mixed = exchange(mixed, "z")
    parts = kernel(down, ((plane, rows, 2 * width), bf16), mixed, mixer_out_weight, out_x)
    parts = exchange(parts, "tp")
    second = kernel(add_mixer, ((2 * plane, rows, 2 * width), bf16), ids, parts, middle, scalars=1)
    second = exchange(second, ("c", "tp")).reshape(2, plane, rows, 2 * width)

    sent = kernel(
        second_products,
        ((ring, rows, 2 * hidden_units + LANES), bf16),
        ids,
        second,
        gains,
        gains_x,
        second_gate_weight,
        gate2_x,
        second_up_weight,
        up2_x,
        scalars=1,
    )
    parts = exchange(sent, "z")
    hidden = kernel(
        activate, ((ring, rows, hidden_units), bf16), parts, features=features
    )
    hidden = exchange(hidden, "z")
    parts = kernel(
        last_down,
        ((2, plane, rows, width), bf16),
        ids,
        hidden,
        second_down_weight,
        down2_x,
        scalars=1,
    )
    parts = exchange(parts.reshape(2 * plane, rows, width), ("c", "tp"))
    parts = parts.reshape(2, plane, rows, width)
    return kernel(finish, ((count, width), bf16), ids, parts, second, scalars=1)


def solution(mesh):
    kv, tp = mesh.shape["kv"], mesh.shape["tp"]
    split = Mesh(mesh.devices.reshape(kv // 2, 2, tp), ("z", "c", "tp"))
    kv = ("z", "c")
    return jax.shard_map(
        body,
        mesh=split,
        in_specs=(
            P("tp", kv),
            P(kv),
            P(kv, "tp"),
            P(kv, "tp"),
            P("tp", kv),
            P(kv),
            P(kv, "tp"),
            P(kv, "tp"),
            P(kv, "tp"),
            P(kv, "tp"),
            P(),
            P(),
            P("tp"),
            P("tp"),
            P(),
            P("tp", kv),
            P(kv),
            P(kv, "tp"),
            P(kv, "tp"),
            P("tp", kv),
            P(kv, "tp", None, None),
            P(kv, None, "tp"),
            P(kv, None, "tp"),
            P("tp", kv, None),
            P("tp", kv, None),
            P("tp", kv, None),
            P(kv),
        ),
        out_specs=P("tp", kv),
        check_vma=False,
    )
```

time: 249 us -> 234 us (0.940)
  blocking collectives: 28.6 us -> 142 us
  waiting for transfers between devices: 70.5 us -> 12 us
  starting transfers between devices: 114 us -> 56.2 us
  Pallas kernels: 0 us -> 15.6 us
  matrix products: 11.2 us -> 0 us
  local copies, waits for them, and re-layouts: 14.2 us -> 4.34 us
  other arithmetic: 5.86 us -> 0.85 us
    all_to_all x2 -> x9, blocking collectives: 28.6 us -> 142 us  [exchange(): return lax.all_to_all(x, axis, 0, 0, tiled=True)]
    all_to_all x10 -> x3, waiting for transfers between devices: 70.4 us -> 10.8 us  [exchange(): return lax.all_to_all(x, axis, 0, 0, tiled=True)]
    all_to_all x10 -> x3, starting transfers between devices: 83.6 us -> 28.9 us  [exchange(): return lax.all_to_all(x, axis, 0, 0, tiled=True)]
    pallas_call x0 -> x13, Pallas kernels: none -> 15.6 us  [kernel(): pl.pallas_call(functools.partial(fn, **static), out_shape=shapes, in_spec...]
    dot_general x34 -> x0, matrix products: 11.2 us -> none  [the longest x11 4.26 us: mm(): return jnp.einsum('bps,bsr->bpr', a, b, precision=HIGHEST)]
    ppermute x9, starting transfers between devices: 30.8 us -> 27.2 us  [swap(): return lax.ppermute(x, 'c', [(0, 1), (1, 0)])]
    broadcast_in_dim x9 -> x0, local copies, waits for them, and re-layouts: 3.48 us -> none  [the longest x5 3.22 us: to_all(): jnp.broadcast_to(x[None], (count, *x.shape))]
    unnamed x47 -> x41, local copies, waits for them, and re-layouts: 5.32 us -> 2.26 us
  transfers between devices with their start and end apart: 19 -> 12, of which waited for: 9 -> 4; matrix products, arithmetic and copies ran while one was open for 7% -> 1% of each run, Pallas kernels for 0% -> 3%
where the time goes in v2:
time: 234 us; the launch traced here: 233 us
  blocking collectives  142 us (61%)
  starting transfers between devices  56.2 us (24%)
  Pallas kernels  15.6 us (7%)
  waiting for transfers between devices  12 us (5%)
  local copies, waits for them, and re-layouts  4.34 us (2%)
    all_to_all x9, blocking collectives, exchange(): return lax.all_to_all(x, axis, 0, 0, tiled=True)  142 us
    all_to_all x3, starting transfers between devices, exchange(): return lax.all_to_all(x, axis, 0, 0, tiled=True)  28.9 us
    ppermute x9, starting transfers between devices, swap(): return lax.ppermute(x, 'c', [(0, 1), (1, 0)])  27.2 us
    pallas_call x13, Pallas kernels, kernel(): pl.pallas_call(functools.partial(fn, **static), out_shape=shapes, in_spec...  15.6 us
    all_to_all x3, waiting for transfers between devices, exchange(): return lax.all_to_all(x, axis, 0, 0, tiled=True)  10.8 us
  transfers between devices with their start and end apart: 12, of which 4 were waited for; matrix products, arithmetic and copies ran while one was open for 1% of the time, Pallas kernels for 3%

profile of v2, /device:TPU:1, one launch (start us, length us, event | category | flops | bytes accessed | tf_op | source)
XLA Modules:
  0.0 232.5 jit_solution(9573545991671613122)
XLA Ops:
  0.0 8.9 %collective-permute-start.1 = (bf16[128,640]{1,0:T(8,128)(2,1)}, bf16[128,640]{1,0:T(8,128)(2,1)S(1)}, u32[]{:S(2)}, u32[]{:S(2)}) collective-permute-start(bf16[128,640]{1,0:T(8,128)(2,1)} %gate.1), channel_id=1, source_target_pairs={{0,16},{16,0},{1,17},{17,1},{2,18},{18,2},{3,19},{19,3},{4,20},{20... | collective-permute-start | bytes 491528 | tf_op jit(solution)/shard_map/early/ppermute | solution.py:272
  8.9 1.9 collective-permute-start.2
  11.5 2.4 %collective-permute-start = (f32[3,128]{1,0:T(4,128)S(1)}, f32[3,128]{1,0:T(4,128)S(1)}, u32[]{:S(2)}, u32[]{:S(2)}) collective-permute-start(f32[3,128]{1,0:T(4,128)S(1)} %pad_maximum_fusion.gains), channel_id=1, source_target_pairs={{0,16},{16,0},{1,17},{17,1},{2,18},{18,2},{3,19},{19,3},{4,20},{20... | collective-permute-start | bytes 4616 | tf_op jit(solution)/shard_map/early/ppermute | solution.py:272
  15.2 3.6 %all-to-all-start = ((bf16[32,8,128]{2,1,0:T(8,128)(2,1)}), bf16[32,8,128]{2,1,0:T(8,128)(2,1)S(1)}, u32[]{:S(2)}, u32[]{:S(2)}) async-start(bf16[32,8,128]{2,1,0:T(8,128)(2,1)} %bitcast.3), calls=%async_computation | async-start | bytes 131072 | tf_op jit(solution)/shard_map/tokens/all_to_all | solution.py:268
  18.9 7.0 %all-to-all-done = bf16[32,8,128]{2,1,0:T(8,128)(2,1)S(1)} async-done(((bf16[32,8,128]{2,1,0:T(8,128)(2,1)}), bf16[32,8,128]{2,1,0:T(8,128)(2,1)S(1)}, u32[]{:S(2)}, u32[]{:S(2)}) %all-to-all-start) | async-done | bytes 65568 | tf_op jit(solution)/shard_map/tokens/all_to_all | solution.py:268
  28.5 13.3 %all-to-all-start.1 = ((bf16[16,8,1408]{2,1,0:T(8,128)(2,1)}), bf16[16,8,1408]{2,1,0:T(8,128)(2,1)S(1)}, u32[]{:S(2)}, u32[]{:S(2)}) async-start(bf16[16,8,1408]{2,1,0:T(8,128)(2,1)} %first_products.1), calls=%async_computation.1 | async-start | bytes 720896 | tf_op jit(solution)/shard_map/all_to_all | solution.py:268
  43.2 2.9 %collective-permute-start.3 = (bf16[640,128]{1,0:T(8,128)(2,1)S(1)}, bf16[640,128]{1,0:T(8,128)(2,1)S(1)}, u32[]{:S(2)}, u32[]{:S(2)}) collective-permute-start(bf16[640,128]{1,0:T(8,128)(2,1)S(1)} %copy-done.1), channel_id=1, source_target_pairs={{0,16},{16,0},{1,17},{17,1},{2,18},{18,2},{3,19},{19,3},{4,20},{20... | collective-permute-start | bytes 491528 | tf_op jit(solution)/shard_map/ppermute | solution.py:272
  46.2 1.9 collective-permute-start.4
  48.8 6.4 %earlier_state.1 = (f32[8,128,128]{2,1,0:T(8,128)S(1)}, f32[8,128]{1,0:T(8,128)S(1)}) custom-call(s32[8]{0:T(128)S(1)} %copy-done.14, f32[2]{0:T(128)S(1)} %pad_maximum_fusion.1.head, f32[8,128,128]{2,1,0:T(8,128)S(1)} %bitcast.31, bf16[8,64,128]{2,1,0:T(8,128)(2,1)S(1)} %copy-done.9, bf16[8,64,128]{2,1,0:T(8,128)(2,1)S(1)} %copy-done.10, ...), custom_call_target="tpu_custom_call" | custom-call | flops 268435456 | bytes 792616 | tf_op jit(solution)/shard_map/earlier_state/pallas_call | solution.py:23
  56.0 2.2 all-to-all-done.1.parts
  59.0 12.0 %all-to-all-start.2 = ((bf16[16,8,640]{2,1,0:T(8,128)(2,1)}), bf16[16,8,640]{2,1,0:T(8,128)(2,1)S(1)}, u32[]{:S(2)}, u32[]{:S(2)}) async-start(bf16[16,8,640]{2,1,0:T(8,128)(2,1)} %activate.2), calls=%async_computation.2 | async-start | bytes 327680 | tf_op jit(solution)/shard_map/all_to_all | solution.py:268
  71.0 3.0 %collective-permute-start.6 = (bf16[128,640]{1,0:T(8,128)(2,1)S(1)}, bf16[128,640]{1,0:T(8,128)(2,1)S(1)}, u32[]{:S(2)}, u32[]{:S(2)}) collective-permute-start(bf16[128,640]{1,0:T(8,128)(2,1)S(1)} %copy-done.4), channel_id=1, source_target_pairs={{0,16},{16,0},{1,17},{17,1},{2,18},{18,2},{3,19},{19,3},{4,20},{20... | collective-permute-start | bytes 491528 | tf_op jit(solution)/shard_map/ppermute | solution.py:272
  74.0 1.9 collective-permute-start.7
  76.0 2.4 %collective-permute-start.8 = (bf16[640,128]{1,0:T(8,128)(2,1)S(1)}, bf16[640,128]{1,0:T(8,128)(2,1)S(1)}, u32[]{:S(2)}, u32[]{:S(2)}) collective-permute-start(bf16[640,128]{1,0:T(8,128)(2,1)S(1)} %copy-done), channel_id=1, source_target_pairs={{0,16},{16,0},{1,17},{17,1},{2,18},{18,2},{3,19},{19,3},{4,20},{20... | collective-permute-start | bytes 491528 | tf_op jit(solution)/shard_map/ppermute | solution.py:272
  78.4 1.9 collective-permute-start.5
  83.4 9.9 %all_to_all.60.parts = bf16[16,8,256]{2,1,0:T(8,128)(2,1)S(1)} all-to-all(bf16[16,8,256]{2,1,0:T(8,128)(2,1)S(1)} %down.2), channel_id=1, replica_groups=mesh['z'=16,'c'=2,'tp'=16] {'tp'}, dimensions={0} | all-to-all | bytes 131072 | tf_op jit(solution)/shard_map/all_to_all | solution.py:268
  93.9 9.4 %all_to_all.61.middle = bf16[16,8,256]{2,1,0:T(8,128)(2,1)S(1)} all-to-all(bf16[16,8,256]{2,1,0:T(8,128)(2,1)S(1)} %add_first.1), channel_id=1, replica_groups=mesh['z'=16,'c'=2,'tp'=16] {'tp'}, dimensions={0} | all-to-all | bytes 131072 | tf_op jit(solution)/shard_map/all_to_all | solution.py:268
  104.1 21.9 %all_to_all.62.parts = bf16[16,8,640]{2,1,0:T(8,128)(2,1)S(1)} all-to-all(bf16[16,8,640]{2,1,0:T(8,128)(2,1)S(1)} %project.1), channel_id=1, replica_groups=mesh['z'=16,'c'=2,'tp'=16] {'z'}, dimensions={0} | all-to-all | bytes 327680 | tf_op jit(solution)/shard_map/all_to_all | solution.py:268
  128.1 16.4 %all_to_all.63.hidden = bf16[16,8,128]{2,1,0:T(8,128)(2,1)S(1)} all-to-all(bf16[16,8,128]{2,1,0:T(8,128)(2,1)S(1)} %new_token.1), channel_id=1, replica_groups=mesh['z'=16,'c'=2,'tp'=16] {'z'}, dimensions={0} | all-to-all | bytes 65536 | tf_op jit(solution)/shard_map/all_to_all | solution.py:268
  144.6 10.6 %all_to_all.64.parts = bf16[16,8,256]{2,1,0:T(8,128)(2,1)S(1)} all-to-all(bf16[16,8,256]{2,1,0:T(8,128)(2,1)S(1)} %down.3), channel_id=1, replica_groups=mesh['z'=16,'c'=2,'tp'=16] {'tp'}, dimensions={0} | all-to-all | bytes 131072 | tf_op jit(solution)/shard_map/all_to_all | solution.py:268
  155.8 16.0 %all_to_all.65 = bf16[32,8,256]{2,1,0:T(8,128)(2,1)S(1)} all-to-all(bf16[32,8,256]{2,1,0:T(8,128)(2,1)S(1)} %add_mixer.1), channel_id=1, replica_groups=mesh['z'=16,'c'=2,'tp'=16] {'c','tp'}, dimensions={0} | all-to-all | bytes 262144 | tf_op jit(solution)/shard_map/all_to_all | solution.py:268
  172.7 18.8 %all_to_all.66.parts = bf16[16,8,1408]{2,1,0:T(8,128)(2,1)S(1)} all-to-all(bf16[16,8,1408]{2,1,0:T(8,128)(2,1)S(1)} %second_products.1), channel_id=1, replica_groups=mesh['z'=16,'c'=2,'tp'=16] {'z'}, dimensions={0} | all-to-all | bytes 720896 | tf_op jit(solution)/shard_map/all_to_all | solution.py:268
  191.7 24.4 %all_to_all.67.hidden = bf16[16,8,640]{2,1,0:T(8,128)(2,1)S(1)} all-to-all(bf16[16,8,640]{2,1,0:T(8,128)(2,1)S(1)} %activate.3), channel_id=1, replica_groups=mesh['z'=16,'c'=2,'tp'=16] {'z'}, dimensions={0} | all-to-all | bytes 327680 | tf_op jit(solution)/shard_map/all_to_all | solution.py:268
  216.8 14.5 %all_to_all.68 = bf16[32,8,128]{2,1,0:T(8,128)(2,1)S(1)} all-to-all(bf16[32,8,128]{2,1,0:T(8,128)(2,1)S(1)} %bitcast.29), channel_id=1, replica_groups=mesh['z'=16,'c'=2,'tp'=16] {'c','tp'}, dimensions={0} | all-to-all | bytes 131072 | tf_op jit(solution)/shard_map/all_to_all | solution.py:268
  (69 shorter events, 17.2 us)
Async XLA Ops:
  0.0 25.9 %copy-start.2 = (bf16[128,640]{1,0:T(8,128)(2,1)S(1)}, bf16[128,640]{1,0:T(8,128)(2,1)}, u32[]{:S(2)}) copy-start(bf16[128,640]{1,0:T(8,128)(2,1)} %gate.1) | copy-start | bytes 491524
  0.0 25.9 %collective-permute-start.1 = (bf16[128,640]{1,0:T(8,128)(2,1)}, bf16[128,640]{1,0:T(8,128)(2,1)S(1)}, u32[]{:S(2)}, u32[]{:S(2)}) collective-permute-start(bf16[128,640]{1,0:T(8,128)(2,1)} %gate.1), channel_id=1, source_target_pairs={{0,16},{16,0},{1,17},{17,1},{2,18},{18,2},{3,19},{19,3},{4,20},{20... | collective-permute-start | bytes 491528 | tf_op jit(solution)/shard_map/early/ppermute | solution.py:272
  8.9 17.1 %collective-permute-start.2 = (bf16[128,640]{1,0:T(8,128)(2,1)}, bf16[128,640]{1,0:T(8,128)(2,1)S(1)}, u32[]{:S(2)}, u32[]{:S(2)}) collective-permute-start(bf16[128,640]{1,0:T(8,128)(2,1)} %up.1), channel_id=1, source_target_pairs={{0,16},{16,0},{1,17},{17,1},{2,18},{18,2},{3,19},{19,3},{4,20},{20... | collective-permute-start | bytes 491528 | tf_op jit(solution)/shard_map/early/ppermute | solution.py:272
  11.5 7.4 %collective-permute-start = (f32[3,128]{1,0:T(4,128)S(1)}, f32[3,128]{1,0:T(4,128)S(1)}, u32[]{:S(2)}, u32[]{:S(2)}) collective-permute-start(f32[3,128]{1,0:T(4,128)S(1)} %pad_maximum_fusion.gains), channel_id=1, source_target_pairs={{0,16},{16,0},{1,17},{17,1},{2,18},{18,2},{3,19},{19,3},{4,20},{20... | collective-permute-start | bytes 4616 | tf_op jit(solution)/shard_map/early/ppermute | solution.py:272
  15.2 10.7 %all-to-all-start = ((bf16[32,8,128]{2,1,0:T(8,128)(2,1)}), bf16[32,8,128]{2,1,0:T(8,128)(2,1)S(1)}, u32[]{:S(2)}, u32[]{:S(2)}) async-start(bf16[32,8,128]{2,1,0:T(8,128)(2,1)} %bitcast.3), calls=%async_computation | async-start | bytes 131072 | tf_op jit(solution)/shard_map/tokens/all_to_all | solution.py:268
  26.9 19.3 %copy-start.16 = (bf16[128,128]{1,0:T(8,128)(2,1)S(1)}, bf16[128,128]{1,0:T(8,128)(2,1)}, u32[]{:S(2)}) copy-start(bf16[128,128]{1,0:T(8,128)(2,1)} %param.34) | copy-start | bytes 98308
  26.9 19.3 %copy-start.17 = (bf16[128,128]{1,0:T(8,128)(2,1)S(1)}, bf16[128,128]{1,0:T(8,128)(2,1)}, u32[]{:S(2)}) copy-start(bf16[128,128]{1,0:T(8,128)(2,1)} %param.35) | copy-start | bytes 98308
  26.9 19.3 %copy-start.18 = (bf16[128,128]{1,0:T(8,128)(2,1)S(1)}, bf16[128,128]{1,0:T(8,128)(2,1)}, u32[]{:S(2)}) copy-start(bf16[128,128]{1,0:T(8,128)(2,1)} %param.36) | copy-start | bytes 98308
  28.5 14.7 %copy-start.1 = (bf16[640,128]{1,0:T(8,128)(2,1)S(1)}, bf16[640,128]{1,0:T(8,128)(2,1)}, u32[]{:S(2)}) copy-start(bf16[640,128]{1,0:T(8,128)(2,1)} %weight) | copy-start | bytes 491524
  28.5 17.7 %copy-start.15 = (bf16[128,128]{1,0:T(8,128)(2,1)S(1)}, bf16[128,128]{1,0:T(8,128)(2,1)}, u32[]{:S(2)}) copy-start(bf16[128,128]{1,0:T(8,128)(2,1)} %param.33) | copy-start | bytes 98308
  28.5 19.7 %copy-start.8 = (f32[8,1,128,128]{3,2,1,0:T(8,128)S(1)}, f32[8,1,128,128]{3,2,1,0:T(8,128)}, u32[]{:S(2)}) copy-start(f32[8,1,128,128]{3,2,1,0:T(8,128)} %param.47) | copy-start | bytes 1572868
  28.5 29.7 %all-to-all-start.1 = ((bf16[16,8,1408]{2,1,0:T(8,128)(2,1)}), bf16[16,8,1408]{2,1,0:T(8,128)(2,1)S(1)}, u32[]{:S(2)}, u32[]{:S(2)}) async-start(bf16[16,8,1408]{2,1,0:T(8,128)(2,1)} %first_products.1), calls=%async_computation.1 | async-start | bytes 720896 | tf_op jit(solution)/shard_map/all_to_all | solution.py:268
  41.8 6.4 %copy-start.12 = (f32[1,8,64]{2,1,0:T(8,128)S(1)}, f32[1,8,64]{2,1,0:T(8,128)}, u32[]{:S(2)}) copy-start(f32[1,8,64]{2,1,0:T(8,128)} %param.51) | copy-start | bytes 6148
  43.2 12.8 %collective-permute-start.3 = (bf16[640,128]{1,0:T(8,128)(2,1)S(1)}, bf16[640,128]{1,0:T(8,128)(2,1)S(1)}, u32[]{:S(2)}, u32[]{:S(2)}) collective-permute-start(bf16[640,128]{1,0:T(8,128)(2,1)S(1)} %copy-done.1), channel_id=1, source_target_pairs={{0,16},{16,0},{1,17},{17,1},{2,18},{18,2},{3,19},{19,3},{4,20},{20... | collective-permute-start | bytes 491528 | tf_op jit(solution)/shard_map/ppermute | solution.py:272
  46.2 9.7 %collective-permute-start.4 = (bf16[128,512]{1,0:T(8,128)(2,1)S(1)}, bf16[128,512]{1,0:T(8,128)(2,1)S(1)}, u32[]{:S(2)}, u32[]{:S(2)}) collective-permute-start(bf16[128,512]{1,0:T(8,128)(2,1)S(1)} %constant_dynamic-update-slice_fusion.main), channel_id=1, source_target_pairs={{0,16},{16,0},{1,17},{17,1},{2,18},{18,2},{3,19},{19,3},{4,20},{20... | collective-permute-start | bytes 393224 | tf_op jit(solution)/shard_map/ppermute | solution.py:272
  58.2 15.9 %copy-start.5 = (bf16[128,640]{1,0:T(8,128)(2,1)S(1)}, bf16[128,640]{1,0:T(8,128)(2,1)}, u32[]{:S(2)}) copy-start(bf16[128,640]{1,0:T(8,128)(2,1)} %up.2) | copy-start | bytes 491524
  58.2 20.2 %copy-start.6 = (bf16[128,128]{1,0:T(8,128)(2,1)S(1)}, bf16[128,128]{1,0:T(8,128)(2,1)}, u32[]{:S(2)}) copy-start(bf16[128,128]{1,0:T(8,128)(2,1)} %weight.1) | copy-start | bytes 98308
  59.0 12.0 %copy-start.4 = (bf16[128,640]{1,0:T(8,128)(2,1)S(1)}, bf16[128,640]{1,0:T(8,128)(2,1)}, u32[]{:S(2)}) copy-start(bf16[128,640]{1,0:T(8,128)(2,1)} %gate.2) | copy-start | bytes 491524
  59.0 16.9 %copy-start = (bf16[640,128]{1,0:T(8,128)(2,1)S(1)}, bf16[640,128]{1,0:T(8,128)(2,1)}, u32[]{:S(2)}) copy-start(bf16[640,128]{1,0:T(8,128)(2,1)} %weight.2) | copy-start | bytes 491524
  59.0 24.1 %all-to-all-start.2 = ((bf16[16,8,640]{2,1,0:T(8,128)(2,1)}), bf16[16,8,640]{2,1,0:T(8,128)(2,1)S(1)}, u32[]{:S(2)}, u32[]{:S(2)}) async-start(bf16[16,8,640]{2,1,0:T(8,128)(2,1)} %activate.2), calls=%async_computation.2 | async-start | bytes 327680 | tf_op jit(solution)/shard_map/all_to_all | solution.py:268
  71.0 10.5 %collective-permute-start.6 = (bf16[128,640]{1,0:T(8,128)(2,1)S(1)}, bf16[128,640]{1,0:T(8,128)(2,1)S(1)}, u32[]{:S(2)}, u32[]{:S(2)}) collective-permute-start(bf16[128,640]{1,0:T(8,128)(2,1)S(1)} %copy-done.4), channel_id=1, source_target_pairs={{0,16},{16,0},{1,17},{17,1},{2,18},{18,2},{3,19},{19,3},{4,20},{20... | collective-permute-start | bytes 491528 | tf_op jit(solution)/shard_map/ppermute | solution.py:272
  74.0 7.5 %collective-permute-start.7 = (bf16[128,640]{1,0:T(8,128)(2,1)S(1)}, bf16[128,640]{1,0:T(8,128)(2,1)S(1)}, u32[]{:S(2)}, u32[]{:S(2)}) collective-permute-start(bf16[128,640]{1,0:T(8,128)(2,1)S(1)} %copy-done.5), channel_id=1, source_target_pairs={{0,16},{16,0},{1,17},{17,1},{2,18},{18,2},{3,19},{19,3},{4,20},{20... | collective-permute-start | bytes 491528 | tf_op jit(solution)/shard_map/ppermute | solution.py:272
  76.0 5.5 %collective-permute-start.8 = (bf16[640,128]{1,0:T(8,128)(2,1)S(1)}, bf16[640,128]{1,0:T(8,128)(2,1)S(1)}, u32[]{:S(2)}, u32[]{:S(2)}) collective-permute-start(bf16[640,128]{1,0:T(8,128)(2,1)S(1)} %copy-done), channel_id=1, source_target_pairs={{0,16},{16,0},{1,17},{17,1},{2,18},{18,2},{3,19},{19,3},{4,20},{20... | collective-permute-start | bytes 491528 | tf_op jit(solution)/shard_map/ppermute | solution.py:272
  78.4 3.1 %collective-permute-start.5 = (bf16[128,128]{1,0:T(8,128)(2,1)S(1)}, bf16[128,128]{1,0:T(8,128)(2,1)S(1)}, u32[]{:S(2)}, u32[]{:S(2)}) collective-permute-start(bf16[128,128]{1,0:T(8,128)(2,1)S(1)} %copy-done.6), channel_id=1, source_target_pairs={{0,16},{16,0},{1,17},{17,1},{2,18},{18,2},{3,19},{19,3},{4,20},{20... | collective-permute-start | bytes 98312 | tf_op jit(solution)/shard_map/ppermute | solution.py:272
  (7 other events, 20.7 us)

commit v3 on v2

--- a/solution.py
+++ b/solution.py
@@ -27,7 +27,6 @@
         out_specs=[vmem] * len(outs),
         compiler_params=pltpu.CompilerParams(vmem_limit_bytes=limit),
         cost_estimate=pl.CostEstimate(flops=flops, bytes_accessed=size, transcendentals=0),
-        name=fn.__name__,
     )(*args)
     return got if isinstance(out, list) else got[0]
 
@@ -169,7 +168,9 @@
     out[:, :, n:] = blocked(lane_tile(wide.shape[0], columns), count).astype(bf16)
 
 
-def earlier_state(lengths, head, recurrent, keys, values, strength, decay, extra, state, new):
+def earlier_state(
+    lengths, head, recurrent, keys, values, strength, decay, extra, gain, state, new, gains
+):
     count, span = strength.shape
     sequence = lax.broadcasted_iota(jnp.int32, (count, span), 0)
     lane = lax.broadcasted_iota(jnp.int32, (count, span), 1)
@@ -182,6 +183,7 @@
     amount = jnp.where(before, amount, 0.0)
     new_extra = jnp.sum(jnp.where(lane == latest, extra[...], 0.0), -1, keepdims=True)
     new[...] = jnp.broadcast_to(new_extra, new.shape)
+    gains[...] = jnp.broadcast_to(gain[...], gains.shape)
     row = lax.broadcasted_iota(jnp.int32, (span, span), 0)
     col = lax.broadcasted_iota(jnp.int32, (span, span), 1)
     cumul = exact(amount, (row <= col).astype(f32))
@@ -276,7 +278,7 @@
     return lax.optimization_barrier(trees)
 
 
-def body(
+def layer(
     tokens,
     first_norm_gain,
     first_gate_weight,
@@ -316,13 +318,13 @@
     head = jnp.concatenate([head_decay_speed, head_decay_offset])
 
     blocks = jnp.broadcast_to(tokens.reshape(2, 1, rows, width), (2, plane, rows, width))
-    with jax.named_scope("tokens"):
-        got = exchange(blocks.reshape(2 * plane, rows, width), ("c", "tp"))
+    got = exchange(blocks.reshape(2 * plane, rows, width), ("c", "tp"))
     got = got.reshape(2, plane, rows, width)
 
     gains = jnp.stack([first_norm_gain, mixer_norm_gain, second_norm_gain])
-    with jax.named_scope("early"):
-        gains_x, gate_x, up_x = swap(gains), swap(first_gate_weight), swap(first_up_weight)
+    gate_x = swap(first_gate_weight)
+    up_x = swap(first_up_weight)
+    gains_x = swap(gains)
     sent = kernel(
         first_products,
         ((ring, rows, 2 * hidden_units + LANES), bf16),
@@ -354,6 +356,7 @@
             decay_input_history,
             position_decay_extra,
             lengths,
+            head_norm_gain,
             mixer_out_weight,
             second_gate_weight,
             second_up_weight,
@@ -375,6 +378,7 @@
         decay_input_history,
         position_decay_extra,
         lengths,
+        head_norm_gain,
         mixer_out_weight,
         second_gate_weight,
         second_up_weight,
@@ -393,9 +397,13 @@
     ws, ws_x = small(strength_weight, core), small(strength_weight, 1 - core)
     wd, wd_x = small(decay_weight, core), small(decay_weight, 1 - core)
     local = lengths.shape[0]
-    state, new_extra = kernel(
+    state, new_extra, norm_gain = kernel(
         earlier_state,
-        [((local, dk, recurrent.shape[-1]), f32), ((local, LANES), f32)],
+        [
+            ((local, dk, recurrent.shape[-1]), f32),
+            ((local, LANES), f32),
+            ((local, recurrent.shape[-1]), f32),
+        ],
         lengths,
         head,
         recurrent[:, 0],
@@ -404,11 +412,12 @@
         strength_logit_history[0],
         decay_input_history[0],
         position_decay_extra[0],
+        head_norm_gain[None],
         scalars=2,
         flops=1 << 28,
     )
-    parts, down_x, main, main_x, ws, ws_x, wd, wd_x, state, new_extra = together(
-        parts, down_x, main, main_x, ws, ws_x, wd, wd_x, state, new_extra
+    parts, down_x, main, main_x, ws, ws_x, wd, wd_x, state, new_extra, norm_gain = together(
+        parts, down_x, main, main_x, ws, ws_x, wd, wd_x, state, new_extra, norm_gain
     )
 
     hidden = kernel(
@@ -451,7 +460,7 @@
         parts,
         state,
         new_extra,
-        head_norm_gain[None],
+        norm_gain,
         scalars=1,
         features=features,
     )
@@ -498,7 +507,7 @@
     split = Mesh(mesh.devices.reshape(kv // 2, 2, tp), ("z", "c", "tp"))
     kv = ("z", "c")
     return jax.shard_map(
-        body,
+        layer,
         mesh=split,
         in_specs=(
             P("tp", kv),

time: 234 us -> 233 us (level)
  no operation moved by 1% of the time
where the time goes in v3:
time: 233 us; the launch traced here: 232 us
  blocking collectives  142 us (61%)
  starting transfers between devices  56.2 us (24%)
  Pallas kernels  15.6 us (7%)
  waiting for transfers between devices  12 us (5%)
  local copies, waits for them, and re-layouts  3.72 us (2%)
    all_to_all x9, blocking collectives, exchange(): return lax.all_to_all(x, axis, 0, 0, tiled=True)  142 us
    all_to_all x3, starting transfers between devices, exchange(): return lax.all_to_all(x, axis, 0, 0, tiled=True)  28.9 us
    ppermute x9, starting transfers between devices, swap(): return lax.ppermute(x, 'c', [(0, 1), (1, 0)])  27.2 us
    pallas_call x13, Pallas kernels, kernel(): pl.pallas_call(functools.partial(fn, **static), out_shape=shapes, in_spec...  15.6 us
    all_to_all x3, waiting for transfers between devices, exchange(): return lax.all_to_all(x, axis, 0, 0, tiled=True)  10.8 us
  transfers between devices with their start and end apart: 12, of which 4 were waited for; matrix products, arithmetic and copies ran while one was open for 1% of the time, Pallas kernels for 3%

profile of v3, /device:TPU:1, one launch (start us, length us, event | category | flops | bytes accessed | tf_op | source)
XLA Modules:
  0.0 231.9 jit_solution(13301234435236248429)
XLA Ops:
  0.0 8.9 %collective-permute-start.1 = (bf16[128,640]{1,0:T(8,128)(2,1)}, bf16[128,640]{1,0:T(8,128)(2,1)S(1)}, u32[]{:S(2)}, u32[]{:S(2)}) collective-permute-start(bf16[128,640]{1,0:T(8,128)(2,1)} %gate.1), channel_id=1, source_target_pairs={{0,16},{16,0},{1,17},{17,1},{2,18},{18,2},{3,19},{19,3},{4,20},{20... | collective-permute-start | bytes 491528 | tf_op jit(solution)/shard_map/ppermute | solution.py:274
  8.9 1.9 collective-permute-start.2
  11.5 2.4 %collective-permute-start = (f32[3,128]{1,0:T(4,128)S(1)}, f32[3,128]{1,0:T(4,128)S(1)}, u32[]{:S(2)}, u32[]{:S(2)}) collective-permute-start(f32[3,128]{1,0:T(4,128)S(1)} %pad_maximum_fusion.gains), channel_id=1, source_target_pairs={{0,16},{16,0},{1,17},{17,1},{2,18},{18,2},{3,19},{19,3},{4,20},{20... | collective-permute-start | bytes 4616 | tf_op jit(solution)/shard_map/ppermute | solution.py:274
  15.2 3.6 %all-to-all-start = ((bf16[32,8,128]{2,1,0:T(8,128)(2,1)}), bf16[32,8,128]{2,1,0:T(8,128)(2,1)S(1)}, u32[]{:S(2)}, u32[]{:S(2)}) async-start(bf16[32,8,128]{2,1,0:T(8,128)(2,1)} %bitcast.3), calls=%async_computation | async-start | bytes 131072 | tf_op jit(solution)/shard_map/all_to_all | solution.py:270
  18.9 7.0 %all-to-all-done = bf16[32,8,128]{2,1,0:T(8,128)(2,1)S(1)} async-done(((bf16[32,8,128]{2,1,0:T(8,128)(2,1)}), bf16[32,8,128]{2,1,0:T(8,128)(2,1)S(1)}, u32[]{:S(2)}, u32[]{:S(2)}) %all-to-all-start) | async-done | bytes 65568 | tf_op jit(solution)/shard_map/all_to_all | solution.py:270
  28.5 13.3 %all-to-all-start.1 = ((bf16[16,8,1408]{2,1,0:T(8,128)(2,1)}), bf16[16,8,1408]{2,1,0:T(8,128)(2,1)S(1)}, u32[]{:S(2)}, u32[]{:S(2)}) async-start(bf16[16,8,1408]{2,1,0:T(8,128)(2,1)} %shard_map.253), calls=%async_computation.1 | async-start | bytes 720896 | tf_op jit(solution)/shard_map/all_to_all | solution.py:270
  43.2 2.9 %collective-permute-start.3 = (bf16[640,128]{1,0:T(8,128)(2,1)S(1)}, bf16[640,128]{1,0:T(8,128)(2,1)S(1)}, u32[]{:S(2)}, u32[]{:S(2)}) collective-permute-start(bf16[640,128]{1,0:T(8,128)(2,1)S(1)} %copy-done.1), channel_id=1, source_target_pairs={{0,16},{16,0},{1,17},{17,1},{2,18},{18,2},{3,19},{19,3},{4,20},{20... | collective-permute-start | bytes 491528 | tf_op jit(solution)/shard_map/ppermute | solution.py:274
  46.2 1.9 collective-permute-start.4
  48.9 6.4 %shard_map.254 = (f32[8,128,128]{2,1,0:T(8,128)S(1)}, f32[8,128]{1,0:T(8,128)S(1)}, f32[8,128]{1,0:T(8,128)S(1)}) custom-call(s32[8]{0:T(128)S(1)} %copy-done.13, f32[2]{0:T(128)S(1)} %pad_maximum_fusion.1.head, f32[8,128,128]{2,1,0:T(8,128)S(1)} %bitcast.30, bf16[8,64,128]{2,1,0:T(8,128)(2,1)S(1)} %copy-done.8, bf16[8,64,128]{2,1,0:T(8,128)(2,1)S(1)} %copy-done.9, ...), custom_call_target="tpu_custom_call" | custom-call | flops 268435456 | bytes 793128 | tf_op jit(solution)/shard_map/pallas_call | solution.py:23
  56.0 2.2 all-to-all-done.1.parts
  59.0 12.0 %all-to-all-start.2 = ((bf16[16,8,640]{2,1,0:T(8,128)(2,1)}), bf16[16,8,640]{2,1,0:T(8,128)(2,1)S(1)}, u32[]{:S(2)}, u32[]{:S(2)}) async-start(bf16[16,8,640]{2,1,0:T(8,128)(2,1)} %shard_map.255), calls=%async_computation.2 | async-start | bytes 327680 | tf_op jit(solution)/shard_map/all_to_all | solution.py:270
  71.0 3.0 %collective-permute-start.6 = (bf16[128,640]{1,0:T(8,128)(2,1)S(1)}, bf16[128,640]{1,0:T(8,128)(2,1)S(1)}, u32[]{:S(2)}, u32[]{:S(2)}) collective-permute-start(bf16[128,640]{1,0:T(8,128)(2,1)S(1)} %copy-done.4), channel_id=1, source_target_pairs={{0,16},{16,0},{1,17},{17,1},{2,18},{18,2},{3,19},{19,3},{4,20},{20... | collective-permute-start | bytes 491528 | tf_op jit(solution)/shard_map/ppermute | solution.py:274
  74.0 1.9 collective-permute-start.7
  76.0 2.4 %collective-permute-start.8 = (bf16[640,128]{1,0:T(8,128)(2,1)S(1)}, bf16[640,128]{1,0:T(8,128)(2,1)S(1)}, u32[]{:S(2)}, u32[]{:S(2)}) collective-permute-start(bf16[640,128]{1,0:T(8,128)(2,1)S(1)} %copy-done), channel_id=1, source_target_pairs={{0,16},{16,0},{1,17},{17,1},{2,18},{18,2},{3,19},{19,3},{4,20},{20... | collective-permute-start | bytes 491528 | tf_op jit(solution)/shard_map/ppermute | solution.py:274
  78.4 1.9 collective-permute-start.5
  83.4 9.9 %all_to_all.60.parts = bf16[16,8,256]{2,1,0:T(8,128)(2,1)S(1)} all-to-all(bf16[16,8,256]{2,1,0:T(8,128)(2,1)S(1)} %shard_map.256), channel_id=1, replica_groups=mesh['z'=16,'c'=2,'tp'=16] {'tp'}, dimensions={0} | all-to-all | bytes 131072 | tf_op jit(solution)/shard_map/all_to_all | solution.py:270
  93.9 9.4 %all_to_all.61.middle = bf16[16,8,256]{2,1,0:T(8,128)(2,1)S(1)} all-to-all(bf16[16,8,256]{2,1,0:T(8,128)(2,1)S(1)} %shard_map.257), channel_id=1, replica_groups=mesh['z'=16,'c'=2,'tp'=16] {'tp'}, dimensions={0} | all-to-all | bytes 131072 | tf_op jit(solution)/shard_map/all_to_all | solution.py:270
  104.1 21.9 %all_to_all.62.parts = bf16[16,8,640]{2,1,0:T(8,128)(2,1)S(1)} all-to-all(bf16[16,8,640]{2,1,0:T(8,128)(2,1)S(1)} %shard_map.258), channel_id=1, replica_groups=mesh['z'=16,'c'=2,'tp'=16] {'z'}, dimensions={0} | all-to-all | bytes 327680 | tf_op jit(solution)/shard_map/all_to_all | solution.py:270
  127.4 16.4 %all_to_all.63.hidden = bf16[16,8,128]{2,1,0:T(8,128)(2,1)S(1)} all-to-all(bf16[16,8,128]{2,1,0:T(8,128)(2,1)S(1)} %shard_map.259), channel_id=1, replica_groups=mesh['z'=16,'c'=2,'tp'=16] {'z'}, dimensions={0} | all-to-all | bytes 65536 | tf_op jit(solution)/shard_map/all_to_all | solution.py:270
  143.9 10.6 %all_to_all.64.parts = bf16[16,8,256]{2,1,0:T(8,128)(2,1)S(1)} all-to-all(bf16[16,8,256]{2,1,0:T(8,128)(2,1)S(1)} %shard_map.260), channel_id=1, replica_groups=mesh['z'=16,'c'=2,'tp'=16] {'tp'}, dimensions={0} | all-to-all | bytes 131072 | tf_op jit(solution)/shard_map/all_to_all | solution.py:270
  155.1 16.0 %all_to_all.65 = bf16[32,8,256]{2,1,0:T(8,128)(2,1)S(1)} all-to-all(bf16[32,8,256]{2,1,0:T(8,128)(2,1)S(1)} %shard_map.261), channel_id=1, replica_groups=mesh['z'=16,'c'=2,'tp'=16] {'c','tp'}, dimensions={0} | all-to-all | bytes 262144 | tf_op jit(solution)/shard_map/all_to_all | solution.py:270
  172.0 18.8 %all_to_all.66.parts = bf16[16,8,1408]{2,1,0:T(8,128)(2,1)S(1)} all-to-all(bf16[16,8,1408]{2,1,0:T(8,128)(2,1)S(1)} %shard_map.262), channel_id=1, replica_groups=mesh['z'=16,'c'=2,'tp'=16] {'z'}, dimensions={0} | all-to-all | bytes 720896 | tf_op jit(solution)/shard_map/all_to_all | solution.py:270
  191.0 24.4 %all_to_all.67.hidden = bf16[16,8,640]{2,1,0:T(8,128)(2,1)S(1)} all-to-all(bf16[16,8,640]{2,1,0:T(8,128)(2,1)S(1)} %shard_map.263), channel_id=1, replica_groups=mesh['z'=16,'c'=2,'tp'=16] {'z'}, dimensions={0} | all-to-all | bytes 327680 | tf_op jit(solution)/shard_map/all_to_all | solution.py:270
  216.2 14.5 %all_to_all.68 = bf16[32,8,128]{2,1,0:T(8,128)(2,1)S(1)} all-to-all(bf16[32,8,128]{2,1,0:T(8,128)(2,1)S(1)} %bitcast.29), channel_id=1, replica_groups=mesh['z'=16,'c'=2,'tp'=16] {'c','tp'}, dimensions={0} | all-to-all | bytes 131072 | tf_op jit(solution)/shard_map/all_to_all | solution.py:270
  (69 shorter events, 16.6 us)
Async XLA Ops:
  0.0 25.9 %copy-start.2 = (bf16[128,640]{1,0:T(8,128)(2,1)S(1)}, bf16[128,640]{1,0:T(8,128)(2,1)}, u32[]{:S(2)}) copy-start(bf16[128,640]{1,0:T(8,128)(2,1)} %gate.1) | copy-start | bytes 491524
  0.0 25.9 %collective-permute-start.1 = (bf16[128,640]{1,0:T(8,128)(2,1)}, bf16[128,640]{1,0:T(8,128)(2,1)S(1)}, u32[]{:S(2)}, u32[]{:S(2)}) collective-permute-start(bf16[128,640]{1,0:T(8,128)(2,1)} %gate.1), channel_id=1, source_target_pairs={{0,16},{16,0},{1,17},{17,1},{2,18},{18,2},{3,19},{19,3},{4,20},{20... | collective-permute-start | bytes 491528 | tf_op jit(solution)/shard_map/ppermute | solution.py:274
  8.9 17.1 %collective-permute-start.2 = (bf16[128,640]{1,0:T(8,128)(2,1)}, bf16[128,640]{1,0:T(8,128)(2,1)S(1)}, u32[]{:S(2)}, u32[]{:S(2)}) collective-permute-start(bf16[128,640]{1,0:T(8,128)(2,1)} %up.1), channel_id=1, source_target_pairs={{0,16},{16,0},{1,17},{17,1},{2,18},{18,2},{3,19},{19,3},{4,20},{20... | collective-permute-start | bytes 491528 | tf_op jit(solution)/shard_map/ppermute | solution.py:274
  11.5 7.4 %collective-permute-start = (f32[3,128]{1,0:T(4,128)S(1)}, f32[3,128]{1,0:T(4,128)S(1)}, u32[]{:S(2)}, u32[]{:S(2)}) collective-permute-start(f32[3,128]{1,0:T(4,128)S(1)} %pad_maximum_fusion.gains), channel_id=1, source_target_pairs={{0,16},{16,0},{1,17},{17,1},{2,18},{18,2},{3,19},{19,3},{4,20},{20... | collective-permute-start | bytes 4616 | tf_op jit(solution)/shard_map/ppermute | solution.py:274
  15.2 10.7 %all-to-all-start = ((bf16[32,8,128]{2,1,0:T(8,128)(2,1)}), bf16[32,8,128]{2,1,0:T(8,128)(2,1)S(1)}, u32[]{:S(2)}, u32[]{:S(2)}) async-start(bf16[32,8,128]{2,1,0:T(8,128)(2,1)} %bitcast.3), calls=%async_computation | async-start | bytes 131072 | tf_op jit(solution)/shard_map/all_to_all | solution.py:270
  26.9 19.3 %copy-start.16 = (bf16[128,128]{1,0:T(8,128)(2,1)S(1)}, bf16[128,128]{1,0:T(8,128)(2,1)}, u32[]{:S(2)}) copy-start(bf16[128,128]{1,0:T(8,128)(2,1)} %param.34) | copy-start | bytes 98308
  26.9 19.3 %copy-start.17 = (bf16[128,128]{1,0:T(8,128)(2,1)S(1)}, bf16[128,128]{1,0:T(8,128)(2,1)}, u32[]{:S(2)}) copy-start(bf16[128,128]{1,0:T(8,128)(2,1)} %param.35) | copy-start | bytes 98308
  26.9 19.3 %copy-start.18 = (bf16[128,128]{1,0:T(8,128)(2,1)S(1)}, bf16[128,128]{1,0:T(8,128)(2,1)}, u32[]{:S(2)}) copy-start(bf16[128,128]{1,0:T(8,128)(2,1)} %param.36) | copy-start | bytes 98308
  28.5 14.7 %copy-start.1 = (bf16[640,128]{1,0:T(8,128)(2,1)S(1)}, bf16[640,128]{1,0:T(8,128)(2,1)}, u32[]{:S(2)}) copy-start(bf16[640,128]{1,0:T(8,128)(2,1)} %weight) | copy-start | bytes 491524
  28.5 17.6 %copy-start.15 = (bf16[128,128]{1,0:T(8,128)(2,1)S(1)}, bf16[128,128]{1,0:T(8,128)(2,1)}, u32[]{:S(2)}) copy-start(bf16[128,128]{1,0:T(8,128)(2,1)} %param.33) | copy-start | bytes 98308
  28.5 19.7 %copy-start.7 = (f32[8,1,128,128]{3,2,1,0:T(8,128)S(1)}, f32[8,1,128,128]{3,2,1,0:T(8,128)}, u32[]{:S(2)}) copy-start(f32[8,1,128,128]{3,2,1,0:T(8,128)} %param.47) | copy-start | bytes 1572868
  28.5 29.7 %all-to-all-start.1 = ((bf16[16,8,1408]{2,1,0:T(8,128)(2,1)}), bf16[16,8,1408]{2,1,0:T(8,128)(2,1)S(1)}, u32[]{:S(2)}, u32[]{:S(2)}) async-start(bf16[16,8,1408]{2,1,0:T(8,128)(2,1)} %shard_map.253), calls=%async_computation.1 | async-start | bytes 720896 | tf_op jit(solution)/shard_map/all_to_all | solution.py:270
  41.8 6.4 %copy-start.12 = (f32[1,8,64]{2,1,0:T(8,128)S(1)}, f32[1,8,64]{2,1,0:T(8,128)}, u32[]{:S(2)}) copy-start(f32[1,8,64]{2,1,0:T(8,128)} %param.52) | copy-start | bytes 6148
  43.2 12.8 %collective-permute-start.3 = (bf16[640,128]{1,0:T(8,128)(2,1)S(1)}, bf16[640,128]{1,0:T(8,128)(2,1)S(1)}, u32[]{:S(2)}, u32[]{:S(2)}) collective-permute-start(bf16[640,128]{1,0:T(8,128)(2,1)S(1)} %copy-done.1), channel_id=1, source_target_pairs={{0,16},{16,0},{1,17},{17,1},{2,18},{18,2},{3,19},{19,3},{4,20},{20... | collective-permute-start | bytes 491528 | tf_op jit(solution)/shard_map/ppermute | solution.py:274
  46.2 9.8 %collective-permute-start.4 = (bf16[128,512]{1,0:T(8,128)(2,1)S(1)}, bf16[128,512]{1,0:T(8,128)(2,1)S(1)}, u32[]{:S(2)}, u32[]{:S(2)}) collective-permute-start(bf16[128,512]{1,0:T(8,128)(2,1)S(1)} %constant_dynamic-update-slice_fusion.main), channel_id=1, source_target_pairs={{0,16},{16,0},{1,17},{17,1},{2,18},{18,2},{3,19},{19,3},{4,20},{20... | collective-permute-start | bytes 393224 | tf_op jit(solution)/shard_map/ppermute | solution.py:274
  58.2 15.9 %copy-start.5 = (bf16[128,640]{1,0:T(8,128)(2,1)S(1)}, bf16[128,640]{1,0:T(8,128)(2,1)}, u32[]{:S(2)}) copy-start(bf16[128,640]{1,0:T(8,128)(2,1)} %up.2) | copy-start | bytes 491524
  58.2 20.2 %copy-start.6 = (bf16[128,128]{1,0:T(8,128)(2,1)S(1)}, bf16[128,128]{1,0:T(8,128)(2,1)}, u32[]{:S(2)}) copy-start(bf16[128,128]{1,0:T(8,128)(2,1)} %weight.1) | copy-start | bytes 98308
  59.0 12.0 %copy-start.4 = (bf16[128,640]{1,0:T(8,128)(2,1)S(1)}, bf16[128,640]{1,0:T(8,128)(2,1)}, u32[]{:S(2)}) copy-start(bf16[128,640]{1,0:T(8,128)(2,1)} %gate.2) | copy-start | bytes 491524
  59.0 16.9 %copy-start = (bf16[640,128]{1,0:T(8,128)(2,1)S(1)}, bf16[640,128]{1,0:T(8,128)(2,1)}, u32[]{:S(2)}) copy-start(bf16[640,128]{1,0:T(8,128)(2,1)} %weight.2) | copy-start | bytes 491524
  59.0 24.1 %all-to-all-start.2 = ((bf16[16,8,640]{2,1,0:T(8,128)(2,1)}), bf16[16,8,640]{2,1,0:T(8,128)(2,1)S(1)}, u32[]{:S(2)}, u32[]{:S(2)}) async-start(bf16[16,8,640]{2,1,0:T(8,128)(2,1)} %shard_map.255), calls=%async_computation.2 | async-start | bytes 327680 | tf_op jit(solution)/shard_map/all_to_all | solution.py:270
  71.0 10.5 %collective-permute-start.6 = (bf16[128,640]{1,0:T(8,128)(2,1)S(1)}, bf16[128,640]{1,0:T(8,128)(2,1)S(1)}, u32[]{:S(2)}, u32[]{:S(2)}) collective-permute-start(bf16[128,640]{1,0:T(8,128)(2,1)S(1)} %copy-done.4), channel_id=1, source_target_pairs={{0,16},{16,0},{1,17},{17,1},{2,18},{18,2},{3,19},{19,3},{4,20},{20... | collective-permute-start | bytes 491528 | tf_op jit(solution)/shard_map/ppermute | solution.py:274
  74.0 7.5 %collective-permute-start.7 = (bf16[128,640]{1,0:T(8,128)(2,1)S(1)}, bf16[128,640]{1,0:T(8,128)(2,1)S(1)}, u32[]{:S(2)}, u32[]{:S(2)}) collective-permute-start(bf16[128,640]{1,0:T(8,128)(2,1)S(1)} %copy-done.5), channel_id=1, source_target_pairs={{0,16},{16,0},{1,17},{17,1},{2,18},{18,2},{3,19},{19,3},{4,20},{20... | collective-permute-start | bytes 491528 | tf_op jit(solution)/shard_map/ppermute | solution.py:274
  76.0 5.5 %collective-permute-start.8 = (bf16[640,128]{1,0:T(8,128)(2,1)S(1)}, bf16[640,128]{1,0:T(8,128)(2,1)S(1)}, u32[]{:S(2)}, u32[]{:S(2)}) collective-permute-start(bf16[640,128]{1,0:T(8,128)(2,1)S(1)} %copy-done), channel_id=1, source_target_pairs={{0,16},{16,0},{1,17},{17,1},{2,18},{18,2},{3,19},{19,3},{4,20},{20... | collective-permute-start | bytes 491528 | tf_op jit(solution)/shard_map/ppermute | solution.py:274
  78.4 3.1 %collective-permute-start.5 = (bf16[128,128]{1,0:T(8,128)(2,1)S(1)}, bf16[128,128]{1,0:T(8,128)(2,1)S(1)}, u32[]{:S(2)}, u32[]{:S(2)}) collective-permute-start(bf16[128,128]{1,0:T(8,128)(2,1)S(1)} %copy-done.6), channel_id=1, source_target_pairs={{0,16},{16,0},{1,17},{17,1},{2,18},{18,2},{3,19},{19,3},{4,20},{20... | collective-permute-start | bytes 98312 | tf_op jit(solution)/shard_map/ppermute | solution.py:274
  (7 other events, 13.7 us)

commit v4 on v3

--- a/solution.py
+++ b/solution.py
@@ -11,6 +11,7 @@
 f32 = jnp.float32
 bf16 = jnp.bfloat16
 LANES = 128
+Z = ("zh", "za")
 EPS = 1e-06
 
 
@@ -77,42 +78,32 @@
     return jnp.maximum(x, 0.0) + jnp.log1p(jnp.exp(-jnp.abs(x)))
 
 
-def gate_up(own, other, gain, gain_x, gates, ups, out):
+def gate_up(slots, gates, ups, out):
     n = gates[0].shape[1]
     count = out.shape[0]
-    scaled, scaled_x = (own * gain).astype(bf16), (other * gain_x).astype(bf16)
-    for at, pair in ((0, gates), (n, ups)):
-        part = dot(scaled, pair[0][...]) + dot(scaled_x, pair[1][...])
+    scaled = [(x * gain).astype(bf16) for x, gain in slots]
+    for at, weights in ((0, gates), (n, ups)):
+        part = sum(dot(x, w[...]) for x, w in zip(scaled, weights))
         out[:, :, at : at + n] = blocked(part, count).astype(bf16)
-    square = jnp.sum(own * own + other * other, -1, keepdims=True)
-    out[:, :, 2 * n :] = blocked(lane_tile(own.shape[0], [square]), count).astype(bf16)
+    square = jnp.sum(sum(x * x for x, _ in slots), -1, keepdims=True)
+    out[:, :, 2 * n :] = blocked(lane_tile(square.shape[0], [square]), count).astype(bf16)
 
 
 def first_products(ids, got, gains, gains_x, gate, gate_x, up, up_x, out):
     core = ids[0]
-    gate_up(
-        flat(got[core]),
-        flat(got[1 - core]),
-        gains[0:1],
-        gains_x[0:1],
-        (gate, gate_x),
-        (up, up_x),
-        out,
-    )
-
-
-def second_products(ids, got, gains, gains_x, gate, gate_x, up, up_x, out):
-    wide = flat(got[ids[0]])
-    half = wide.shape[1] // 2
-    gate_up(
-        wide[:, :half],
-        wide[:, half:],
-        gains[2:3],
-        gains_x[2:3],
-        (gate, gate_x),
-        (up, up_x),
-        out,
-    )
+    slots = [(flat(got[core]), gains[0:1]), (flat(got[1 - core]), gains_x[0:1])]
+    gate_up(slots, (gate, gate_x), (up, up_x), out)
+
+
+def second_products(ids, got, gains, gains_x, gains_z, *refs):
+    out = refs[-1]
+    side = ids[2]
+    slots = []
+    for chip, pair in ((side, (gains, gains_x)), (1 - side, (gains_z.at[0], gains_z.at[1]))):
+        wide = flat(got[chip, :, side])
+        half = wide.shape[1] // 2
+        slots += [(wide[:, :half], pair[0][2:3]), (wide[:, half:], pair[1][2:3])]
+    gate_up(slots, refs[0:4], refs[4:8], out)
 
 
 def activate(parts, out, *, features):
@@ -130,10 +121,14 @@
     out[:, :, half:] = blocked(dot(rows, weight_x[...]), out.shape[0]).astype(bf16)
 
 
-def last_down(ids, hidden, weight, weight_x, out):
+def last_down(ids, hidden, *refs):
+    out = refs[-1]
+    core, side = ids[0], ids[2]
     rows = flat(hidden[...]).astype(bf16)
-    out[ids[0]] = blocked(dot(rows, weight[...]), out.shape[1]).astype(bf16)
-    out[1 - ids[0]] = blocked(dot(rows, weight_x[...]), out.shape[1]).astype(bf16)
+    out[...] = jnp.zeros(out.shape, bf16)
+    for i, weight in enumerate(refs[:-1]):
+        chip, half = (side, 1 - side)[i // 2], (core, 1 - core)[i % 2]
+        out[chip, half, :, side] = blocked(dot(rows, weight[...]), out.shape[2]).astype(bf16)
 
 
 def add_first(ids, parts, got, out):
@@ -144,10 +139,11 @@
     out[...] = jnp.broadcast_to(rows[None], out.shape).astype(bf16)
 
 
-def add_mixer(ids, parts, middle, out):
+def add_mixer(ids, parts, middle, out, other):
     sums = jnp.sum(parts[...].astype(f32), axis=0)
-    rows = middle[ids[1]].astype(f32) + sums
-    out[...] = jnp.broadcast_to(rows[None], out.shape).astype(bf16)
+    rows = (middle[ids[1]].astype(f32) + sums).astype(bf16)
+    out[...] = jnp.broadcast_to(rows.astype(f32)[None], out.shape).astype(bf16)
+    other[...] = rows[:, rows.shape[1] // 2 :]
 
 
 def project(ids, middle, gains, gains_x, main, main_x, ws, ws_x, wd, wd_x, out):
@@ -254,16 +250,14 @@
     out[...] = jnp.broadcast_to(rows[None], out.shape).astype(bf16)
 
 
-def finish(ids, parts, got, out):
-    core, block = ids[0], ids[1]
-    sums = jnp.sum(parts[...].astype(f32), axis=1)
-    half = sums.shape[-1]
-    rows = []
-    for c in range(2):
-        wide = got[c, block].astype(f32)
-        mine = jnp.where(core == c, wide[:, :half], wide[:, half:])
-        rows.append(mine + 0.5 * sums[c])
-    out[...] = jnp.concatenate(rows, 0).astype(bf16)
+def finish(ids, parts, got, other, out):
+    core, block, side = ids[0], ids[1], ids[2]
+    sums = jnp.sum(parts[ids[3]].astype(f32), axis=1)
+    mine = got[side, block][:, : sums.shape[-1]].astype(f32)
+    theirs = other[...].astype(f32)
+    low = jnp.where(core == 0, mine, theirs) + 0.5 * sums[0]
+    high = jnp.where(core == 0, theirs, mine) + 0.5 * sums[1]
+    out[...] = jnp.concatenate([low, high], 0).astype(bf16)
 
 
 def exchange(x, axis):
@@ -272,6 +266,10 @@
 
 def swap(x):
     return lax.ppermute(x, "c", [(0, 1), (1, 0)])
+
+
+def swap_chips(x):
+    return lax.ppermute(x, "za", [(0, 1), (1, 0)])
 
 
 def together(*trees):
@@ -307,14 +305,15 @@
     position_decay_extra,
     lengths,
 ):
-    core, tp, z = lax.axis_index("c"), lax.axis_index("tp"), lax.axis_index("z")
-    plane, ring = lax.axis_size("tp"), lax.axis_size("z")
+    core, tp, z = lax.axis_index("c"), lax.axis_index("tp"), lax.axis_index(Z)
+    side = lax.axis_index("za")
+    plane, ring = lax.axis_size("tp"), lax.axis_size(Z)
     count, width = tokens.shape
     rows = count // 2
     features = 2 * ring * width
     hidden_units = first_gate_weight.shape[1]
     dk = query_weight_matrix.shape[1]
-    ids = jnp.stack([core, tp]).astype(jnp.int32)
+    ids = jnp.stack([core, tp, side, tp % 2]).astype(jnp.int32)
     head = jnp.concatenate([head_decay_speed, head_decay_offset])
 
     blocks = jnp.broadcast_to(tokens.reshape(2, 1, rows, width), (2, plane, rows, width))
@@ -384,7 +383,7 @@
         second_up_weight,
         second_down_weight,
     ) = later
-    parts = exchange(sent, "z")
+    parts = exchange(sent, Z)
     down_x = swap(first_down_weight)
     main = jnp.concatenate(
         [query_weight_matrix, key_weight_matrix, value_weight_matrix, output_gate_weight], 1
@@ -427,15 +426,25 @@
         hidden, (mixer_out_weight, second_gate_weight, second_up_weight, second_down_weight)
     )
     mixer_out_weight, second_gate_weight, second_up_weight, second_down_weight = later
-    hidden = exchange(hidden, "z")
+    hidden = exchange(hidden, Z)
     out_x, gate2_x = swap(mixer_out_weight), swap(second_gate_weight)
     up2_x, down2_x = swap(second_up_weight), swap(second_down_weight)
     hidden, out_x, gate2_x, up2_x, down2_x = together(hidden, out_x, gate2_x, up2_x, down2_x)
 
     parts = kernel(down, ((plane, rows, 2 * width), bf16), hidden, first_down_weight, down_x)
+    parts, gate2, up2, down2 = together(
+        parts, second_gate_weight, second_up_weight, second_down_weight
+    )
     parts = exchange(parts, "tp")
+    gate2_z = swap_chips(gate2)
+    up2_z = swap_chips(up2)
+    parts, gate2_z, up2_z = together(parts, gate2_z, up2_z)
     middle = kernel(add_first, ((plane, rows, 2 * width), bf16), ids, parts, got, scalars=1)
+    middle, down2, both_gains = together(middle, down2, jnp.stack([gains, gains_x]))
     middle = exchange(middle, "tp")
+    down2_z = swap_chips(down2)
+    gains_z = swap_chips(both_gains)
+    middle, down2_z, gains_z = together(middle, down2_z, gains_z)
 
     parts = kernel(
         project,
@@ -452,7 +461,10 @@
         wd_x,
         scalars=1,
     )
-    parts = exchange(parts, "z")
+    parts, gate2_z, up2_z, down2_z = together(parts, gate2_z, up2_z, down2_z)
+    parts = exchange(parts, Z)
+    gate2_zx, up2_zx, down2_zx = swap(gate2_z), swap(up2_z), swap(down2_z)
+    parts, gate2_zx, up2_zx, down2_zx = together(parts, gate2_zx, up2_zx, down2_zx)
     mixed = kernel(
         new_token,
         ((ring, rows, dk), bf16),
@@ -464,48 +476,62 @@
         scalars=1,
         features=features,
     )
-    mixed = exchange(mixed, "z")
+    mixed = exchange(mixed, Z)
     parts = kernel(down, ((plane, rows, 2 * width), bf16), mixed, mixer_out_weight, out_x)
     parts = exchange(parts, "tp")
-    second = kernel(add_mixer, ((2 * plane, rows, 2 * width), bf16), ids, parts, middle, scalars=1)
-    second = exchange(second, ("c", "tp")).reshape(2, plane, rows, 2 * width)
-
+    second, other = kernel(
+        add_mixer,
+        [((2 * plane, rows, 2 * width), bf16), ((rows, width), bf16)],
+        ids,
+        parts,
+        middle,
+        scalars=1,
+    )
+    second = exchange(second, ("za", "tp"))
+    other = swap(other)
+    second, other = together(second, other)
+    half = ring // 2
     sent = kernel(
         second_products,
-        ((ring, rows, 2 * hidden_units + LANES), bf16),
+        ((half, rows, 2 * hidden_units + LANES), bf16),
         ids,
-        second,
+        second.reshape(2, plane // 2, 2, rows, 2 * width),
         gains,
         gains_x,
-        second_gate_weight,
-        gate2_x,
-        second_up_weight,
-        up2_x,
-        scalars=1,
-    )
-    parts = exchange(sent, "z")
+        gains_z,
+        *(second_gate_weight, gate2_x, gate2_z, gate2_zx),
+        *(second_up_weight, up2_x, up2_z, up2_zx),
+        scalars=1,
+    )
+    parts = exchange(sent, "zh")
     hidden = kernel(
-        activate, ((ring, rows, hidden_units), bf16), parts, features=features
-    )
-    hidden = exchange(hidden, "z")
+        activate, ((half, rows, hidden_units), bf16), parts, features=features
+    )
+    hidden = exchange(hidden, "zh")
     parts = kernel(
         last_down,
-        ((2, plane, rows, width), bf16),
+        ((2, 2, plane // 2, 2, rows, width), bf16),
         ids,
         hidden,
-        second_down_weight,
-        down2_x,
-        scalars=1,
-    )
-    parts = exchange(parts.reshape(2 * plane, rows, width), ("c", "tp"))
-    parts = parts.reshape(2, plane, rows, width)
-    return kernel(finish, ((count, width), bf16), ids, parts, second, scalars=1)
+        *(second_down_weight, down2_x, down2_z, down2_zx),
+        scalars=1,
+    )
+    parts = exchange(parts.reshape(4 * plane, rows, width), ("za", "c", "tp"))
+    return kernel(
+        finish,
+        ((count, width), bf16),
+        ids,
+        parts.reshape(2, 2, plane, rows, width),
+        second.reshape(2, plane, rows, 2 * width),
+        other,
+        scalars=1,
+    )
 
 
 def solution(mesh):
     kv, tp = mesh.shape["kv"], mesh.shape["tp"]
-    split = Mesh(mesh.devices.reshape(kv // 2, 2, tp), ("z", "c", "tp"))
-    kv = ("z", "c")
+    split = Mesh(mesh.devices.reshape(kv // 4, 2, 2, tp), (*Z, "c", "tp"))
+    kv = (*Z, "c")
     return jax.shard_map(
         layer,
         mesh=split,

time: 233 us -> 240 us (1.030)
  blocking collectives: 142 us -> 85.1 us
  starting transfers between devices: 56.2 us -> 101 us
  waiting for transfers between devices: 12 us -> 27.7 us
  Pallas kernels: 15.6 us -> 18.2 us
    all_to_all x9 -> x5, blocking collectives: 142 us -> 85.1 us  [exchange(): return lax.all_to_all(x, axis, 0, 0, tiled=True)]
    all_to_all x3 -> x7, starting transfers between devices: 28.9 us -> 47.7 us  [exchange(): return lax.all_to_all(x, axis, 0, 0, tiled=True)]
    ppermute x9 -> x13, starting transfers between devices: 27.2 us -> 42 us  [swap(): return lax.ppermute(x, 'c', [(0, 1), (1, 0)])]
    ppermute x0 -> x4, starting transfers between devices: none -> 11.8 us  [swap_chips(): return lax.ppermute(x, 'za', [(0, 1), (1, 0)])]
    all_to_all x3 -> x7, waiting for transfers between devices: 10.8 us -> 22.3 us  [exchange(): return lax.all_to_all(x, axis, 0, 0, tiled=True)]
    pallas_call x13, Pallas kernels: 15.6 us -> 18.2 us  [kernel(): pl.pallas_call(functools.partial(fn, **static), out_shape=shapes, in_spec...]
    ppermute x0 -> x4, waiting for transfers between devices: none -> 2.43 us  [swap_chips(): return lax.ppermute(x, 'za', [(0, 1), (1, 0)])]
  transfers between devices with their start and end apart: 12 -> 24, of which waited for: 4 -> 11; matrix products, arithmetic and copies ran while one was open for 1% -> 1% of each run, Pallas kernels for 3% -> 3%
where the time goes in v4:
time: 240 us; the launch traced here: 239 us
  starting transfers between devices  101 us (42%)
  blocking collectives  85.1 us (35%)
  waiting for transfers between devices  27.7 us (12%)
  Pallas kernels  18.2 us (8%)
  local copies, waits for them, and re-layouts  3.72 us (2%)
    all_to_all x5, blocking collectives, exchange(): return lax.all_to_all(x, axis, 0, 0, tiled=True)  85.1 us
    all_to_all x7, starting transfers between devices, exchange(): return lax.all_to_all(x, axis, 0, 0, tiled=True)  47.7 us
    ppermute x13, starting transfers between devices, swap(): return lax.ppermute(x, 'c', [(0, 1), (1, 0)])  42 us
    all_to_all x7, waiting for transfers between devices, exchange(): return lax.all_to_all(x, axis, 0, 0, tiled=True)  22.3 us
    pallas_call x13, Pallas kernels, kernel(): pl.pallas_call(functools.partial(fn, **static), out_shape=shapes, in_spec...  18.2 us
    ppermute x4, starting transfers between devices, swap_chips(): return lax.ppermute(x, 'za', [(0, 1), (1, 0)])  11.8 us
  transfers between devices with their start and end apart: 24, of which 11 were waited for; matrix products, arithmetic and copies ran while one was open for 1% of the time, Pallas kernels for 3%

profile of v4, /device:TPU:1, one launch (start us, length us, event | category | flops | bytes accessed | tf_op | source)
XLA Modules:
  0.0 238.8 jit_solution(54061345355883331)
XLA Ops:
  0.0 8.9 %collective-permute-start.1 = (bf16[128,640]{1,0:T(8,128)(2,1)}, bf16[128,640]{1,0:T(8,128)(2,1)S(1)}, u32[]{:S(2)}, u32[]{:S(2)}) collective-permute-start(bf16[128,640]{1,0:T(8,128)(2,1)} %gate.1), channel_id=1, source_target_pairs={{0,16},{16,0},{1,17},{17,1},{2,18},{18,2},{3,19},{19,3},{4,20},{20... | collective-permute-start | bytes 491528 | tf_op jit(solution)/shard_map/ppermute | solution.py:268
  15.2 3.6 %all-to-all-start = ((bf16[32,8,128]{2,1,0:T(8,128)(2,1)}), bf16[32,8,128]{2,1,0:T(8,128)(2,1)S(1)}, u32[]{:S(2)}, u32[]{:S(2)}) async-start(bf16[32,8,128]{2,1,0:T(8,128)(2,1)} %bitcast.5), calls=%async_computation | async-start | bytes 131072 | tf_op jit(solution)/shard_map/all_to_all | solution.py:264
  19.0 7.0 %all-to-all-done = bf16[32,8,128]{2,1,0:T(8,128)(2,1)S(1)} async-done(((bf16[32,8,128]{2,1,0:T(8,128)(2,1)}), bf16[32,8,128]{2,1,0:T(8,128)(2,1)S(1)}, u32[]{:S(2)}, u32[]{:S(2)}) %all-to-all-start) | async-done | bytes 65568 | tf_op jit(solution)/shard_map/all_to_all | solution.py:264
  28.5 13.3 %all-to-all-start.1 = ((bf16[16,8,1408]{2,1,0:T(8,128)(2,1)}), bf16[16,8,1408]{2,1,0:T(8,128)(2,1)S(1)}, u32[]{:S(2)}, u32[]{:S(2)}) async-start(bf16[16,8,1408]{2,1,0:T(8,128)(2,1)} %shard_map.253), calls=%async_computation.1 | async-start | bytes 720896 | tf_op jit(solution)/shard_map/all_to_all | solution.py:264
  43.2 2.9 %collective-permute-start.3 = (bf16[640,128]{1,0:T(8,128)(2,1)S(1)}, bf16[640,128]{1,0:T(8,128)(2,1)S(1)}, u32[]{:S(2)}, u32[]{:S(2)}) collective-permute-start(bf16[640,128]{1,0:T(8,128)(2,1)S(1)} %copy-done.2), channel_id=1, source_target_pairs={{0,16},{16,0},{1,17},{17,1},{2,18},{18,2},{3,19},{19,3},{4,20},{20... | collective-permute-start | bytes 491528 | tf_op jit(solution)/shard_map/ppermute | solution.py:268
  48.9 6.4 %shard_map.254 = (f32[8,128,128]{2,1,0:T(8,128)S(1)}, f32[8,128]{1,0:T(8,128)S(1)}, f32[8,128]{1,0:T(8,128)S(1)}) custom-call(s32[8]{0:T(128)S(1)} %copy-done.13, f32[2]{0:T(128)S(1)} %pad_maximum_fusion.2.head, f32[8,128,128]{2,1,0:T(8,128)S(1)} %bitcast.37, bf16[8,64,128]{2,1,0:T(8,128)(2,1)S(1)} %copy-done.8, bf16[8,64,128]{2,1,0:T(8,128)(2,1)S(1)} %copy-done.9, ...), custom_call_target="tpu_custom_call" | custom-call | flops 268435456 | bytes 793128 | tf_op jit(solution)/shard_map/pallas_call | solution.py:24
  59.0 12.0 %all-to-all-start.2 = ((bf16[16,8,640]{2,1,0:T(8,128)(2,1)}), bf16[16,8,640]{2,1,0:T(8,128)(2,1)S(1)}, u32[]{:S(2)}, u32[]{:S(2)}) async-start(bf16[16,8,640]{2,1,0:T(8,128)(2,1)} %shard_map.255), calls=%async_computation.2 | async-start | bytes 327680 | tf_op jit(solution)/shard_map/all_to_all | solution.py:264
  71.0 3.0 %collective-permute-start.6 = (bf16[128,640]{1,0:T(8,128)(2,1)S(1)}, bf16[128,640]{1,0:T(8,128)(2,1)S(1)}, u32[]{:S(2)}, u32[]{:S(2)}) collective-permute-start(bf16[128,640]{1,0:T(8,128)(2,1)S(1)} %copy-done), channel_id=1, source_target_pairs={{0,16},{16,0},{1,17},{17,1},{2,18},{18,2},{3,19},{19,3},{4,20},{20... | collective-permute-start | bytes 491528 | tf_op jit(solution)/shard_map/ppermute | solution.py:268
  76.0 2.4 %collective-permute-start.8 = (bf16[640,128]{1,0:T(8,128)(2,1)S(1)}, bf16[640,128]{1,0:T(8,128)(2,1)S(1)}, u32[]{:S(2)}, u32[]{:S(2)}) collective-permute-start(bf16[640,128]{1,0:T(8,128)(2,1)S(1)} %copy-done.3), channel_id=1, source_target_pairs={{0,16},{16,0},{1,17},{17,1},{2,18},{18,2},{3,19},{19,3},{4,20},{20... | collective-permute-start | bytes 491528 | tf_op jit(solution)/shard_map/ppermute | solution.py:268
  84.0 4.6 %collective-permute-start.9 = (bf16[128,640]{1,0:T(8,128)(2,1)S(1)}, bf16[128,640]{1,0:T(8,128)(2,1)S(1)}, u32[]{:S(2)}, u32[]{:S(2)}) collective-permute-start(bf16[128,640]{1,0:T(8,128)(2,1)S(1)} %copy-done), channel_id=1, source_target_pairs={{0,32},{32,0},{1,33},{33,1},{2,34},{34,2},{3,35},{35,3},{4,36},{36... | collective-permute-start | bytes 491528 | tf_op jit(solution)/shard_map/ppermute | solution.py:272
  90.5 4.4 %all-to-all-start.3 = ((bf16[16,8,256]{2,1,0:T(8,128)(2,1)}), bf16[16,8,256]{2,1,0:T(8,128)(2,1)S(1)}, u32[]{:S(2)}, u32[]{:S(2)}) async-start(bf16[16,8,256]{2,1,0:T(8,128)(2,1)} %shard_map.256), calls=%async_computation.3 | async-start | bytes 131072 | tf_op jit(solution)/shard_map/all_to_all | solution.py:264
  95.0 6.5 %all-to-all-done.3.parts = bf16[16,8,256]{2,1,0:T(8,128)(2,1)S(1)} async-done(((bf16[16,8,256]{2,1,0:T(8,128)(2,1)}), bf16[16,8,256]{2,1,0:T(8,128)(2,1)S(1)}, u32[]{:S(2)}, u32[]{:S(2)}) %all-to-all-start.3) | async-done | bytes 65568 | tf_op jit(solution)/shard_map/all_to_all | solution.py:264
  102.7 3.4 %collective-permute-start.11 = (bf16[640,128]{1,0:T(8,128)(2,1)S(1)}, bf16[640,128]{1,0:T(8,128)(2,1)S(1)}, u32[]{:S(2)}, u32[]{:S(2)}) collective-permute-start(bf16[640,128]{1,0:T(8,128)(2,1)S(1)} %copy-done.3), channel_id=1, source_target_pairs={{0,32},{32,0},{1,33},{33,1},{2,34},{34,2},{3,35},{35,3},{4,36},{36... | collective-permute-start | bytes 491528 | tf_op jit(solution)/shard_map/ppermute | solution.py:272
  106.1 3.5 %all-to-all-start.4 = ((bf16[16,8,256]{2,1,0:T(8,128)(2,1)}), bf16[16,8,256]{2,1,0:T(8,128)(2,1)S(1)}, u32[]{:S(2)}, u32[]{:S(2)}) async-start(bf16[16,8,256]{2,1,0:T(8,128)(2,1)} %shard_map.257), calls=%async_computation.4 | async-start | bytes 131072 | tf_op jit(solution)/shard_map/all_to_all | solution.py:264
  111.5 2.4 %collective-permute-done.12.gains_z = f32[2,3,128]{2,1,0:T(4,128)S(1)} collective-permute-done((f32[2,3,128]{2,1,0:T(4,128)S(1)}, f32[2,3,128]{2,1,0:T(4,128)S(1)}, u32[]{:S(2)}, u32[]{:S(2)}) %collective-permute-start.12) | collective-permute-done | bytes 3104 | tf_op jit(solution)/shard_map/ppermute | solution.py:272
  117.6 6.7 %all-to-all-start.5 = ((bf16[16,8,640]{2,1,0:T(8,128)(2,1)}), bf16[16,8,640]{2,1,0:T(8,128)(2,1)S(1)}, u32[]{:S(2)}, u32[]{:S(2)}) async-start(bf16[16,8,640]{2,1,0:T(8,128)(2,1)} %shard_map.258), calls=%async_computation.5 | async-start | bytes 327680 | tf_op jit(solution)/shard_map/all_to_all | solution.py:264
  124.3 5.5 %collective-permute-start.13 = (bf16[128,640]{1,0:T(8,128)(2,1)S(1)}, bf16[128,640]{1,0:T(8,128)(2,1)S(1)}, u32[]{:S(2)}, u32[]{:S(2)}) collective-permute-start(bf16[128,640]{1,0:T(8,128)(2,1)S(1)} %collective-permute-done.9.refs_2_), channel_id=1, source_target_pairs={{0,16},{16,0},{1,17},{17,1},{2,18},{18,2},{3,19},{19,3},{4,20},{20... | collective-permute-start | bytes 491528 | tf_op jit(solution)/shard_map/ppermute | solution.py:268
  137.8 21.8 %all_to_all.60.hidden = bf16[16,8,128]{2,1,0:T(8,128)(2,1)S(1)} all-to-all(bf16[16,8,128]{2,1,0:T(8,128)(2,1)S(1)} %shard_map.259), channel_id=1, replica_groups=mesh['zh'=8,'za'=2,'c'=2,'tp'=16] {'zh','za'}, dimensions={0} | all-to-all | bytes 65536 | tf_op jit(solution)/shard_map/all_to_all | solution.py:264
  159.7 11.1 %all_to_all.61.parts = bf16[16,8,256]{2,1,0:T(8,128)(2,1)S(1)} all-to-all(bf16[16,8,256]{2,1,0:T(8,128)(2,1)S(1)} %shard_map.260), channel_id=1, replica_groups=mesh['zh'=8,'za'=2,'c'=2,'tp'=16] {'tp'}, dimensions={0} | all-to-all | bytes 131072 | tf_op jit(solution)/shard_map/all_to_all | solution.py:264
  172.0 4.1 %all-to-all-start.8 = ((bf16[32,8,256]{2,1,0:T(8,128)(2,1)}), bf16[32,8,256]{2,1,0:T(8,128)(2,1)S(1)}, u32[]{:S(2)}, u32[]{:S(2)}) async-start(bf16[32,8,256]{2,1,0:T(8,128)(2,1)} %get-tuple-element.132), calls=%async_computation.8 | async-start | bytes 262144 | tf_op jit(solution)/shard_map/all_to_all | solution.py:264
  176.1 4.9 %collective-permute-start.16 = (bf16[8,128]{1,0:T(8,128)(2,1)S(1)}, bf16[8,128]{1,0:T(8,128)(2,1)S(1)}, u32[]{:S(2)}, u32[]{:S(2)}) collective-permute-start(bf16[8,128]{1,0:T(8,128)(2,1)S(1)} %get-tuple-element.133), channel_id=1, source_target_pairs={{0,16},{16,0},{1,17},{17,1},{2,18},{18,2},{3,19},{19,3},{4,20},{20... | collective-permute-start | bytes 6152 | tf_op jit(solution)/shard_map/ppermute | solution.py:268
  184.4 16.7 %all_to_all.62.parts = bf16[8,8,1408]{2,1,0:T(8,128)(2,1)S(1)} all-to-all(bf16[8,8,1408]{2,1,0:T(8,128)(2,1)S(1)} %shard_map.262), channel_id=1, replica_groups=mesh['zh'=8,'za'=2,'c'=2,'tp'=16] {'zh'}, dimensions={0} | all-to-all | bytes 360448 | tf_op jit(solution)/shard_map/all_to_all | solution.py:264
  201.2 14.9 %all_to_all.63.hidden = bf16[8,8,640]{2,1,0:T(8,128)(2,1)S(1)} all-to-all(bf16[8,8,640]{2,1,0:T(8,128)(2,1)S(1)} %shard_map.263), channel_id=1, replica_groups=mesh['zh'=8,'za'=2,'c'=2,'tp'=16] {'zh'}, dimensions={0} | all-to-all | bytes 163840 | tf_op jit(solution)/shard_map/all_to_all | solution.py:264
  217.0 20.6 %all_to_all.64 = bf16[64,8,128]{2,1,0:T(8,128)(2,1)S(1)} all-to-all(bf16[64,8,128]{2,1,0:T(8,128)(2,1)S(1)} %bitcast.35), channel_id=1, replica_groups=mesh['zh'=8,'za'=2,'c'=2,'tp'=16] {'za','c','tp'}, dimensions={0} | all-to-all | bytes 262144 | tf_op jit(solution)/shard_map/all_to_all | solution.py:264
  (90 shorter events, 46.4 us)
Async XLA Ops:
  0.0 25.9 %collective-permute-start.1 = (bf16[128,640]{1,0:T(8,128)(2,1)}, bf16[128,640]{1,0:T(8,128)(2,1)S(1)}, u32[]{:S(2)}, u32[]{:S(2)}) collective-permute-start(bf16[128,640]{1,0:T(8,128)(2,1)} %gate.1), channel_id=1, source_target_pairs={{0,16},{16,0},{1,17},{17,1},{2,18},{18,2},{3,19},{19,3},{4,20},{20... | collective-permute-start | bytes 491528 | tf_op jit(solution)/shard_map/ppermute | solution.py:268
  8.9 17.1 %collective-permute-start.2 = (bf16[128,640]{1,0:T(8,128)(2,1)}, bf16[128,640]{1,0:T(8,128)(2,1)S(1)}, u32[]{:S(2)}, u32[]{:S(2)}) collective-permute-start(bf16[128,640]{1,0:T(8,128)(2,1)} %up.1), channel_id=1, source_target_pairs={{0,16},{16,0},{1,17},{17,1},{2,18},{18,2},{3,19},{19,3},{4,20},{20... | collective-permute-start | bytes 491528 | tf_op jit(solution)/shard_map/ppermute | solution.py:268
  11.5 7.5 %collective-permute-start = (f32[3,128]{1,0:T(4,128)S(1)}, f32[3,128]{1,0:T(4,128)S(1)}, u32[]{:S(2)}, u32[]{:S(2)}) collective-permute-start(f32[3,128]{1,0:T(4,128)S(1)} %get-tuple-element.148.gains), channel_id=1, source_target_pairs={{0,16},{16,0},{1,17},{17,1},{2,18},{18,2},{3,19},{19,3},{4,20},{20... | collective-permute-start | bytes 4616 | tf_op jit(solution)/shard_map/ppermute | solution.py:268
  15.2 10.7 %all-to-all-start = ((bf16[32,8,128]{2,1,0:T(8,128)(2,1)}), bf16[32,8,128]{2,1,0:T(8,128)(2,1)S(1)}, u32[]{:S(2)}, u32[]{:S(2)}) async-start(bf16[32,8,128]{2,1,0:T(8,128)(2,1)} %bitcast.5), calls=%async_computation | async-start | bytes 131072 | tf_op jit(solution)/shard_map/all_to_all | solution.py:264
  28.5 29.7 %all-to-all-start.1 = ((bf16[16,8,1408]{2,1,0:T(8,128)(2,1)}), bf16[16,8,1408]{2,1,0:T(8,128)(2,1)S(1)}, u32[]{:S(2)}, u32[]{:S(2)}) async-start(bf16[16,8,1408]{2,1,0:T(8,128)(2,1)} %shard_map.253), calls=%async_computation.1 | async-start | bytes 720896 | tf_op jit(solution)/shard_map/all_to_all | solution.py:264
  43.2 12.8 %collective-permute-start.3 = (bf16[640,128]{1,0:T(8,128)(2,1)S(1)}, bf16[640,128]{1,0:T(8,128)(2,1)S(1)}, u32[]{:S(2)}, u32[]{:S(2)}) collective-permute-start(bf16[640,128]{1,0:T(8,128)(2,1)S(1)} %copy-done.2), channel_id=1, source_target_pairs={{0,16},{16,0},{1,17},{17,1},{2,18},{18,2},{3,19},{19,3},{4,20},{20... | collective-permute-start | bytes 491528 | tf_op jit(solution)/shard_map/ppermute | solution.py:268
  46.2 9.8 %collective-permute-start.4 = (bf16[128,512]{1,0:T(8,128)(2,1)S(1)}, bf16[128,512]{1,0:T(8,128)(2,1)S(1)}, u32[]{:S(2)}, u32[]{:S(2)}) collective-permute-start(bf16[128,512]{1,0:T(8,128)(2,1)S(1)} %constant_dynamic-update-slice_fusion.main), channel_id=1, source_target_pairs={{0,16},{16,0},{1,17},{17,1},{2,18},{18,2},{3,19},{19,3},{4,20},{20... | collective-permute-start | bytes 393224 | tf_op jit(solution)/shard_map/ppermute | solution.py:268
  59.0 24.1 %all-to-all-start.2 = ((bf16[16,8,640]{2,1,0:T(8,128)(2,1)}), bf16[16,8,640]{2,1,0:T(8,128)(2,1)S(1)}, u32[]{:S(2)}, u32[]{:S(2)}) async-start(bf16[16,8,640]{2,1,0:T(8,128)(2,1)} %shard_map.255), calls=%async_computation.2 | async-start | bytes 327680 | tf_op jit(solution)/shard_map/all_to_all | solution.py:264
  71.0 10.5 %collective-permute-start.6 = (bf16[128,640]{1,0:T(8,128)(2,1)S(1)}, bf16[128,640]{1,0:T(8,128)(2,1)S(1)}, u32[]{:S(2)}, u32[]{:S(2)}) collective-permute-start(bf16[128,640]{1,0:T(8,128)(2,1)S(1)} %copy-done), channel_id=1, source_target_pairs={{0,16},{16,0},{1,17},{17,1},{2,18},{18,2},{3,19},{19,3},{4,20},{20... | collective-permute-start | bytes 491528 | tf_op jit(solution)/shard_map/ppermute | solution.py:268
  74.0 7.5 %collective-permute-start.7 = (bf16[128,640]{1,0:T(8,128)(2,1)S(1)}, bf16[128,640]{1,0:T(8,128)(2,1)S(1)}, u32[]{:S(2)}, u32[]{:S(2)}) collective-permute-start(bf16[128,640]{1,0:T(8,128)(2,1)S(1)} %copy-done.1), channel_id=1, source_target_pairs={{0,16},{16,0},{1,17},{17,1},{2,18},{18,2},{3,19},{19,3},{4,20},{20... | collective-permute-start | bytes 491528 | tf_op jit(solution)/shard_map/ppermute | solution.py:268
  76.0 5.5 %collective-permute-start.8 = (bf16[640,128]{1,0:T(8,128)(2,1)S(1)}, bf16[640,128]{1,0:T(8,128)(2,1)S(1)}, u32[]{:S(2)}, u32[]{:S(2)}) collective-permute-start(bf16[640,128]{1,0:T(8,128)(2,1)S(1)} %copy-done.3), channel_id=1, source_target_pairs={{0,16},{16,0},{1,17},{17,1},{2,18},{18,2},{3,19},{19,3},{4,20},{20... | collective-permute-start | bytes 491528 | tf_op jit(solution)/shard_map/ppermute | solution.py:268
  78.4 3.1 %collective-permute-start.5 = (bf16[128,128]{1,0:T(8,128)(2,1)S(1)}, bf16[128,128]{1,0:T(8,128)(2,1)S(1)}, u32[]{:S(2)}, u32[]{:S(2)}) collective-permute-start(bf16[128,128]{1,0:T(8,128)(2,1)S(1)} %copy-done.6), channel_id=1, source_target_pairs={{0,16},{16,0},{1,17},{17,1},{2,18},{18,2},{3,19},{19,3},{4,20},{20... | collective-permute-start | bytes 98312 | tf_op jit(solution)/shard_map/ppermute | solution.py:268
  84.0 17.5 %collective-permute-start.9 = (bf16[128,640]{1,0:T(8,128)(2,1)S(1)}, bf16[128,640]{1,0:T(8,128)(2,1)S(1)}, u32[]{:S(2)}, u32[]{:S(2)}) collective-permute-start(bf16[128,640]{1,0:T(8,128)(2,1)S(1)} %copy-done), channel_id=1, source_target_pairs={{0,32},{32,0},{1,33},{33,1},{2,34},{34,2},{3,35},{35,3},{4,36},{36... | collective-permute-start | bytes 491528 | tf_op jit(solution)/shard_map/ppermute | solution.py:272
  88.6 12.9 %collective-permute-start.10 = (bf16[128,640]{1,0:T(8,128)(2,1)S(1)}, bf16[128,640]{1,0:T(8,128)(2,1)S(1)}, u32[]{:S(2)}, u32[]{:S(2)}) collective-permute-start(bf16[128,640]{1,0:T(8,128)(2,1)S(1)} %copy-done.1), channel_id=1, source_target_pairs={{0,32},{32,0},{1,33},{33,1},{2,34},{34,2},{3,35},{35,3},{4,36},{36... | collective-permute-start | bytes 491528 | tf_op jit(solution)/shard_map/ppermute | solution.py:272
  90.5 11.0 %all-to-all-start.3 = ((bf16[16,8,256]{2,1,0:T(8,128)(2,1)}), bf16[16,8,256]{2,1,0:T(8,128)(2,1)S(1)}, u32[]{:S(2)}, u32[]{:S(2)}) async-start(bf16[16,8,256]{2,1,0:T(8,128)(2,1)} %shard_map.256), calls=%async_computation.3 | async-start | bytes 131072 | tf_op jit(solution)/shard_map/all_to_all | solution.py:264
  102.7 13.3 %collective-permute-start.11 = (bf16[640,128]{1,0:T(8,128)(2,1)S(1)}, bf16[640,128]{1,0:T(8,128)(2,1)S(1)}, u32[]{:S(2)}, u32[]{:S(2)}) collective-permute-start(bf16[640,128]{1,0:T(8,128)(2,1)S(1)} %copy-done.3), channel_id=1, source_target_pairs={{0,32},{32,0},{1,33},{33,1},{2,34},{34,2},{3,35},{35,3},{4,36},{36... | collective-permute-start | bytes 491528 | tf_op jit(solution)/shard_map/ppermute | solution.py:272
  106.1 10.0 %all-to-all-start.4 = ((bf16[16,8,256]{2,1,0:T(8,128)(2,1)}), bf16[16,8,256]{2,1,0:T(8,128)(2,1)S(1)}, u32[]{:S(2)}, u32[]{:S(2)}) async-start(bf16[16,8,256]{2,1,0:T(8,128)(2,1)} %shard_map.257), calls=%async_computation.4 | async-start | bytes 131072 | tf_op jit(solution)/shard_map/all_to_all | solution.py:264
  109.6 4.4 %collective-permute-start.12 = (f32[2,3,128]{2,1,0:T(4,128)S(1)}, f32[2,3,128]{2,1,0:T(4,128)S(1)}, u32[]{:S(2)}, u32[]{:S(2)}) collective-permute-start(f32[2,3,128]{2,1,0:T(4,128)S(1)} %pad_maximum_fusion), channel_id=1, source_target_pairs={{0,32},{32,0},{1,33},{33,1},{2,34},{34,2},{3,35},{35,3},{4,36},{36... | collective-permute-start | bytes 9224 | tf_op jit(solution)/shard_map/ppermute | solution.py:272
  117.6 18.8 %all-to-all-start.5 = ((bf16[16,8,640]{2,1,0:T(8,128)(2,1)}), bf16[16,8,640]{2,1,0:T(8,128)(2,1)S(1)}, u32[]{:S(2)}, u32[]{:S(2)}) async-start(bf16[16,8,640]{2,1,0:T(8,128)(2,1)} %shard_map.258), calls=%async_computation.5 | async-start | bytes 327680 | tf_op jit(solution)/shard_map/all_to_all | solution.py:264
  124.3 9.9 %collective-permute-start.13 = (bf16[128,640]{1,0:T(8,128)(2,1)S(1)}, bf16[128,640]{1,0:T(8,128)(2,1)S(1)}, u32[]{:S(2)}, u32[]{:S(2)}) collective-permute-start(bf16[128,640]{1,0:T(8,128)(2,1)S(1)} %collective-permute-done.9.refs_2_), channel_id=1, source_target_pairs={{0,16},{16,0},{1,17},{17,1},{2,18},{18,2},{3,19},{19,3},{4,20},{20... | collective-permute-start | bytes 491528 | tf_op jit(solution)/shard_map/ppermute | solution.py:268
  129.8 4.4 %collective-permute-start.14 = (bf16[128,640]{1,0:T(8,128)(2,1)S(1)}, bf16[128,640]{1,0:T(8,128)(2,1)S(1)}, u32[]{:S(2)}, u32[]{:S(2)}) collective-permute-start(bf16[128,640]{1,0:T(8,128)(2,1)S(1)} %collective-permute-done.10.refs_6_), channel_id=1, source_target_pairs={{0,16},{16,0},{1,17},{17,1},{2,18},{18,2},{3,19},{19,3},{4,20},{20... | collective-permute-start | bytes 491528 | tf_op jit(solution)/shard_map/ppermute | solution.py:268
  131.8 3.4 %collective-permute-start.15 = (bf16[640,128]{1,0:T(8,128)(2,1)S(1)}, bf16[640,128]{1,0:T(8,128)(2,1)S(1)}, u32[]{:S(2)}, u32[]{:S(2)}) collective-permute-start(bf16[640,128]{1,0:T(8,128)(2,1)S(1)} %collective-permute-done.11.refs_2_), channel_id=1, source_target_pairs={{0,16},{16,0},{1,17},{17,1},{2,18},{18,2},{3,19},{19,3},{4,20},{20... | collective-permute-start | bytes 491528 | tf_op jit(solution)/shard_map/ppermute | solution.py:268
  172.0 11.4 %all-to-all-start.8 = ((bf16[32,8,256]{2,1,0:T(8,128)(2,1)}), bf16[32,8,256]{2,1,0:T(8,128)(2,1)S(1)}, u32[]{:S(2)}, u32[]{:S(2)}) async-start(bf16[32,8,256]{2,1,0:T(8,128)(2,1)} %get-tuple-element.132), calls=%async_computation.8 | async-start | bytes 262144 | tf_op jit(solution)/shard_map/all_to_all | solution.py:264
  176.1 5.7 %collective-permute-start.16 = (bf16[8,128]{1,0:T(8,128)(2,1)S(1)}, bf16[8,128]{1,0:T(8,128)(2,1)S(1)}, u32[]{:S(2)}, u32[]{:S(2)}) collective-permute-start(bf16[8,128]{1,0:T(8,128)(2,1)S(1)} %get-tuple-element.133), channel_id=1, source_target_pairs={{0,16},{16,0},{1,17},{17,1},{2,18},{18,2},{3,19},{19,3},{4,20},{20... | collective-permute-start | bytes 6152 | tf_op jit(solution)/shard_map/ppermute | solution.py:268
  (19 other events, 206.3 us)

commit v5 on v4

--- a/solution.py
+++ b/solution.py
@@ -338,6 +338,7 @@
         scalars=1,
     )
 
+    both_gains = jnp.stack([gains, gains_x])
     sent, later = together(
         sent,
         (
@@ -415,8 +416,27 @@
         scalars=2,
         flops=1 << 28,
     )
-    parts, down_x, main, main_x, ws, ws_x, wd, wd_x, state, new_extra, norm_gain = together(
-        parts, down_x, main, main_x, ws, ws_x, wd, wd_x, state, new_extra, norm_gain
+    state, gate2, up2, down2 = together(
+        state, second_gate_weight, second_up_weight, second_down_weight
+    )
+    gate2_z = swap_chips(gate2)
+    up2_z = swap_chips(up2)
+    down2_z = swap_chips(down2)
+    parts, down_x, main, main_x, ws, ws_x, wd, wd_x, state, new_extra, norm_gain, both_gains = (
+        together(
+            parts,
+            down_x,
+            main,
+            main_x,
+            ws,
+            ws_x,
+            wd,
+            wd_x,
+            state,
+            new_extra,
+            norm_gain,
+            both_gains,
+        )
     )
 
     hidden = kernel(
@@ -429,22 +449,14 @@
     hidden = exchange(hidden, Z)
     out_x, gate2_x = swap(mixer_out_weight), swap(second_gate_weight)
     up2_x, down2_x = swap(second_up_weight), swap(second_down_weight)
-    hidden, out_x, gate2_x, up2_x, down2_x = together(hidden, out_x, gate2_x, up2_x, down2_x)
+    hidden, out_x, gate2_x, up2_x, down2_x, gate2_z, up2_z, down2_z = together(
+        hidden, out_x, gate2_x, up2_x, down2_x, gate2_z, up2_z, down2_z
+    )
 
     parts = kernel(down, ((plane, rows, 2 * width), bf16), hidden, first_down_weight, down_x)
-    parts, gate2, up2, down2 = together(
-        parts, second_gate_weight, second_up_weight, second_down_weight
-    )
     parts = exchange(parts, "tp")
-    gate2_z = swap_chips(gate2)
-    up2_z = swap_chips(up2)
-    parts, gate2_z, up2_z = together(parts, gate2_z, up2_z)
     middle = kernel(add_first, ((plane, rows, 2 * width), bf16), ids, parts, got, scalars=1)
-    middle, down2, both_gains = together(middle, down2, jnp.stack([gains, gains_x]))
     middle = exchange(middle, "tp")
-    down2_z = swap_chips(down2)
-    gains_z = swap_chips(both_gains)
-    middle, down2_z, gains_z = together(middle, down2_z, gains_z)
 
     parts = kernel(
         project,
@@ -461,10 +473,15 @@
         wd_x,
         scalars=1,
     )
-    parts, gate2_z, up2_z, down2_z = together(parts, gate2_z, up2_z, down2_z)
+    parts, gate2_z, up2_z, down2_z, both_gains = together(
+        parts, gate2_z, up2_z, down2_z, both_gains
+    )
     parts = exchange(parts, Z)
     gate2_zx, up2_zx, down2_zx = swap(gate2_z), swap(up2_z), swap(down2_z)
-    parts, gate2_zx, up2_zx, down2_zx = together(parts, gate2_zx, up2_zx, down2_zx)
+    gains_z = swap_chips(both_gains)
+    parts, gate2_zx, up2_zx, down2_zx, gains_z = together(
+        parts, gate2_zx, up2_zx, down2_zx, gains_z
+    )
     mixed = kernel(
         new_token,
         ((ring, rows, dk), bf16),

time: 240 us -> 242 us (level)
  blocking collectives: 85.1 us -> 105 us
  waiting for transfers between devices: 27.7 us -> 12.8 us
    all_to_all x5 -> x7, blocking collectives: 85.1 us -> 105 us  [exchange(): return lax.all_to_all(x, axis, 0, 0, tiled=True)]
    all_to_all x7 -> x5, waiting for transfers between devices: 22.3 us -> 9.85 us  [exchange(): return lax.all_to_all(x, axis, 0, 0, tiled=True)]
    all_to_all x7 -> x5, starting transfers between devices: 47.7 us -> 43.1 us  [exchange(): return lax.all_to_all(x, axis, 0, 0, tiled=True)]
    ppermute x13, starting transfers between devices: 42 us -> 44.4 us  [swap(): return lax.ppermute(x, 'c', [(0, 1), (1, 0)])]
  transfers between devices with their start and end apart: 24 -> 22, of which waited for: 11 -> 6; matrix products, arithmetic and copies ran while one was open for 1% -> 1% of each run, Pallas kernels for 3% -> 3%
where the time goes in v5:
time: 242 us; the launch traced here: 240 us
  blocking collectives  105 us (43%)
  starting transfers between devices  99.5 us (41%)
  Pallas kernels  16.9 us (7%)
  waiting for transfers between devices  12.8 us (5%)
  local copies, waits for them, and re-layouts  3.72 us (2%)
    all_to_all x7, blocking collectives, exchange(): return lax.all_to_all(x, axis, 0, 0, tiled=True)  105 us
    ppermute x13, starting transfers between devices, swap(): return lax.ppermute(x, 'c', [(0, 1), (1, 0)])  44.4 us
    all_to_all x5, starting transfers between devices, exchange(): return lax.all_to_all(x, axis, 0, 0, tiled=True)  43.1 us
    pallas_call x13, Pallas kernels, kernel(): pl.pallas_call(functools.partial(fn, **static), out_shape=shapes, in_spec...  16.9 us
    ppermute x4, starting transfers between devices, swap_chips(): return lax.ppermute(x, 'za', [(0, 1), (1, 0)])  12.1 us
    all_to_all x5, waiting for transfers between devices, exchange(): return lax.all_to_all(x, axis, 0, 0, tiled=True)  9.85 us
  transfers between devices with their start and end apart: 22, of which 6 were waited for; matrix products, arithmetic and copies ran while one was open for 1% of the time, Pallas kernels for 3%

profile of v5, /device:TPU:1, one launch (start us, length us, event | category | flops | bytes accessed | tf_op | source)
XLA Modules:
  0.0 240.2 jit_solution(16289496547688790770)
XLA Ops:
  0.0 8.9 %collective-permute-start.1 = (bf16[128,640]{1,0:T(8,128)(2,1)}, bf16[128,640]{1,0:T(8,128)(2,1)S(1)}, u32[]{:S(2)}, u32[]{:S(2)}) collective-permute-start(bf16[128,640]{1,0:T(8,128)(2,1)} %gate.1), channel_id=1, source_target_pairs={{0,16},{16,0},{1,17},{17,1},{2,18},{18,2},{3,19},{19,3},{4,20},{20... | collective-permute-start | bytes 491528 | tf_op jit(solution)/shard_map/ppermute | solution.py:268
  15.2 3.6 %all-to-all-start = ((bf16[32,8,128]{2,1,0:T(8,128)(2,1)}), bf16[32,8,128]{2,1,0:T(8,128)(2,1)S(1)}, u32[]{:S(2)}, u32[]{:S(2)}) async-start(bf16[32,8,128]{2,1,0:T(8,128)(2,1)} %bitcast.5), calls=%async_computation | async-start | bytes 131072 | tf_op jit(solution)/shard_map/all_to_all | solution.py:264
  18.9 7.0 %all-to-all-done = bf16[32,8,128]{2,1,0:T(8,128)(2,1)S(1)} async-done(((bf16[32,8,128]{2,1,0:T(8,128)(2,1)}), bf16[32,8,128]{2,1,0:T(8,128)(2,1)S(1)}, u32[]{:S(2)}, u32[]{:S(2)}) %all-to-all-start) | async-done | bytes 65568 | tf_op jit(solution)/shard_map/all_to_all | solution.py:264
  28.4 13.3 %all-to-all-start.1 = ((bf16[16,8,1408]{2,1,0:T(8,128)(2,1)}), bf16[16,8,1408]{2,1,0:T(8,128)(2,1)S(1)}, u32[]{:S(2)}, u32[]{:S(2)}) async-start(bf16[16,8,1408]{2,1,0:T(8,128)(2,1)} %shard_map.253), calls=%async_computation.1 | async-start | bytes 720896 | tf_op jit(solution)/shard_map/all_to_all | solution.py:264
  43.2 2.9 %collective-permute-start.3 = (bf16[640,128]{1,0:T(8,128)(2,1)S(1)}, bf16[640,128]{1,0:T(8,128)(2,1)S(1)}, u32[]{:S(2)}, u32[]{:S(2)}) collective-permute-start(bf16[640,128]{1,0:T(8,128)(2,1)S(1)} %copy-done.2), channel_id=1, source_target_pairs={{0,16},{16,0},{1,17},{17,1},{2,18},{18,2},{3,19},{19,3},{4,20},{20... | collective-permute-start | bytes 491528 | tf_op jit(solution)/shard_map/ppermute | solution.py:268
  48.9 6.4 %shard_map.254 = (f32[8,128,128]{2,1,0:T(8,128)S(1)}, f32[8,128]{1,0:T(8,128)S(1)}, f32[8,128]{1,0:T(8,128)S(1)}) custom-call(s32[8]{0:T(128)S(1)} %copy-done.13, f32[2]{0:T(128)S(1)} %pad_maximum_fusion.2.head, f32[8,128,128]{2,1,0:T(8,128)S(1)} %bitcast.37, bf16[8,64,128]{2,1,0:T(8,128)(2,1)S(1)} %copy-done.8, bf16[8,64,128]{2,1,0:T(8,128)(2,1)S(1)} %copy-done.9, ...), custom_call_target="tpu_custom_call" | custom-call | flops 268435456 | bytes 793128 | tf_op jit(solution)/shard_map/pallas_call | solution.py:24
  59.0 12.0 %all-to-all-start.2 = ((bf16[16,8,640]{2,1,0:T(8,128)(2,1)}), bf16[16,8,640]{2,1,0:T(8,128)(2,1)S(1)}, u32[]{:S(2)}, u32[]{:S(2)}) async-start(bf16[16,8,640]{2,1,0:T(8,128)(2,1)} %shard_map.255), calls=%async_computation.2 | async-start | bytes 327680 | tf_op jit(solution)/shard_map/all_to_all | solution.py:264
  71.1 3.3 %collective-permute-start.9 = (bf16[128,640]{1,0:T(8,128)(2,1)S(1)}, bf16[128,640]{1,0:T(8,128)(2,1)S(1)}, u32[]{:S(2)}, u32[]{:S(2)}) collective-permute-start(bf16[128,640]{1,0:T(8,128)(2,1)S(1)} %copy-done), channel_id=1, source_target_pairs={{0,32},{32,0},{1,33},{33,1},{2,34},{34,2},{3,35},{35,3},{4,36},{36... | collective-permute-start | bytes 491528 | tf_op jit(solution)/shard_map/ppermute | solution.py:272
  76.4 3.3 %collective-permute-start.11 = (bf16[640,128]{1,0:T(8,128)(2,1)S(1)}, bf16[640,128]{1,0:T(8,128)(2,1)S(1)}, u32[]{:S(2)}, u32[]{:S(2)}) collective-permute-start(bf16[640,128]{1,0:T(8,128)(2,1)S(1)} %copy-done.3), channel_id=1, source_target_pairs={{0,32},{32,0},{1,33},{33,1},{2,34},{34,2},{3,35},{35,3},{4,36},{36... | collective-permute-start | bytes 491528 | tf_op jit(solution)/shard_map/ppermute | solution.py:272
  79.7 4.1 %collective-permute-start.6 = (bf16[128,640]{1,0:T(8,128)(2,1)S(1)}, bf16[128,640]{1,0:T(8,128)(2,1)S(1)}, u32[]{:S(2)}, u32[]{:S(2)}) collective-permute-start(bf16[128,640]{1,0:T(8,128)(2,1)S(1)} %copy-done), channel_id=1, source_target_pairs={{0,16},{16,0},{1,17},{17,1},{2,18},{18,2},{3,19},{19,3},{4,20},{20... | collective-permute-start | bytes 491528 | tf_op jit(solution)/shard_map/ppermute | solution.py:268
  85.7 2.4 %collective-permute-start.8 = (bf16[640,128]{1,0:T(8,128)(2,1)S(1)}, bf16[640,128]{1,0:T(8,128)(2,1)S(1)}, u32[]{:S(2)}, u32[]{:S(2)}) collective-permute-start(bf16[640,128]{1,0:T(8,128)(2,1)S(1)} %copy-done.3), channel_id=1, source_target_pairs={{0,16},{16,0},{1,17},{17,1},{2,18},{18,2},{3,19},{19,3},{4,20},{20... | collective-permute-start | bytes 491528 | tf_op jit(solution)/shard_map/ppermute | solution.py:268
  88.1 2.8 %collective-permute-start.5 = (bf16[128,128]{1,0:T(8,128)(2,1)S(1)}, bf16[128,128]{1,0:T(8,128)(2,1)S(1)}, u32[]{:S(2)}, u32[]{:S(2)}) collective-permute-start(bf16[128,128]{1,0:T(8,128)(2,1)S(1)} %copy-done.6), channel_id=1, source_target_pairs={{0,16},{16,0},{1,17},{17,1},{2,18},{18,2},{3,19},{19,3},{4,20},{20... | collective-permute-start | bytes 98312 | tf_op jit(solution)/shard_map/ppermute | solution.py:268
  92.0 9.7 %all_to_all.60.parts = bf16[16,8,256]{2,1,0:T(8,128)(2,1)S(1)} all-to-all(bf16[16,8,256]{2,1,0:T(8,128)(2,1)S(1)} %shard_map.256), channel_id=1, replica_groups=mesh['zh'=8,'za'=2,'c'=2,'tp'=16] {'tp'}, dimensions={0} | all-to-all | bytes 131072 | tf_op jit(solution)/shard_map/all_to_all | solution.py:264
  102.3 9.7 %all_to_all.61.middle = bf16[16,8,256]{2,1,0:T(8,128)(2,1)S(1)} all-to-all(bf16[16,8,256]{2,1,0:T(8,128)(2,1)S(1)} %shard_map.257), channel_id=1, replica_groups=mesh['zh'=8,'za'=2,'c'=2,'tp'=16] {'tp'}, dimensions={0} | all-to-all | bytes 131072 | tf_op jit(solution)/shard_map/all_to_all | solution.py:264
  113.5 10.2 %all-to-all-start.5 = ((bf16[16,8,640]{2,1,0:T(8,128)(2,1)}), bf16[16,8,640]{2,1,0:T(8,128)(2,1)S(1)}, u32[]{:S(2)}, u32[]{:S(2)}) async-start(bf16[16,8,640]{2,1,0:T(8,128)(2,1)} %shard_map.258), calls=%async_computation.5 | async-start | bytes 327680 | tf_op jit(solution)/shard_map/all_to_all | solution.py:264
  123.7 5.1 %collective-permute-start.12 = (bf16[128,640]{1,0:T(8,128)(2,1)S(1)}, bf16[128,640]{1,0:T(8,128)(2,1)S(1)}, u32[]{:S(2)}, u32[]{:S(2)}) collective-permute-start(bf16[128,640]{1,0:T(8,128)(2,1)S(1)} %collective-permute-done.9.refs_2_), channel_id=1, source_target_pairs={{0,16},{16,0},{1,17},{17,1},{2,18},{18,2},{3,19},{19,3},{4,20},{20... | collective-permute-start | bytes 491528 | tf_op jit(solution)/shard_map/ppermute | solution.py:268
  133.2 3.5 %collective-permute-start.15 = (f32[2,3,128]{2,1,0:T(4,128)S(1)}, f32[2,3,128]{2,1,0:T(4,128)S(1)}, u32[]{:S(2)}, u32[]{:S(2)}) collective-permute-start(f32[2,3,128]{2,1,0:T(4,128)S(1)} %pad_maximum_fusion), channel_id=1, source_target_pairs={{0,32},{32,0},{1,33},{33,1},{2,34},{34,2},{3,35},{35,3},{4,36},{36... | collective-permute-start | bytes 9224 | tf_op jit(solution)/shard_map/ppermute | solution.py:272
  139.3 22.6 %all_to_all.62.hidden = bf16[16,8,128]{2,1,0:T(8,128)(2,1)S(1)} all-to-all(bf16[16,8,128]{2,1,0:T(8,128)(2,1)S(1)} %shard_map.259), channel_id=1, replica_groups=mesh['zh'=8,'za'=2,'c'=2,'tp'=16] {'zh','za'}, dimensions={0} | all-to-all | bytes 65536 | tf_op jit(solution)/shard_map/all_to_all | solution.py:264
  162.1 9.4 %all_to_all.63.parts = bf16[16,8,256]{2,1,0:T(8,128)(2,1)S(1)} all-to-all(bf16[16,8,256]{2,1,0:T(8,128)(2,1)S(1)} %shard_map.260), channel_id=1, replica_groups=mesh['zh'=8,'za'=2,'c'=2,'tp'=16] {'tp'}, dimensions={0} | all-to-all | bytes 131072 | tf_op jit(solution)/shard_map/all_to_all | solution.py:264
  172.7 3.8 %all-to-all-start.8 = ((bf16[32,8,256]{2,1,0:T(8,128)(2,1)}), bf16[32,8,256]{2,1,0:T(8,128)(2,1)S(1)}, u32[]{:S(2)}, u32[]{:S(2)}) async-start(bf16[32,8,256]{2,1,0:T(8,128)(2,1)} %get-tuple-element.126), calls=%async_computation.8 | async-start | bytes 262144 | tf_op jit(solution)/shard_map/all_to_all | solution.py:264
  176.6 5.8 %collective-permute-start.16 = (bf16[8,128]{1,0:T(8,128)(2,1)S(1)}, bf16[8,128]{1,0:T(8,128)(2,1)S(1)}, u32[]{:S(2)}, u32[]{:S(2)}) collective-permute-start(bf16[8,128]{1,0:T(8,128)(2,1)S(1)} %get-tuple-element.127), channel_id=1, source_target_pairs={{0,16},{16,0},{1,17},{17,1},{2,18},{18,2},{3,19},{19,3},{4,20},{20... | collective-permute-start | bytes 6152 | tf_op jit(solution)/shard_map/ppermute | solution.py:268
  184.9 16.9 %all_to_all.64.parts = bf16[8,8,1408]{2,1,0:T(8,128)(2,1)S(1)} all-to-all(bf16[8,8,1408]{2,1,0:T(8,128)(2,1)S(1)} %shard_map.262), channel_id=1, replica_groups=mesh['zh'=8,'za'=2,'c'=2,'tp'=16] {'zh'}, dimensions={0} | all-to-all | bytes 360448 | tf_op jit(solution)/shard_map/all_to_all | solution.py:264
  201.9 15.1 %all_to_all.65.hidden = bf16[8,8,640]{2,1,0:T(8,128)(2,1)S(1)} all-to-all(bf16[8,8,640]{2,1,0:T(8,128)(2,1)S(1)} %shard_map.263), channel_id=1, replica_groups=mesh['zh'=8,'za'=2,'c'=2,'tp'=16] {'zh'}, dimensions={0} | all-to-all | bytes 163840 | tf_op jit(solution)/shard_map/all_to_all | solution.py:264
  217.8 21.2 %all_to_all.66 = bf16[64,8,128]{2,1,0:T(8,128)(2,1)S(1)} all-to-all(bf16[64,8,128]{2,1,0:T(8,128)(2,1)S(1)} %bitcast.35), channel_id=1, replica_groups=mesh['zh'=8,'za'=2,'c'=2,'tp'=16] {'za','c','tp'}, dimensions={0} | all-to-all | bytes 262144 | tf_op jit(solution)/shard_map/all_to_all | solution.py:264
  (88 shorter events, 35.4 us)
Async XLA Ops:
  0.0 25.9 %copy-start.4 = (bf16[128,640]{1,0:T(8,128)(2,1)S(1)}, bf16[128,640]{1,0:T(8,128)(2,1)}, u32[]{:S(2)}) copy-start(bf16[128,640]{1,0:T(8,128)(2,1)} %gate.1) | copy-start | bytes 491524
  0.0 25.9 %collective-permute-start.1 = (bf16[128,640]{1,0:T(8,128)(2,1)}, bf16[128,640]{1,0:T(8,128)(2,1)S(1)}, u32[]{:S(2)}, u32[]{:S(2)}) collective-permute-start(bf16[128,640]{1,0:T(8,128)(2,1)} %gate.1), channel_id=1, source_target_pairs={{0,16},{16,0},{1,17},{17,1},{2,18},{18,2},{3,19},{19,3},{4,20},{20... | collective-permute-start | bytes 491528 | tf_op jit(solution)/shard_map/ppermute | solution.py:268
  8.9 17.0 %collective-permute-start.2 = (bf16[128,640]{1,0:T(8,128)(2,1)}, bf16[128,640]{1,0:T(8,128)(2,1)S(1)}, u32[]{:S(2)}, u32[]{:S(2)}) collective-permute-start(bf16[128,640]{1,0:T(8,128)(2,1)} %up.1), channel_id=1, source_target_pairs={{0,16},{16,0},{1,17},{17,1},{2,18},{18,2},{3,19},{19,3},{4,20},{20... | collective-permute-start | bytes 491528 | tf_op jit(solution)/shard_map/ppermute | solution.py:268
  11.5 7.4 %collective-permute-start = (f32[3,128]{1,0:T(4,128)S(1)}, f32[3,128]{1,0:T(4,128)S(1)}, u32[]{:S(2)}, u32[]{:S(2)}) collective-permute-start(f32[3,128]{1,0:T(4,128)S(1)} %get-tuple-element.142.gains), channel_id=1, source_target_pairs={{0,16},{16,0},{1,17},{17,1},{2,18},{18,2},{3,19},{19,3},{4,20},{20... | collective-permute-start | bytes 4616 | tf_op jit(solution)/shard_map/ppermute | solution.py:268
  15.2 10.7 %all-to-all-start = ((bf16[32,8,128]{2,1,0:T(8,128)(2,1)}), bf16[32,8,128]{2,1,0:T(8,128)(2,1)S(1)}, u32[]{:S(2)}, u32[]{:S(2)}) async-start(bf16[32,8,128]{2,1,0:T(8,128)(2,1)} %bitcast.5), calls=%async_computation | async-start | bytes 131072 | tf_op jit(solution)/shard_map/all_to_all | solution.py:264
  28.4 29.7 %all-to-all-start.1 = ((bf16[16,8,1408]{2,1,0:T(8,128)(2,1)}), bf16[16,8,1408]{2,1,0:T(8,128)(2,1)S(1)}, u32[]{:S(2)}, u32[]{:S(2)}) async-start(bf16[16,8,1408]{2,1,0:T(8,128)(2,1)} %shard_map.253), calls=%async_computation.1 | async-start | bytes 720896 | tf_op jit(solution)/shard_map/all_to_all | solution.py:264
  43.2 12.8 %collective-permute-start.3 = (bf16[640,128]{1,0:T(8,128)(2,1)S(1)}, bf16[640,128]{1,0:T(8,128)(2,1)S(1)}, u32[]{:S(2)}, u32[]{:S(2)}) collective-permute-start(bf16[640,128]{1,0:T(8,128)(2,1)S(1)} %copy-done.2), channel_id=1, source_target_pairs={{0,16},{16,0},{1,17},{17,1},{2,18},{18,2},{3,19},{19,3},{4,20},{20... | collective-permute-start | bytes 491528 | tf_op jit(solution)/shard_map/ppermute | solution.py:268
  46.3 9.8 %collective-permute-start.4 = (bf16[128,512]{1,0:T(8,128)(2,1)S(1)}, bf16[128,512]{1,0:T(8,128)(2,1)S(1)}, u32[]{:S(2)}, u32[]{:S(2)}) collective-permute-start(bf16[128,512]{1,0:T(8,128)(2,1)S(1)} %constant_dynamic-update-slice_fusion.main), channel_id=1, source_target_pairs={{0,16},{16,0},{1,17},{17,1},{2,18},{18,2},{3,19},{19,3},{4,20},{20... | collective-permute-start | bytes 393224 | tf_op jit(solution)/shard_map/ppermute | solution.py:268
  58.2 29.9 %copy-start.6 = (bf16[128,128]{1,0:T(8,128)(2,1)S(1)}, bf16[128,128]{1,0:T(8,128)(2,1)}, u32[]{:S(2)}) copy-start(bf16[128,128]{1,0:T(8,128)(2,1)} %weight.1) | copy-start | bytes 98308
  59.0 32.7 %all-to-all-start.2 = ((bf16[16,8,640]{2,1,0:T(8,128)(2,1)}), bf16[16,8,640]{2,1,0:T(8,128)(2,1)S(1)}, u32[]{:S(2)}, u32[]{:S(2)}) async-start(bf16[16,8,640]{2,1,0:T(8,128)(2,1)} %shard_map.255), calls=%async_computation.2 | async-start | bytes 327680 | tf_op jit(solution)/shard_map/all_to_all | solution.py:264
  71.1 14.6 %collective-permute-start.9 = (bf16[128,640]{1,0:T(8,128)(2,1)S(1)}, bf16[128,640]{1,0:T(8,128)(2,1)S(1)}, u32[]{:S(2)}, u32[]{:S(2)}) collective-permute-start(bf16[128,640]{1,0:T(8,128)(2,1)S(1)} %copy-done), channel_id=1, source_target_pairs={{0,32},{32,0},{1,33},{33,1},{2,34},{34,2},{3,35},{35,3},{4,36},{36... | collective-permute-start | bytes 491528 | tf_op jit(solution)/shard_map/ppermute | solution.py:272
  74.4 13.7 %collective-permute-start.10 = (bf16[128,640]{1,0:T(8,128)(2,1)S(1)}, bf16[128,640]{1,0:T(8,128)(2,1)S(1)}, u32[]{:S(2)}, u32[]{:S(2)}) collective-permute-start(bf16[128,640]{1,0:T(8,128)(2,1)S(1)} %copy-done.1), channel_id=1, source_target_pairs={{0,32},{32,0},{1,33},{33,1},{2,34},{34,2},{3,35},{35,3},{4,36},{36... | collective-permute-start | bytes 491528 | tf_op jit(solution)/shard_map/ppermute | solution.py:272
  76.4 14.5 %collective-permute-start.11 = (bf16[640,128]{1,0:T(8,128)(2,1)S(1)}, bf16[640,128]{1,0:T(8,128)(2,1)S(1)}, u32[]{:S(2)}, u32[]{:S(2)}) collective-permute-start(bf16[640,128]{1,0:T(8,128)(2,1)S(1)} %copy-done.3), channel_id=1, source_target_pairs={{0,32},{32,0},{1,33},{33,1},{2,34},{34,2},{3,35},{35,3},{4,36},{36... | collective-permute-start | bytes 491528 | tf_op jit(solution)/shard_map/ppermute | solution.py:272
  79.7 12.1 %collective-permute-start.6 = (bf16[128,640]{1,0:T(8,128)(2,1)S(1)}, bf16[128,640]{1,0:T(8,128)(2,1)S(1)}, u32[]{:S(2)}, u32[]{:S(2)}) collective-permute-start(bf16[128,640]{1,0:T(8,128)(2,1)S(1)} %copy-done), channel_id=1, source_target_pairs={{0,16},{16,0},{1,17},{17,1},{2,18},{18,2},{3,19},{19,3},{4,20},{20... | collective-permute-start | bytes 491528 | tf_op jit(solution)/shard_map/ppermute | solution.py:268
  83.8 8.0 %collective-permute-start.7 = (bf16[128,640]{1,0:T(8,128)(2,1)S(1)}, bf16[128,640]{1,0:T(8,128)(2,1)S(1)}, u32[]{:S(2)}, u32[]{:S(2)}) collective-permute-start(bf16[128,640]{1,0:T(8,128)(2,1)S(1)} %copy-done.1), channel_id=1, source_target_pairs={{0,16},{16,0},{1,17},{17,1},{2,18},{18,2},{3,19},{19,3},{4,20},{20... | collective-permute-start | bytes 491528 | tf_op jit(solution)/shard_map/ppermute | solution.py:268
  85.7 6.0 %collective-permute-start.8 = (bf16[640,128]{1,0:T(8,128)(2,1)S(1)}, bf16[640,128]{1,0:T(8,128)(2,1)S(1)}, u32[]{:S(2)}, u32[]{:S(2)}) collective-permute-start(bf16[640,128]{1,0:T(8,128)(2,1)S(1)} %copy-done.3), channel_id=1, source_target_pairs={{0,16},{16,0},{1,17},{17,1},{2,18},{18,2},{3,19},{19,3},{4,20},{20... | collective-permute-start | bytes 491528 | tf_op jit(solution)/shard_map/ppermute | solution.py:268
  88.1 3.6 %collective-permute-start.5 = (bf16[128,128]{1,0:T(8,128)(2,1)S(1)}, bf16[128,128]{1,0:T(8,128)(2,1)S(1)}, u32[]{:S(2)}, u32[]{:S(2)}) collective-permute-start(bf16[128,128]{1,0:T(8,128)(2,1)S(1)} %copy-done.6), channel_id=1, source_target_pairs={{0,16},{16,0},{1,17},{17,1},{2,18},{18,2},{3,19},{19,3},{4,20},{20... | collective-permute-start | bytes 98312 | tf_op jit(solution)/shard_map/ppermute | solution.py:268
  113.5 24.5 %all-to-all-start.5 = ((bf16[16,8,640]{2,1,0:T(8,128)(2,1)}), bf16[16,8,640]{2,1,0:T(8,128)(2,1)S(1)}, u32[]{:S(2)}, u32[]{:S(2)}) async-start(bf16[16,8,640]{2,1,0:T(8,128)(2,1)} %shard_map.258), calls=%async_computation.5 | async-start | bytes 327680 | tf_op jit(solution)/shard_map/all_to_all | solution.py:264
  123.7 14.3 %collective-permute-start.12 = (bf16[128,640]{1,0:T(8,128)(2,1)S(1)}, bf16[128,640]{1,0:T(8,128)(2,1)S(1)}, u32[]{:S(2)}, u32[]{:S(2)}) collective-permute-start(bf16[128,640]{1,0:T(8,128)(2,1)S(1)} %collective-permute-done.9.refs_2_), channel_id=1, source_target_pairs={{0,16},{16,0},{1,17},{17,1},{2,18},{18,2},{3,19},{19,3},{4,20},{20... | collective-permute-start | bytes 491528 | tf_op jit(solution)/shard_map/ppermute | solution.py:268
  128.8 9.2 %collective-permute-start.13 = (bf16[128,640]{1,0:T(8,128)(2,1)S(1)}, bf16[128,640]{1,0:T(8,128)(2,1)S(1)}, u32[]{:S(2)}, u32[]{:S(2)}) collective-permute-start(bf16[128,640]{1,0:T(8,128)(2,1)S(1)} %collective-permute-done.10.refs_6_), channel_id=1, source_target_pairs={{0,16},{16,0},{1,17},{17,1},{2,18},{18,2},{3,19},{19,3},{4,20},{20... | collective-permute-start | bytes 491528 | tf_op jit(solution)/shard_map/ppermute | solution.py:268
  130.7 7.2 %collective-permute-start.14 = (bf16[640,128]{1,0:T(8,128)(2,1)S(1)}, bf16[640,128]{1,0:T(8,128)(2,1)S(1)}, u32[]{:S(2)}, u32[]{:S(2)}) collective-permute-start(bf16[640,128]{1,0:T(8,128)(2,1)S(1)} %collective-permute-done.11.refs_2_), channel_id=1, source_target_pairs={{0,16},{16,0},{1,17},{17,1},{2,18},{18,2},{3,19},{19,3},{4,20},{20... | collective-permute-start | bytes 491528 | tf_op jit(solution)/shard_map/ppermute | solution.py:268
  133.2 4.8 %collective-permute-start.15 = (f32[2,3,128]{2,1,0:T(4,128)S(1)}, f32[2,3,128]{2,1,0:T(4,128)S(1)}, u32[]{:S(2)}, u32[]{:S(2)}) collective-permute-start(f32[2,3,128]{2,1,0:T(4,128)S(1)} %pad_maximum_fusion), channel_id=1, source_target_pairs={{0,32},{32,0},{1,33},{33,1},{2,34},{34,2},{3,35},{35,3},{4,36},{36... | collective-permute-start | bytes 9224 | tf_op jit(solution)/shard_map/ppermute | solution.py:272
  172.7 11.2 %all-to-all-start.8 = ((bf16[32,8,256]{2,1,0:T(8,128)(2,1)}), bf16[32,8,256]{2,1,0:T(8,128)(2,1)S(1)}, u32[]{:S(2)}, u32[]{:S(2)}) async-start(bf16[32,8,256]{2,1,0:T(8,128)(2,1)} %get-tuple-element.126), calls=%async_computation.8 | async-start | bytes 262144 | tf_op jit(solution)/shard_map/all_to_all | solution.py:264
  176.6 6.6 %collective-permute-start.16 = (bf16[8,128]{1,0:T(8,128)(2,1)S(1)}, bf16[8,128]{1,0:T(8,128)(2,1)S(1)}, u32[]{:S(2)}, u32[]{:S(2)}) collective-permute-start(bf16[8,128]{1,0:T(8,128)(2,1)S(1)} %get-tuple-element.127), channel_id=1, source_target_pairs={{0,16},{16,0},{1,17},{17,1},{2,18},{18,2},{3,19},{19,3},{4,20},{20... | collective-permute-start | bytes 6152 | tf_op jit(solution)/shard_map/ppermute | solution.py:268
  (17 other events, 161.2 us)

commit v6 on v5

--- a/solution.py
+++ b/solution.py
@@ -78,13 +78,30 @@
     return jnp.maximum(x, 0.0) + jnp.log1p(jnp.exp(-jnp.abs(x)))
 
 
-def gate_up(slots, gates, ups, out):
-    n = gates[0].shape[1]
+def pack(gate, up, down, gains, out):
+    n = gate.shape[1]
+    out[:, :n] = gate[...]
+    out[:, n : 2 * n] = up[...]
+    for i in range(n // LANES):
+        at = 2 * n + i * LANES
+        out[:, at : at + LANES] = down[i * LANES : (i + 1) * LANES]
+    rest = gains[2:3]
+    row = lax.broadcasted_iota(jnp.int32, (out.shape[0], LANES), 0)
+    tile = jnp.zeros(row.shape, f32)
+    for i in range(3):
+        part = rest.astype(bf16).astype(f32)
+        tile = jnp.where(row == i, part, tile)
+        rest = rest - part
+    out[:, 3 * n :] = tile.astype(bf16)
+
+
+def gate_up(slots, weights, out):
+    n = (out.shape[2] - LANES) // 2
     count = out.shape[0]
     scaled = [(x * gain).astype(bf16) for x, gain in slots]
-    for at, weights in ((0, gates), (n, ups)):
-        part = sum(dot(x, w[...]) for x, w in zip(scaled, weights))
-        out[:, :, at : at + n] = blocked(part, count).astype(bf16)
+    for i in range(2):
+        part = sum(dot(x, w[i]) for x, w in zip(scaled, weights))
+        out[:, :, i * n : (i + 1) * n] = blocked(part, count).astype(bf16)
     square = jnp.sum(sum(x * x for x, _ in slots), -1, keepdims=True)
     out[:, :, 2 * n :] = blocked(lane_tile(square.shape[0], [square]), count).astype(bf16)
 
@@ -92,18 +109,23 @@
 def first_products(ids, got, gains, gains_x, gate, gate_x, up, up_x, out):
     core = ids[0]
     slots = [(flat(got[core]), gains[0:1]), (flat(got[1 - core]), gains_x[0:1])]
-    gate_up(slots, (gate, gate_x), (up, up_x), out)
-
-
-def second_products(ids, got, gains, gains_x, gains_z, *refs):
+    gate_up(slots, ((gate[...], up[...]), (gate_x[...], up_x[...])), out)
+
+
+def second_products(ids, got, *refs):
     out = refs[-1]
     side = ids[2]
-    slots = []
-    for chip, pair in ((side, (gains, gains_x)), (1 - side, (gains_z.at[0], gains_z.at[1]))):
-        wide = flat(got[chip, :, side])
+    n = (out.shape[2] - LANES) // 2
+    slots, weights = [], []
+    for i, packed in enumerate(refs[:-1]):
+        if i % 2 == 0:
+            wide = flat(got[(side, 1 - side)[i // 2], :, side])
         half = wide.shape[1] // 2
-        slots += [(wide[:, :half], pair[0][2:3]), (wide[:, half:], pair[1][2:3])]
-    gate_up(slots, refs[0:4], refs[4:8], out)
+        gain = packed[0:16, 3 * n :].astype(f32)
+        gain = gain[0:1] + gain[1:2] + gain[2:3]
+        slots.append((wide[:, i % 2 * half : (i % 2 + 1) * half], gain))
+        weights.append((packed[:, :n], packed[:, n : 2 * n]))
+    gate_up(slots, weights, out)
 
 
 def activate(parts, out, *, features):
@@ -121,14 +143,20 @@
     out[:, :, half:] = blocked(dot(rows, weight_x[...]), out.shape[0]).astype(bf16)
 
 
-def last_down(ids, hidden, *refs):
+def last_down(ids, hidden, second, *refs):
     out = refs[-1]
     core, side = ids[0], ids[2]
     rows = flat(hidden[...]).astype(bf16)
-    out[...] = jnp.zeros(out.shape, bf16)
-    for i, weight in enumerate(refs[:-1]):
+    n = rows.shape[1]
+    for i, packed in enumerate(refs[:-1]):
         chip, half = (side, 1 - side)[i // 2], (core, 1 - core)[i % 2]
-        out[chip, half, :, side] = blocked(dot(rows, weight[...]), out.shape[2]).astype(bf16)
+        part = sum(
+            dot(rows[:, j : j + LANES], packed[:, 2 * n + j : 2 * n + j + LANES])
+            for j in range(0, n, LANES)
+        )
+        out[chip, half, :, side] = blocked(part, out.shape[2]).astype(bf16)
+        at = i % 2 * LANES
+        out[chip, half, :, 1 - side] = second[chip, :, 1 - side, :, at : at + LANES]
 
 
 def add_first(ids, parts, got, out):
@@ -139,11 +167,10 @@
     out[...] = jnp.broadcast_to(rows[None], out.shape).astype(bf16)
 
 
-def add_mixer(ids, parts, middle, out, other):
+def add_mixer(ids, parts, middle, out):
     sums = jnp.sum(parts[...].astype(f32), axis=0)
-    rows = (middle[ids[1]].astype(f32) + sums).astype(bf16)
-    out[...] = jnp.broadcast_to(rows.astype(f32)[None], out.shape).astype(bf16)
-    other[...] = rows[:, rows.shape[1] // 2 :]
+    rows = middle[ids[1]].astype(f32) + sums
+    out[...] = jnp.broadcast_to(rows[None], out.shape).astype(bf16)
 
 
 def project(ids, middle, gains, gains_x, main, main_x, ws, ws_x, wd, wd_x, out):
@@ -250,14 +277,10 @@
     out[...] = jnp.broadcast_to(rows[None], out.shape).astype(bf16)
 
 
-def finish(ids, parts, got, other, out):
-    core, block, side = ids[0], ids[1], ids[2]
+def finish(ids, parts, out):
     sums = jnp.sum(parts[ids[3]].astype(f32), axis=1)
-    mine = got[side, block][:, : sums.shape[-1]].astype(f32)
-    theirs = other[...].astype(f32)
-    low = jnp.where(core == 0, mine, theirs) + 0.5 * sums[0]
-    high = jnp.where(core == 0, theirs, mine) + 0.5 * sums[1]
-    out[...] = jnp.concatenate([low, high], 0).astype(bf16)
+    rows = [parts[1 - ids[3], c, 0].astype(f32) + 0.5 * sums[c] for c in range(2)]
+    out[...] = jnp.concatenate(rows, 0).astype(bf16)
 
 
 def exchange(x, axis):
@@ -338,7 +361,6 @@
         scalars=1,
     )
 
-    both_gains = jnp.stack([gains, gains_x])
     sent, later = together(
         sent,
         (
@@ -416,13 +438,17 @@
         scalars=2,
         flops=1 << 28,
     )
-    state, gate2, up2, down2 = together(
-        state, second_gate_weight, second_up_weight, second_down_weight
-    )
-    gate2_z = swap_chips(gate2)
-    up2_z = swap_chips(up2)
-    down2_z = swap_chips(down2)
-    parts, down_x, main, main_x, ws, ws_x, wd, wd_x, state, new_extra, norm_gain, both_gains = (
+    packed = kernel(
+        pack,
+        ((width, 3 * hidden_units + LANES), bf16),
+        second_gate_weight,
+        second_up_weight,
+        second_down_weight,
+        gains,
+    )
+    state, packed = together(state, packed)
+    packed_z = swap_chips(packed)
+    parts, down_x, main, main_x, ws, ws_x, wd, wd_x, state, new_extra, norm_gain, packed = (
         together(
             parts,
             down_x,
@@ -435,22 +461,19 @@
             state,
             new_extra,
             norm_gain,
-            both_gains,
+            packed,
         )
     )
 
     hidden = kernel(
         activate, ((ring, rows, hidden_units), bf16), parts, features=features
     )
-    hidden, later = together(
-        hidden, (mixer_out_weight, second_gate_weight, second_up_weight, second_down_weight)
-    )
-    mixer_out_weight, second_gate_weight, second_up_weight, second_down_weight = later
+    hidden, mixer_out_weight, packed = together(hidden, mixer_out_weight, packed)
     hidden = exchange(hidden, Z)
-    out_x, gate2_x = swap(mixer_out_weight), swap(second_gate_weight)
-    up2_x, down2_x = swap(second_up_weight), swap(second_down_weight)
-    hidden, out_x, gate2_x, up2_x, down2_x, gate2_z, up2_z, down2_z = together(
-        hidden, out_x, gate2_x, up2_x, down2_x, gate2_z, up2_z, down2_z
+    out_x, packed_x = swap(mixer_out_weight), swap(packed)
+    packed_zx = swap(packed_z)
+    hidden, out_x, packed_x, packed_z, packed_zx = together(
+        hidden, out_x, packed_x, packed_z, packed_zx
     )
 
     parts = kernel(down, ((plane, rows, 2 * width), bf16), hidden, first_down_weight, down_x)
@@ -473,15 +496,7 @@
         wd_x,
         scalars=1,
     )
-    parts, gate2_z, up2_z, down2_z, both_gains = together(
-        parts, gate2_z, up2_z, down2_z, both_gains
-    )
     parts = exchange(parts, Z)
-    gate2_zx, up2_zx, down2_zx = swap(gate2_z), swap(up2_z), swap(down2_z)
-    gains_z = swap_chips(both_gains)
-    parts, gate2_zx, up2_zx, down2_zx, gains_z = together(
-        parts, gate2_zx, up2_zx, down2_zx, gains_z
-    )
     mixed = kernel(
         new_token,
         ((ring, rows, dk), bf16),
@@ -496,28 +511,16 @@
     mixed = exchange(mixed, Z)
     parts = kernel(down, ((plane, rows, 2 * width), bf16), mixed, mixer_out_weight, out_x)
     parts = exchange(parts, "tp")
-    second, other = kernel(
-        add_mixer,
-        [((2 * plane, rows, 2 * width), bf16), ((rows, width), bf16)],
-        ids,
-        parts,
-        middle,
-        scalars=1,
-    )
-    second = exchange(second, ("za", "tp"))
-    other = swap(other)
-    second, other = together(second, other)
+    second = kernel(add_mixer, ((2 * plane, rows, 2 * width), bf16), ids, parts, middle, scalars=1)
+    second = exchange(second, ("za", "tp")).reshape(2, plane // 2, 2, rows, 2 * width)
     half = ring // 2
+    slots = (packed, packed_x, packed_z, packed_zx)
     sent = kernel(
         second_products,
         ((half, rows, 2 * hidden_units + LANES), bf16),
         ids,
-        second.reshape(2, plane // 2, 2, rows, 2 * width),
-        gains,
-        gains_x,
-        gains_z,
-        *(second_gate_weight, gate2_x, gate2_z, gate2_zx),
-        *(second_up_weight, up2_x, up2_z, up2_zx),
+        second,
+        *slots,
         scalars=1,
     )
     parts = exchange(sent, "zh")
@@ -530,19 +533,13 @@
         ((2, 2, plane // 2, 2, rows, width), bf16),
         ids,
         hidden,
-        *(second_down_weight, down2_x, down2_z, down2_zx),
+        second,
+        *slots,
         scalars=1,
     )
     parts = exchange(parts.reshape(4 * plane, rows, width), ("za", "c", "tp"))
-    return kernel(
-        finish,
-        ((count, width), bf16),
-        ids,
-        parts.reshape(2, 2, plane, rows, width),
-        second.reshape(2, plane, rows, 2 * width),
-        other,
-        scalars=1,
-    )
+    parts = parts.reshape(2, 2, plane, rows, width)
+    return kernel(finish, ((count, width), bf16), ids, parts, scalars=1)
 
 
 def solution(mesh):

time: 242 us -> 224 us (0.926)
  starting transfers between devices: 99.5 us -> 56.1 us
  blocking collectives: 105 us -> 130 us
    all_to_all x7 -> x9, blocking collectives: 105 us -> 130 us  [exchange(): return lax.all_to_all(x, axis, 0, 0, tiled=True)]
    ppermute x13 -> x8, starting transfers between devices: 44.4 us -> 25.1 us  [swap(): return lax.ppermute(x, 'c', [(0, 1), (1, 0)])]
    all_to_all x5 -> x3, starting transfers between devices: 43.1 us -> 27.5 us  [exchange(): return lax.all_to_all(x, axis, 0, 0, tiled=True)]
    ppermute x4 -> x1, starting transfers between devices: 12.1 us -> 3.55 us  [swap_chips(): return lax.ppermute(x, 'za', [(0, 1), (1, 0)])]
    all_to_all x5 -> x3, waiting for transfers between devices: 9.85 us -> 11.5 us  [exchange(): return lax.all_to_all(x, axis, 0, 0, tiled=True)]
    pallas_call x13 -> x14, Pallas kernels: 16.9 us -> 15.7 us  [kernel(): pl.pallas_call(functools.partial(fn, **static), out_shape=shapes, in_spec...]
  transfers between devices with their start and end apart: 22 -> 12, of which waited for: 6 -> 4; matrix products, arithmetic and copies ran while one was open for 1% -> 1% of each run, Pallas kernels for 3% -> 3%
where the time goes in v6:
time: 224 us; the launch traced here: 222 us
  blocking collectives  130 us (58%)
  starting transfers between devices  56.1 us (25%)
  Pallas kernels  15.7 us (7%)
  waiting for transfers between devices  12.6 us (6%)
  local copies, waits for them, and re-layouts  5.2 us (2%)
    all_to_all x9, blocking collectives, exchange(): return lax.all_to_all(x, axis, 0, 0, tiled=True)  130 us
    all_to_all x3, starting transfers between devices, exchange(): return lax.all_to_all(x, axis, 0, 0, tiled=True)  27.5 us
    ppermute x8, starting transfers between devices, swap(): return lax.ppermute(x, 'c', [(0, 1), (1, 0)])  25.1 us
    pallas_call x14, Pallas kernels, kernel(): pl.pallas_call(functools.partial(fn, **static), out_shape=shapes, in_spec...  15.7 us
    all_to_all x3, waiting for transfers between devices, exchange(): return lax.all_to_all(x, axis, 0, 0, tiled=True)  11.5 us
  transfers between devices with their start and end apart: 12, of which 4 were waited for; matrix products, arithmetic and copies ran while one was open for 1% of the time, Pallas kernels for 3%

profile of v6, /device:TPU:1, one launch (start us, length us, event | category | flops | bytes accessed | tf_op | source)
XLA Modules:
  0.0 222.4 jit_solution(5152444706038362010)
XLA Ops:
  0.0 8.9 %collective-permute-start.1 = (bf16[128,640]{1,0:T(8,128)(2,1)}, bf16[128,640]{1,0:T(8,128)(2,1)S(1)}, u32[]{:S(2)}, u32[]{:S(2)}) collective-permute-start(bf16[128,640]{1,0:T(8,128)(2,1)} %gate.1), channel_id=1, source_target_pairs={{0,16},{16,0},{1,17},{17,1},{2,18},{18,2},{3,19},{19,3},{4,20},{20... | collective-permute-start | bytes 491528 | tf_op jit(solution)/shard_map/ppermute | solution.py:291
  8.9 1.9 collective-permute-start.2
  11.5 2.4 %collective-permute-start = (f32[3,128]{1,0:T(4,128)S(1)}, f32[3,128]{1,0:T(4,128)S(1)}, u32[]{:S(2)}, u32[]{:S(2)}) collective-permute-start(f32[3,128]{1,0:T(4,128)S(1)} %pad_maximum_fusion.gains), channel_id=1, source_target_pairs={{0,16},{16,0},{1,17},{17,1},{2,18},{18,2},{3,19},{19,3},{4,20},{20... | collective-permute-start | bytes 4616 | tf_op jit(solution)/shard_map/ppermute | solution.py:291
  15.2 3.6 %all-to-all-start = ((bf16[32,8,128]{2,1,0:T(8,128)(2,1)}), bf16[32,8,128]{2,1,0:T(8,128)(2,1)S(1)}, u32[]{:S(2)}, u32[]{:S(2)}) async-start(bf16[32,8,128]{2,1,0:T(8,128)(2,1)} %bitcast.5), calls=%async_computation | async-start | bytes 131072 | tf_op jit(solution)/shard_map/all_to_all | solution.py:287
  19.0 7.0 %all-to-all-done = bf16[32,8,128]{2,1,0:T(8,128)(2,1)S(1)} async-done(((bf16[32,8,128]{2,1,0:T(8,128)(2,1)}), bf16[32,8,128]{2,1,0:T(8,128)(2,1)S(1)}, u32[]{:S(2)}, u32[]{:S(2)}) %all-to-all-start) | async-done | bytes 65568 | tf_op jit(solution)/shard_map/all_to_all | solution.py:287
  28.5 13.3 %all-to-all-start.1 = ((bf16[16,8,1408]{2,1,0:T(8,128)(2,1)}), bf16[16,8,1408]{2,1,0:T(8,128)(2,1)S(1)}, u32[]{:S(2)}, u32[]{:S(2)}) async-start(bf16[16,8,1408]{2,1,0:T(8,128)(2,1)} %shard_map.253), calls=%async_computation.1 | async-start | bytes 720896 | tf_op jit(solution)/shard_map/all_to_all | solution.py:287
  43.2 2.9 %collective-permute-start.3 = (bf16[640,128]{1,0:T(8,128)(2,1)S(1)}, bf16[640,128]{1,0:T(8,128)(2,1)S(1)}, u32[]{:S(2)}, u32[]{:S(2)}) collective-permute-start(bf16[640,128]{1,0:T(8,128)(2,1)S(1)} %copy-done.3), channel_id=1, source_target_pairs={{0,16},{16,0},{1,17},{17,1},{2,18},{18,2},{3,19},{19,3},{4,20},{20... | collective-permute-start | bytes 491528 | tf_op jit(solution)/shard_map/ppermute | solution.py:291
  47.0 6.4 %shard_map.254 = (f32[8,128,128]{2,1,0:T(8,128)S(1)}, f32[8,128]{1,0:T(8,128)S(1)}, f32[8,128]{1,0:T(8,128)S(1)}) custom-call(s32[8]{0:T(128)S(1)} %copy-done.13, f32[2]{0:T(128)S(1)} %pad_maximum_fusion.1.head, f32[8,128,128]{2,1,0:T(8,128)S(1)} %bitcast.32, bf16[8,64,128]{2,1,0:T(8,128)(2,1)S(1)} %copy-done.8, bf16[8,64,128]{2,1,0:T(8,128)(2,1)S(1)} %copy-done.9, ...), custom_call_target="tpu_custom_call" | custom-call | flops 268435456 | bytes 793128 | tf_op jit(solution)/shard_map/pallas_call | solution.py:24
  53.4 3.5 %collective-permute-start.7 = (bf16[128,2048]{1,0:T(8,128)(2,1)S(1)}, bf16[128,2048]{1,0:T(8,128)(2,1)S(1)}, u32[]{:S(2)}, u32[]{:S(2)}) collective-permute-start(bf16[128,2048]{1,0:T(8,128)(2,1)S(1)} %shard_map.255.refs_0_), channel_id=1, source_target_pairs={{0,32},{32,0},{1,33},{33,1},{2,34},{34,2},{3,35},{35,3},{4,36},{36... | collective-permute-start | bytes 1572872 | tf_op jit(solution)/shard_map/ppermute | solution.py:295
  58.5 2.2 collective-permute-start.4
  62.6 10.5 %all-to-all-start.2 = ((bf16[16,8,640]{2,1,0:T(8,128)(2,1)}), bf16[16,8,640]{2,1,0:T(8,128)(2,1)S(1)}, u32[]{:S(2)}, u32[]{:S(2)}) async-start(bf16[16,8,640]{2,1,0:T(8,128)(2,1)} %shard_map.256), calls=%async_computation.2 | async-start | bytes 327680 | tf_op jit(solution)/shard_map/all_to_all | solution.py:287
  73.1 2.5 %collective-permute-start.8 = (bf16[128,2048]{1,0:T(8,128)(2,1)S(1)}, bf16[128,2048]{1,0:T(8,128)(2,1)S(1)}, u32[]{:S(2)}, u32[]{:S(2)}) collective-permute-start(bf16[128,2048]{1,0:T(8,128)(2,1)S(1)} %collective-permute-done.7.refs_2_), channel_id=1, source_target_pairs={{0,16},{16,0},{1,17},{17,1},{2,18},{18,2},{3,19},{19,3},{4,20},{20... | collective-permute-start | bytes 1572872 | tf_op jit(solution)/shard_map/ppermute | solution.py:291
  75.6 1.9 collective-permute-start.6
  77.6 2.4 %collective-permute-start.5 = (bf16[128,128]{1,0:T(8,128)(2,1)S(1)}, bf16[128,128]{1,0:T(8,128)(2,1)S(1)}, u32[]{:S(2)}, u32[]{:S(2)}) collective-permute-start(bf16[128,128]{1,0:T(8,128)(2,1)S(1)} %copy-done.6), channel_id=1, source_target_pairs={{0,16},{16,0},{1,17},{17,1},{2,18},{18,2},{3,19},{19,3},{4,20},{20... | collective-permute-start | bytes 98312 | tf_op jit(solution)/shard_map/ppermute | solution.py:291
  80.8 4.5 %all-to-all-done.2.hidden = bf16[16,8,640]{2,1,0:T(8,128)(2,1)S(1)} async-done(((bf16[16,8,640]{2,1,0:T(8,128)(2,1)}), bf16[16,8,640]{2,1,0:T(8,128)(2,1)S(1)}, u32[]{:S(2)}, u32[]{:S(2)}) %all-to-all-start.2) | async-done | bytes 163872 | tf_op jit(solution)/shard_map/all_to_all | solution.py:287
  85.6 9.3 %all_to_all.60.parts = bf16[16,8,256]{2,1,0:T(8,128)(2,1)S(1)} all-to-all(bf16[16,8,256]{2,1,0:T(8,128)(2,1)S(1)} %shard_map.257), channel_id=1, replica_groups=mesh['zh'=8,'za'=2,'c'=2,'tp'=16] {'tp'}, dimensions={0} | all-to-all | bytes 131072 | tf_op jit(solution)/shard_map/all_to_all | solution.py:287
  95.5 9.4 %all_to_all.61.middle = bf16[16,8,256]{2,1,0:T(8,128)(2,1)S(1)} all-to-all(bf16[16,8,256]{2,1,0:T(8,128)(2,1)S(1)} %shard_map.258), channel_id=1, replica_groups=mesh['zh'=8,'za'=2,'c'=2,'tp'=16] {'tp'}, dimensions={0} | all-to-all | bytes 131072 | tf_op jit(solution)/shard_map/all_to_all | solution.py:287
  105.7 20.0 %all_to_all.62.parts = bf16[16,8,640]{2,1,0:T(8,128)(2,1)S(1)} all-to-all(bf16[16,8,640]{2,1,0:T(8,128)(2,1)S(1)} %shard_map.259), channel_id=1, replica_groups=mesh['zh'=8,'za'=2,'c'=2,'tp'=16] {'zh','za'}, dimensions={0} | all-to-all | bytes 327680 | tf_op jit(solution)/shard_map/all_to_all | solution.py:287
  127.1 15.9 %all_to_all.63.hidden = bf16[16,8,128]{2,1,0:T(8,128)(2,1)S(1)} all-to-all(bf16[16,8,128]{2,1,0:T(8,128)(2,1)S(1)} %shard_map.260), channel_id=1, replica_groups=mesh['zh'=8,'za'=2,'c'=2,'tp'=16] {'zh','za'}, dimensions={0} | all-to-all | bytes 65536 | tf_op jit(solution)/shard_map/all_to_all | solution.py:287
  143.1 9.7 %all_to_all.64.parts = bf16[16,8,256]{2,1,0:T(8,128)(2,1)S(1)} all-to-all(bf16[16,8,256]{2,1,0:T(8,128)(2,1)S(1)} %shard_map.261), channel_id=1, replica_groups=mesh['zh'=8,'za'=2,'c'=2,'tp'=16] {'tp'}, dimensions={0} | all-to-all | bytes 131072 | tf_op jit(solution)/shard_map/all_to_all | solution.py:287
  153.3 10.7 %all_to_all.65 = bf16[32,8,256]{2,1,0:T(8,128)(2,1)S(1)} all-to-all(bf16[32,8,256]{2,1,0:T(8,128)(2,1)S(1)} %shard_map.262), channel_id=1, replica_groups=mesh['zh'=8,'za'=2,'c'=2,'tp'=16] {'za','tp'}, dimensions={0} | all-to-all | bytes 262144 | tf_op jit(solution)/shard_map/all_to_all | solution.py:287
  165.0 16.9 %all_to_all.66.parts = bf16[8,8,1408]{2,1,0:T(8,128)(2,1)S(1)} all-to-all(bf16[8,8,1408]{2,1,0:T(8,128)(2,1)S(1)} %shard_map.263), channel_id=1, replica_groups=mesh['zh'=8,'za'=2,'c'=2,'tp'=16] {'zh'}, dimensions={0} | all-to-all | bytes 360448 | tf_op jit(solution)/shard_map/all_to_all | solution.py:287
  182.0 14.8 %all_to_all.67.hidden = bf16[8,8,640]{2,1,0:T(8,128)(2,1)S(1)} all-to-all(bf16[8,8,640]{2,1,0:T(8,128)(2,1)S(1)} %shard_map.264), channel_id=1, replica_groups=mesh['zh'=8,'za'=2,'c'=2,'tp'=16] {'zh'}, dimensions={0} | all-to-all | bytes 163840 | tf_op jit(solution)/shard_map/all_to_all | solution.py:287
  197.7 23.6 %all_to_all.68 = bf16[64,8,128]{2,1,0:T(8,128)(2,1)S(1)} all-to-all(bf16[64,8,128]{2,1,0:T(8,128)(2,1)S(1)} %bitcast.31), channel_id=1, replica_groups=mesh['zh'=8,'za'=2,'c'=2,'tp'=16] {'za','c','tp'}, dimensions={0} | all-to-all | bytes 262144 | tf_op jit(solution)/shard_map/all_to_all | solution.py:287
  (70 shorter events, 16.5 us)
Async XLA Ops:
  0.0 25.9 %copy-start.4 = (bf16[128,640]{1,0:T(8,128)(2,1)S(1)}, bf16[128,640]{1,0:T(8,128)(2,1)}, u32[]{:S(2)}) copy-start(bf16[128,640]{1,0:T(8,128)(2,1)} %gate.1) | copy-start | bytes 491524
  0.0 25.9 %collective-permute-start.1 = (bf16[128,640]{1,0:T(8,128)(2,1)}, bf16[128,640]{1,0:T(8,128)(2,1)S(1)}, u32[]{:S(2)}, u32[]{:S(2)}) collective-permute-start(bf16[128,640]{1,0:T(8,128)(2,1)} %gate.1), channel_id=1, source_target_pairs={{0,16},{16,0},{1,17},{17,1},{2,18},{18,2},{3,19},{19,3},{4,20},{20... | collective-permute-start | bytes 491528 | tf_op jit(solution)/shard_map/ppermute | solution.py:291
  8.9 17.1 %collective-permute-start.2 = (bf16[128,640]{1,0:T(8,128)(2,1)}, bf16[128,640]{1,0:T(8,128)(2,1)S(1)}, u32[]{:S(2)}, u32[]{:S(2)}) collective-permute-start(bf16[128,640]{1,0:T(8,128)(2,1)} %up.1), channel_id=1, source_target_pairs={{0,16},{16,0},{1,17},{17,1},{2,18},{18,2},{3,19},{19,3},{4,20},{20... | collective-permute-start | bytes 491528 | tf_op jit(solution)/shard_map/ppermute | solution.py:291
  11.5 7.5 %collective-permute-start = (f32[3,128]{1,0:T(4,128)S(1)}, f32[3,128]{1,0:T(4,128)S(1)}, u32[]{:S(2)}, u32[]{:S(2)}) collective-permute-start(f32[3,128]{1,0:T(4,128)S(1)} %pad_maximum_fusion.gains), channel_id=1, source_target_pairs={{0,16},{16,0},{1,17},{17,1},{2,18},{18,2},{3,19},{19,3},{4,20},{20... | collective-permute-start | bytes 4616 | tf_op jit(solution)/shard_map/ppermute | solution.py:291
  15.2 10.7 %all-to-all-start = ((bf16[32,8,128]{2,1,0:T(8,128)(2,1)}), bf16[32,8,128]{2,1,0:T(8,128)(2,1)S(1)}, u32[]{:S(2)}, u32[]{:S(2)}) async-start(bf16[32,8,128]{2,1,0:T(8,128)(2,1)} %bitcast.5), calls=%async_computation | async-start | bytes 131072 | tf_op jit(solution)/shard_map/all_to_all | solution.py:287
  25.9 0.9 copy-start.5
  28.5 14.8 %copy-start.3 = (bf16[640,128]{1,0:T(8,128)(2,1)S(1)}, bf16[640,128]{1,0:T(8,128)(2,1)}, u32[]{:S(2)}) copy-start(bf16[640,128]{1,0:T(8,128)(2,1)} %weight) | copy-start | bytes 491524
  28.5 17.7 %copy-start = (bf16[128,640]{1,0:T(8,128)(2,1)S(1)}, bf16[128,640]{1,0:T(8,128)(2,1)}, u32[]{:S(2)}) copy-start(bf16[128,640]{1,0:T(8,128)(2,1)} %gate.2) | copy-start | bytes 491524
  28.5 17.7 %copy-start.1 = (bf16[128,640]{1,0:T(8,128)(2,1)S(1)}, bf16[128,640]{1,0:T(8,128)(2,1)}, u32[]{:S(2)}) copy-start(bf16[128,640]{1,0:T(8,128)(2,1)} %up.2) | copy-start | bytes 491524
  28.5 17.7 %copy-start.2 = (bf16[640,128]{1,0:T(8,128)(2,1)S(1)}, bf16[640,128]{1,0:T(8,128)(2,1)}, u32[]{:S(2)}) copy-start(bf16[640,128]{1,0:T(8,128)(2,1)} %down) | copy-start | bytes 491524
  28.5 33.3 %all-to-all-start.1 = ((bf16[16,8,1408]{2,1,0:T(8,128)(2,1)}), bf16[16,8,1408]{2,1,0:T(8,128)(2,1)S(1)}, u32[]{:S(2)}, u32[]{:S(2)}) async-start(bf16[16,8,1408]{2,1,0:T(8,128)(2,1)} %shard_map.253), calls=%async_computation.1 | async-start | bytes 720896 | tf_op jit(solution)/shard_map/all_to_all | solution.py:287
  41.8 4.5 %copy-start.7 = (f32[8,1,128,128]{3,2,1,0:T(8,128)S(1)}, f32[8,1,128,128]{3,2,1,0:T(8,128)}, u32[]{:S(2)}) copy-start(f32[8,1,128,128]{3,2,1,0:T(8,128)} %param.47) | copy-start | bytes 1572868
  43.2 3.1 %copy-start.8 = (bf16[8,64,128]{2,1,0:T(8,128)(2,1)S(1)}, bf16[8,64,128]{2,1,0:T(8,128)(2,1)}, u32[]{:S(2)}) copy-start(bf16[8,64,128]{2,1,0:T(8,128)(2,1)} %keys) | copy-start | bytes 393220
  43.2 3.1 %copy-start.9 = (bf16[8,64,128]{2,1,0:T(8,128)(2,1)S(1)}, bf16[8,64,128]{2,1,0:T(8,128)(2,1)}, u32[]{:S(2)}) copy-start(bf16[8,64,128]{2,1,0:T(8,128)(2,1)} %values) | copy-start | bytes 393220
  43.2 18.5 %collective-permute-start.3 = (bf16[640,128]{1,0:T(8,128)(2,1)S(1)}, bf16[640,128]{1,0:T(8,128)(2,1)S(1)}, u32[]{:S(2)}, u32[]{:S(2)}) collective-permute-start(bf16[640,128]{1,0:T(8,128)(2,1)S(1)} %copy-done.3), channel_id=1, source_target_pairs={{0,16},{16,0},{1,17},{17,1},{2,18},{18,2},{3,19},{19,3},{4,20},{20... | collective-permute-start | bytes 491528 | tf_op jit(solution)/shard_map/ppermute | solution.py:291
  47.0 10.0 %copy-start.15 = (bf16[128,128]{1,0:T(8,128)(2,1)S(1)}, bf16[128,128]{1,0:T(8,128)(2,1)}, u32[]{:S(2)}) copy-start(bf16[128,128]{1,0:T(8,128)(2,1)} %param.33) | copy-start | bytes 98308
  53.4 3.6 %copy-start.16 = (bf16[128,128]{1,0:T(8,128)(2,1)S(1)}, bf16[128,128]{1,0:T(8,128)(2,1)}, u32[]{:S(2)}) copy-start(bf16[128,128]{1,0:T(8,128)(2,1)} %param.34) | copy-start | bytes 98308
  53.4 19.7 %collective-permute-start.7 = (bf16[128,2048]{1,0:T(8,128)(2,1)S(1)}, bf16[128,2048]{1,0:T(8,128)(2,1)S(1)}, u32[]{:S(2)}, u32[]{:S(2)}) collective-permute-start(bf16[128,2048]{1,0:T(8,128)(2,1)S(1)} %shard_map.255.refs_0_), channel_id=1, source_target_pairs={{0,32},{32,0},{1,33},{33,1},{2,34},{34,2},{3,35},{35,3},{4,36},{36... | collective-permute-start | bytes 1572872 | tf_op jit(solution)/shard_map/ppermute | solution.py:295
  58.5 3.2 %collective-permute-start.4 = (bf16[128,512]{1,0:T(8,128)(2,1)S(1)}, bf16[128,512]{1,0:T(8,128)(2,1)S(1)}, u32[]{:S(2)}, u32[]{:S(2)}) collective-permute-start(bf16[128,512]{1,0:T(8,128)(2,1)S(1)} %constant_dynamic-update-slice_fusion.main), channel_id=1, source_target_pairs={{0,16},{16,0},{1,17},{17,1},{2,18},{18,2},{3,19},{19,3},{4,20},{20... | collective-permute-start | bytes 393224 | tf_op jit(solution)/shard_map/ppermute | solution.py:291
  62.6 15.0 %copy-start.6 = (bf16[128,128]{1,0:T(8,128)(2,1)S(1)}, bf16[128,128]{1,0:T(8,128)(2,1)}, u32[]{:S(2)}) copy-start(bf16[128,128]{1,0:T(8,128)(2,1)} %weight.1) | copy-start | bytes 98308
  62.6 22.7 %all-to-all-start.2 = ((bf16[16,8,640]{2,1,0:T(8,128)(2,1)}), bf16[16,8,640]{2,1,0:T(8,128)(2,1)S(1)}, u32[]{:S(2)}, u32[]{:S(2)}) async-start(bf16[16,8,640]{2,1,0:T(8,128)(2,1)} %shard_map.256), calls=%async_computation.2 | async-start | bytes 327680 | tf_op jit(solution)/shard_map/all_to_all | solution.py:287
  73.1 6.8 %collective-permute-start.8 = (bf16[128,2048]{1,0:T(8,128)(2,1)S(1)}, bf16[128,2048]{1,0:T(8,128)(2,1)S(1)}, u32[]{:S(2)}, u32[]{:S(2)}) collective-permute-start(bf16[128,2048]{1,0:T(8,128)(2,1)S(1)} %collective-permute-done.7.refs_2_), channel_id=1, source_target_pairs={{0,16},{16,0},{1,17},{17,1},{2,18},{18,2},{3,19},{19,3},{4,20},{20... | collective-permute-start | bytes 1572872 | tf_op jit(solution)/shard_map/ppermute | solution.py:291
  75.6 5.2 %collective-permute-start.6 = (bf16[128,2048]{1,0:T(8,128)(2,1)S(1)}, bf16[128,2048]{1,0:T(8,128)(2,1)S(1)}, u32[]{:S(2)}, u32[]{:S(2)}) collective-permute-start(bf16[128,2048]{1,0:T(8,128)(2,1)S(1)} %shard_map.255.refs_0_), channel_id=1, source_target_pairs={{0,16},{16,0},{1,17},{17,1},{2,18},{18,2},{3,19},{19,3},{4,20},{20... | collective-permute-start | bytes 1572872 | tf_op jit(solution)/shard_map/ppermute | solution.py:291
  77.6 3.3 %collective-permute-start.5 = (bf16[128,128]{1,0:T(8,128)(2,1)S(1)}, bf16[128,128]{1,0:T(8,128)(2,1)S(1)}, u32[]{:S(2)}, u32[]{:S(2)}) collective-permute-start(bf16[128,128]{1,0:T(8,128)(2,1)S(1)} %copy-done.6), channel_id=1, source_target_pairs={{0,16},{16,0},{1,17},{17,1},{2,18},{18,2},{3,19},{19,3},{4,20},{20... | collective-permute-start | bytes 98312 | tf_op jit(solution)/shard_map/ppermute | solution.py:291
  (7 other events, 5.0 us)

commit v7 on v6

--- a/solution.py
+++ b/solution.py
@@ -78,54 +78,83 @@
     return jnp.maximum(x, 0.0) + jnp.log1p(jnp.exp(-jnp.abs(x)))
 
 
-def pack(gate, up, down, gains, out):
+def spread(tokens, gain, out):
+    raw = tokens[...].astype(f32)
+    both = jnp.concatenate([raw, raw * gain[...]], 1)
+    both = both.reshape(out.shape[0], 1, out.shape[2], out.shape[3])
+    out[...] = jnp.broadcast_to(both, out.shape).astype(bf16)
+
+
+def pack_first(gate, up, out):
     n = gate.shape[1]
     out[:, :n] = gate[...]
-    out[:, n : 2 * n] = up[...]
-    for i in range(n // LANES):
-        at = 2 * n + i * LANES
-        out[:, at : at + LANES] = down[i * LANES : (i + 1) * LANES]
-    rest = gains[2:3]
+    out[:, n:] = up[...]
+
+
+def pack(gate, up, down, query, key, value, outer, mixer_out, gains, out):
+    n = gate.shape[1]
+    down = [down[i : i + LANES] for i in range(0, n, LANES)]
+    at = 0
+    for part in (gate, up, *down, query, key, value, outer, mixer_out):
+        out[:, at : at + part.shape[1]] = part[...]
+        at += part.shape[1]
     row = lax.broadcasted_iota(jnp.int32, (out.shape[0], LANES), 0)
     tile = jnp.zeros(row.shape, f32)
-    for i in range(3):
-        part = rest.astype(bf16).astype(f32)
-        tile = jnp.where(row == i, part, tile)
-        rest = rest - part
-    out[:, 3 * n :] = tile.astype(bf16)
-
-
-def gate_up(slots, weights, out):
+    for which in range(2):
+        rest = gains[which : which + 1]
+        for i in range(3):
+            part = rest.astype(bf16).astype(f32)
+            tile = jnp.where(row == 3 * which + i, part, tile)
+            rest = rest - part
+    out[:, at:] = tile.astype(bf16)
+
+
+def packed_gain(packed, which):
+    tile = packed[0:16, packed.shape[1] - LANES :].astype(f32)
+    at = 3 * which
+    return tile[at : at + 1] + tile[at + 1 : at + 2] + tile[at + 2 : at + 3]
+
+
+def order(ids):
+    core, side = ids[0], ids[2]
+    return [(chip, half) for chip in (side, 1 - side) for half in (core, 1 - core)]
+
+
+def gate_up(scaled, weights, square, out):
     n = (out.shape[2] - LANES) // 2
     count = out.shape[0]
-    scaled = [(x * gain).astype(bf16) for x, gain in slots]
     for i in range(2):
-        part = sum(dot(x, w[i]) for x, w in zip(scaled, weights))
+        part = sum(dot(x, w[:, i * n : (i + 1) * n]) for x, w in zip(scaled, weights))
         out[:, :, i * n : (i + 1) * n] = blocked(part, count).astype(bf16)
-    square = jnp.sum(sum(x * x for x, _ in slots), -1, keepdims=True)
     out[:, :, 2 * n :] = blocked(lane_tile(square.shape[0], [square]), count).astype(bf16)
 
 
-def first_products(ids, got, gains, gains_x, gate, gate_x, up, up_x, out):
+def row_sum(xs):
+    return jnp.sum(sum(x * x for x in xs), -1, keepdims=True)
+
+
+def first_products(ids, got, weights, weights_x, out):
     core = ids[0]
-    slots = [(flat(got[core]), gains[0:1]), (flat(got[1 - core]), gains_x[0:1])]
-    gate_up(slots, ((gate[...], up[...]), (gate_x[...], up_x[...])), out)
-
-
-def second_products(ids, got, *refs):
-    out = refs[-1]
-    side = ids[2]
-    n = (out.shape[2] - LANES) // 2
-    slots, weights = [], []
-    for i, packed in enumerate(refs[:-1]):
-        if i % 2 == 0:
-            wide = flat(got[(side, 1 - side)[i // 2], :, side])
-        half = wide.shape[1] // 2
-        gain = packed[0:16, 3 * n :].astype(f32)
-        gain = gain[0:1] + gain[1:2] + gain[2:3]
-        slots.append((wide[:, i % 2 * half : (i % 2 + 1) * half], gain))
-        weights.append((packed[:, :n], packed[:, n : 2 * n]))
-    gate_up(slots, weights, out)
+    wide = [flat(got[core]), flat(got[1 - core])]
+    raw = [x[:, :LANES] for x in wide]
+    scaled = [x[:, LANES:].astype(bf16) for x in wide]
+    gate_up(scaled, (weights, weights_x), row_sum(raw), out)
+
+
+def slices(ids, wide):
+    out = []
+    for chip in (ids[2], 1 - ids[2]):
+        rows = flat(wide(chip))
+        half = rows.shape[1] // 2
+        out += [rows[:, :half], rows[:, half:]]
+    return out
+
+
+def second_products(ids, second, *refs):
+    out, packs = refs[-1], refs[:-1]
+    raw = slices(ids, lambda chip: second[:, chip])
+    scaled = [(x * packed_gain(p, 1)).astype(bf16) for x, p in zip(raw, packs)]
+    gate_up(scaled, packs, row_sum(raw), out)
 
 
 def activate(parts, out, *, features):
@@ -136,7 +165,7 @@
     out[...] = jnp.broadcast_to(hidden[None], out.shape).astype(bf16)
 
 
-def down(hidden, weight, weight_x, out):
+def first_down(hidden, weight, weight_x, out):
     rows = flat(hidden[...]).astype(bf16)
     half = weight.shape[1]
     out[:, :, :half] = blocked(dot(rows, weight[...]), out.shape[0]).astype(bf16)
@@ -145,50 +174,62 @@
 
 def last_down(ids, hidden, second, *refs):
     out = refs[-1]
-    core, side = ids[0], ids[2]
+    side = ids[2]
     rows = flat(hidden[...]).astype(bf16)
     n = rows.shape[1]
-    for i, packed in enumerate(refs[:-1]):
-        chip, half = (side, 1 - side)[i // 2], (core, 1 - core)[i % 2]
+    for i, ((chip, half), packed) in enumerate(zip(order(ids), refs[:-1])):
         part = sum(
             dot(rows[:, j : j + LANES], packed[:, 2 * n + j : 2 * n + j + LANES])
             for j in range(0, n, LANES)
         )
-        out[chip, half, :, side] = blocked(part, out.shape[2]).astype(bf16)
+        out[chip, half, :, side, :, :LANES] = blocked(part, out.shape[2]).astype(bf16)
         at = i % 2 * LANES
-        out[chip, half, :, 1 - side] = second[chip, :, 1 - side, :, at : at + LANES]
+        out[chip, half, :, side, :, LANES:] = second[:, chip, :, at : at + LANES]
+        out[chip, half, :, 1 - side] = jnp.zeros((out.shape[2], *out.shape[4:]), bf16)
+
+
+def mixer_down(ids, mixed, *refs):
+    out = refs[-1]
+    rows = flat(mixed[...]).astype(bf16)
+    for i, ((chip, _), packed) in enumerate(zip(order(ids), refs[:-1])):
+        weight = packed[:, packed.shape[1] - 2 * LANES : packed.shape[1] - LANES]
+        at = i % 2 * LANES
+        out[:, chip, :, at : at + LANES] = blocked(dot(rows, weight), out.shape[0]).astype(bf16)
 
 
 def add_first(ids, parts, got, out):
     sums = jnp.sum(parts[...].astype(f32), axis=0)
     core, block = ids[0], ids[1]
     own, other = got[core, block].astype(f32), got[1 - core, block].astype(f32)
-    rows = jnp.concatenate([own, other], 1) + 0.5 * sums
+    rows = jnp.concatenate([own[:, :LANES], other[:, :LANES]], 1) + 0.5 * sums
     out[...] = jnp.broadcast_to(rows[None], out.shape).astype(bf16)
 
 
 def add_mixer(ids, parts, middle, out):
     sums = jnp.sum(parts[...].astype(f32), axis=0)
-    rows = middle[ids[1]].astype(f32) + sums
+    rows = middle[ids[3], ids[4], ids[2]].astype(f32) + sums
     out[...] = jnp.broadcast_to(rows[None], out.shape).astype(bf16)
 
 
-def project(ids, middle, gains, gains_x, main, main_x, ws, ws_x, wd, wd_x, out):
-    wide = flat(middle[...])
-    half = wide.shape[1] // 2
-    own, other = wide[:, :half], wide[:, half:]
-    scaled, scaled_x = (own * gains[1:2]).astype(bf16), (other * gains_x[1:2]).astype(bf16)
-    n, count = main.shape[1], out.shape[0]
-    part = dot(scaled, main[...]) + dot(scaled_x, main_x[...])
+def project(ids, middle, logits, *refs):
+    out, packs = refs[-1], refs[:-1]
+    side = ids[2]
+    n, count = out.shape[2] - LANES, out.shape[0]
+    raw = slices(ids, lambda chip: middle[chip, :, side])
+    scaled = [(x * packed_gain(p, 0)).astype(bf16) for x, p in zip(raw, packs)]
+    at = packs[0].shape[1] - 2 * LANES - n
+    part = sum(dot(x, p[:, at : at + n]) for x, p in zip(scaled, packs))
     out[:, :, :n] = blocked(part, count).astype(bf16)
-    heads = ws.shape[0]
-    mine = lax.broadcasted_iota(jnp.int32, (wide.shape[0], heads), 1) == ids[1]
+    heads = logits.shape[2]
+    mine = lax.broadcasted_iota(jnp.int32, (part.shape[0], heads), 1) == ids[1]
     columns = []
-    for w, w_x in ((ws, ws_x), (wd, wd_x)):
-        logit = dot_t(scaled, w[...]) + dot_t(scaled_x, w_x[...])
+    for i in range(2):
+        logit = sum(
+            dot_t(x, logits[i, chip * 2 + half]) for x, (chip, half) in zip(scaled, order(ids))
+        )
         columns.append(jnp.sum(jnp.where(mine, logit, 0.0), -1, keepdims=True))
-    columns.append(jnp.sum(own * own + other * other, -1, keepdims=True))
-    out[:, :, n:] = blocked(lane_tile(wide.shape[0], columns), count).astype(bf16)
+    columns.append(row_sum(raw))
+    out[:, :, n:] = blocked(lane_tile(part.shape[0], columns), count).astype(bf16)
 
 
 def earlier_state(
@@ -278,8 +319,12 @@
 
 
 def finish(ids, parts, out):
-    sums = jnp.sum(parts[ids[3]].astype(f32), axis=1)
-    rows = [parts[1 - ids[3], c, 0].astype(f32) + 0.5 * sums[c] for c in range(2)]
+    side = ids[3]
+    sums = jnp.sum(parts[side].astype(f32), axis=1)
+    half = out.shape[1]
+    rows = []
+    for c in range(2):
+        rows.append(parts[side, c, 0].astype(f32)[:, half:] + 0.5 * sums[c][:, :half])
     out[...] = jnp.concatenate(rows, 0).astype(bf16)
 
 
@@ -328,36 +373,31 @@
     position_decay_extra,
     lengths,
 ):
-    core, tp, z = lax.axis_index("c"), lax.axis_index("tp"), lax.axis_index(Z)
-    side = lax.axis_index("za")
+    core, tp, side = lax.axis_index("c"), lax.axis_index("tp"), lax.axis_index("za")
     plane, ring = lax.axis_size("tp"), lax.axis_size(Z)
     count, width = tokens.shape
-    rows = count // 2
+    rows, half = count // 2, ring // 2
     features = 2 * ring * width
     hidden_units = first_gate_weight.shape[1]
     dk = query_weight_matrix.shape[1]
-    ids = jnp.stack([core, tp, side, tp % 2]).astype(jnp.int32)
-    head = jnp.concatenate([head_decay_speed, head_decay_offset])
-
-    blocks = jnp.broadcast_to(tokens.reshape(2, 1, rows, width), (2, plane, rows, width))
-    got = exchange(blocks.reshape(2 * plane, rows, width), ("c", "tp"))
-    got = got.reshape(2, plane, rows, width)
-
-    gains = jnp.stack([first_norm_gain, mixer_norm_gain, second_norm_gain])
-    gate_x = swap(first_gate_weight)
-    up_x = swap(first_up_weight)
-    gains_x = swap(gains)
+    ids = jnp.stack([core, tp, side, tp & 1, tp >> 1]).astype(jnp.int32)
+
+    sent = kernel(
+        spread, ((2, plane, rows, 2 * width), bf16), tokens, first_norm_gain[None]
+    )
+    got = exchange(sent.reshape(2 * plane, rows, 2 * width), ("c", "tp"))
+    got = got.reshape(2, plane, rows, 2 * width)
+    first = kernel(
+        pack_first, ((width, 2 * hidden_units), bf16), first_gate_weight, first_up_weight
+    )
+    first_x = swap(first)
     sent = kernel(
         first_products,
         ((ring, rows, 2 * hidden_units + LANES), bf16),
         ids,
         got,
-        gains,
-        gains_x,
-        first_gate_weight,
-        gate_x,
-        first_up_weight,
-        up_x,
+        first,
+        first_x,
         scalars=1,
     )
 
@@ -365,59 +405,22 @@
         sent,
         (
             first_down_weight,
-            query_weight_matrix,
-            key_weight_matrix,
-            value_weight_matrix,
-            output_gate_weight,
-            strength_weight,
-            decay_weight,
-            recurrent,
-            earlier_key_cache,
-            earlier_value_cache,
-            strength_logit_history,
-            decay_input_history,
-            position_decay_extra,
-            lengths,
-            head_norm_gain,
-            mixer_out_weight,
-            second_gate_weight,
-            second_up_weight,
-            second_down_weight,
+            (second_gate_weight, second_up_weight, second_down_weight),
+            (query_weight_matrix, key_weight_matrix, value_weight_matrix, output_gate_weight),
+            (mixer_out_weight, mixer_norm_gain, second_norm_gain),
+            (strength_weight, decay_weight),
+            (head_decay_speed, head_decay_offset),
+            (recurrent, earlier_key_cache, earlier_value_cache),
+            (strength_logit_history, decay_input_history, position_decay_extra),
+            (lengths, head_norm_gain),
         ),
     )
-    (
-        first_down_weight,
-        query_weight_matrix,
-        key_weight_matrix,
-        value_weight_matrix,
-        output_gate_weight,
-        strength_weight,
-        decay_weight,
-        recurrent,
-        earlier_key_cache,
-        earlier_value_cache,
-        strength_logit_history,
-        decay_input_history,
-        position_decay_extra,
-        lengths,
-        head_norm_gain,
-        mixer_out_weight,
-        second_gate_weight,
-        second_up_weight,
-        second_down_weight,
-    ) = later
+    down, branch, heads, outer, logits, decays, caches, histories, others = later
     parts = exchange(sent, Z)
-    down_x = swap(first_down_weight)
-    main = jnp.concatenate(
-        [query_weight_matrix, key_weight_matrix, value_weight_matrix, output_gate_weight], 1
-    )
-    main_x = swap(main)
-
-    def small(w, which):
-        return lax.dynamic_slice_in_dim(w.T, (z * 2 + which) * width, width, 1)
-
-    ws, ws_x = small(strength_weight, core), small(strength_weight, 1 - core)
-    wd, wd_x = small(decay_weight, core), small(decay_weight, 1 - core)
+    down_x = swap(down)
+    gains = jnp.stack(outer[1:])
+    head = jnp.concatenate(decays)
+    lengths, head_norm_gain = others
     local = lengths.shape[0]
     state, new_extra, norm_gain = kernel(
         earlier_state,
@@ -428,78 +431,56 @@
         ],
         lengths,
         head,
-        recurrent[:, 0],
-        earlier_key_cache,
-        earlier_value_cache,
-        strength_logit_history[0],
-        decay_input_history[0],
-        position_decay_extra[0],
+        caches[0][:, 0],
+        *caches[1:],
+        *(h[0] for h in histories),
         head_norm_gain[None],
         scalars=2,
         flops=1 << 28,
     )
     packed = kernel(
         pack,
-        ((width, 3 * hidden_units + LANES), bf16),
-        second_gate_weight,
-        second_up_weight,
-        second_down_weight,
+        ((width, 3 * hidden_units + 4 * dk + width + LANES), bf16),
+        *branch,
+        *heads,
+        outer[0],
         gains,
     )
     state, packed = together(state, packed)
     packed_z = swap_chips(packed)
-    parts, down_x, main, main_x, ws, ws_x, wd, wd_x, state, new_extra, norm_gain, packed = (
-        together(
-            parts,
-            down_x,
-            main,
-            main_x,
-            ws,
-            ws_x,
-            wd,
-            wd_x,
-            state,
-            new_extra,
-            norm_gain,
-            packed,
-        )
-    )
-
-    hidden = kernel(
-        activate, ((ring, rows, hidden_units), bf16), parts, features=features
-    )
-    hidden, mixer_out_weight, packed = together(hidden, mixer_out_weight, packed)
+    start = lax.axis_index("zh") * 4 * width
+    logits = [lax.dynamic_slice_in_dim(w.T, start, 4 * width, 1) for w in logits]
+    logits = jnp.stack(logits).reshape(2, -1, 4, width).transpose(0, 2, 1, 3)
+    parts, down_x, logits, state, new_extra, norm_gain, packed = together(
+        parts, down_x, logits, state, new_extra, norm_gain, packed
+    )
+
+    hidden = kernel(activate, ((ring, rows, hidden_units), bf16), parts, features=features)
+    hidden, packed = together(hidden, packed)
     hidden = exchange(hidden, Z)
-    out_x, packed_x = swap(mixer_out_weight), swap(packed)
+    packed_x = swap(packed)
     packed_zx = swap(packed_z)
-    hidden, out_x, packed_x, packed_z, packed_zx = together(
-        hidden, out_x, packed_x, packed_z, packed_zx
-    )
-
-    parts = kernel(down, ((plane, rows, 2 * width), bf16), hidden, first_down_weight, down_x)
+    hidden, packed_x, packed_z, packed_zx = together(hidden, packed_x, packed_z, packed_zx)
+    packs = (packed, packed_x, packed_z, packed_zx)
+
+    parts = kernel(first_down, ((plane, rows, 2 * width), bf16), hidden, down, down_x)
     parts = exchange(parts, "tp")
-    middle = kernel(add_first, ((plane, rows, 2 * width), bf16), ids, parts, got, scalars=1)
-    middle = exchange(middle, "tp")
+    middle = kernel(add_first, ((2 * plane, rows, 2 * width), bf16), ids, parts, got, scalars=1)
+    middle = exchange(middle, ("za", "tp")).reshape(2, plane // 2, 2, rows, 2 * width)
 
     parts = kernel(
         project,
-        ((ring, rows, 4 * dk + LANES), bf16),
+        ((half, rows, 4 * dk + LANES), bf16),
         ids,
         middle,
-        gains,
-        gains_x,
-        main,
-        main_x,
-        ws,
-        ws_x,
-        wd,
-        wd_x,
+        logits,
+        *packs,
         scalars=1,
     )
-    parts = exchange(parts, Z)
+    parts = exchange(parts, "zh")
     mixed = kernel(
         new_token,
-        ((ring, rows, dk), bf16),
+        ((half, rows, dk), bf16),
         head,
         parts,
         state,
@@ -508,37 +489,36 @@
         scalars=1,
         features=features,
     )
-    mixed = exchange(mixed, Z)
-    parts = kernel(down, ((plane, rows, 2 * width), bf16), mixed, mixer_out_weight, out_x)
-    parts = exchange(parts, "tp")
-    second = kernel(add_mixer, ((2 * plane, rows, 2 * width), bf16), ids, parts, middle, scalars=1)
-    second = exchange(second, ("za", "tp")).reshape(2, plane // 2, 2, rows, 2 * width)
-    half = ring // 2
-    slots = (packed, packed_x, packed_z, packed_zx)
+    mixed = exchange(mixed, "zh")
+    parts = kernel(
+        mixer_down, ((plane // 2, 2, rows, 2 * width), bf16), ids, mixed, *packs, scalars=1
+    )
+    parts = exchange(parts.reshape(plane, rows, 2 * width), "tp")
+    second = kernel(add_mixer, ((plane, rows, 2 * width), bf16), ids, parts, middle, scalars=1)
+    second = exchange(second, "tp").reshape(plane // 2, 2, rows, 2 * width)
+
     sent = kernel(
         second_products,
         ((half, rows, 2 * hidden_units + LANES), bf16),
         ids,
         second,
-        *slots,
+        *packs,
         scalars=1,
     )
     parts = exchange(sent, "zh")
-    hidden = kernel(
-        activate, ((half, rows, hidden_units), bf16), parts, features=features
-    )
+    hidden = kernel(activate, ((half, rows, hidden_units), bf16), parts, features=features)
     hidden = exchange(hidden, "zh")
     parts = kernel(
         last_down,
-        ((2, 2, plane // 2, 2, rows, width), bf16),
+        ((2, 2, plane // 2, 2, rows, 2 * width), bf16),
         ids,
         hidden,
         second,
-        *slots,
+        *packs,
         scalars=1,
     )
-    parts = exchange(parts.reshape(4 * plane, rows, width), ("za", "c", "tp"))
-    parts = parts.reshape(2, 2, plane, rows, width)
+    parts = exchange(parts.reshape(4 * plane, rows, 2 * width), ("za", "c", "tp"))
+    parts = parts.reshape(2, 2, plane, rows, 2 * width)
     return kernel(finish, ((count, width), bf16), ids, parts, scalars=1)
 
 

time: 224 us -> 236 us (1.054)
  waiting for transfers between devices: 12.6 us -> 34.3 us
  starting transfers between devices: 56.1 us -> 47.4 us
    ppermute x1, waiting for transfers between devices: 0.01 us -> 14.6 us  [swap_chips(): return lax.ppermute(x, 'za', [(0, 1), (1, 0)])]
    ppermute x8 -> x4, starting transfers between devices: 25.1 us -> 16.9 us  [swap(): return lax.ppermute(x, 'c', [(0, 1), (1, 0)])]
    all_to_all x3, waiting for transfers between devices: 11.5 us -> 19.7 us  [exchange(): return lax.all_to_all(x, axis, 0, 0, tiled=True)]
    pallas_call x14 -> x16, Pallas kernels: 15.7 us -> 17 us  [kernel(): pl.pallas_call(functools.partial(fn, **static), out_shape=shapes, in_spec...]
  transfers between devices with their start and end apart: 12 -> 8, of which waited for: 4 -> 3; matrix products, arithmetic and copies ran while one was open for 1% -> 0% of each run, Pallas kernels for 3% -> 3%
where the time goes in v7:
time: 236 us
  blocking collectives  130 us (55%)
  starting transfers between devices  47.4 us (20%)
  waiting for transfers between devices  34.3 us (15%)
  Pallas kernels  17 us (7%)
  local copies, waits for them, and re-layouts  5.16 us (2%)
    all_to_all x9, blocking collectives, exchange(): return lax.all_to_all(x, axis, 0, 0, tiled=True)  130 us
    all_to_all x3, starting transfers between devices, exchange(): return lax.all_to_all(x, axis, 0, 0, tiled=True)  27.3 us
    all_to_all x3, waiting for transfers between devices, exchange(): return lax.all_to_all(x, axis, 0, 0, tiled=True)  19.7 us
    pallas_call x16, Pallas kernels, kernel(): pl.pallas_call(functools.partial(fn, **static), out_shape=shapes, in_spec...  17 us
    ppermute x4, starting transfers between devices, swap(): return lax.ppermute(x, 'c', [(0, 1), (1, 0)])  16.9 us
    ppermute x1, waiting for transfers between devices, swap_chips(): return lax.ppermute(x, 'za', [(0, 1), (1, 0)])  14.6 us
  transfers between devices with their start and end apart: 8, of which 3 were waited for; matrix products, arithmetic and copies ran while one was open for 0% of the time, Pallas kernels for 3%

profile of v7, /device:TPU:1, one launch (start us, length us, event | category | flops | bytes accessed | tf_op | source)
XLA Modules:
  0.0 235.5 jit_solution(15567556554964465677)
XLA Ops:
  1.9 8.7 %collective-permute-start = (bf16[128,1280]{1,0:T(8,128)(2,1)S(1)}, bf16[128,1280]{1,0:T(8,128)(2,1)S(1)}, u32[]{:S(2)}, u32[]{:S(2)}) collective-permute-start(bf16[128,1280]{1,0:T(8,128)(2,1)S(1)} %shard_map.254.weights), channel_id=1, source_target_pairs={{0,16},{16,0},{1,17},{17,1},{2,18},{18,2},{3,19},{19,3},{4,20},{20... | collective-permute-start | bytes 983048 | tf_op jit(solution)/shard_map/ppermute | solution.py:336
  11.3 3.6 %all-to-all-start = ((bf16[32,8,256]{2,1,0:T(8,128)(2,1)}), bf16[32,8,256]{2,1,0:T(8,128)(2,1)S(1)}, u32[]{:S(2)}, u32[]{:S(2)}) async-start(bf16[32,8,256]{2,1,0:T(8,128)(2,1)} %bitcast.6), calls=%async_computation | async-start | bytes 262144 | tf_op jit(solution)/shard_map/all_to_all | solution.py:332
  15.0 7.4 %all-to-all-done = bf16[32,8,256]{2,1,0:T(8,128)(2,1)S(1)} async-done(((bf16[32,8,256]{2,1,0:T(8,128)(2,1)}), bf16[32,8,256]{2,1,0:T(8,128)(2,1)S(1)}, u32[]{:S(2)}, u32[]{:S(2)}) %all-to-all-start) | async-done | bytes 131104 | tf_op jit(solution)/shard_map/all_to_all | solution.py:332
  22.5 1.6 shard_map.255
  24.1 13.3 %all-to-all-start.1 = ((bf16[16,8,1408]{2,1,0:T(8,128)(2,1)}), bf16[16,8,1408]{2,1,0:T(8,128)(2,1)S(1)}, u32[]{:S(2)}, u32[]{:S(2)}) async-start(bf16[16,8,1408]{2,1,0:T(8,128)(2,1)} %shard_map.255), calls=%async_computation.1 | async-start | bytes 720896 | tf_op jit(solution)/shard_map/all_to_all | solution.py:332
  40.7 6.4 %shard_map.256 = (f32[8,128,128]{2,1,0:T(8,128)S(1)}, f32[8,128]{1,0:T(8,128)S(1)}, f32[8,128]{1,0:T(8,128)S(1)}) custom-call(s32[8]{0:T(128)S(1)} %copy-done.21, f32[2]{0:T(128)S(1)} %pad_maximum_fusion.1.head, f32[8,128,128]{2,1,0:T(8,128)S(1)} %bitcast.36, bf16[8,64,128]{2,1,0:T(8,128)(2,1)S(1)} %copy-done.16, bf16[8,64,128]{2,1,0:T(8,128)(2,1)S(1)} %copy-done.17, ...), custom_call_target="tpu_custom_call" | custom-call | flops 268435456 | bytes 793128 | tf_op jit(solution)/shard_map/pallas_call | solution.py:24
  47.9 3.3 %collective-permute-start.3 = (bf16[128,2688]{1,0:T(8,128)(2,1)S(1)}, bf16[128,2688]{1,0:T(8,128)(2,1)S(1)}, u32[]{:S(2)}, u32[]{:S(2)}) collective-permute-start(bf16[128,2688]{1,0:T(8,128)(2,1)S(1)} %shard_map.257.refs_0_), channel_id=1, source_target_pairs={{0,32},{32,0},{1,33},{33,1},{2,34},{34,2},{3,35},{35,3},{4,36},{36... | collective-permute-start | bytes 2064392 | tf_op jit(solution)/shard_map/ppermute | solution.py:340
  51.2 3.3 %collective-permute-start.1 = (bf16[640,128]{1,0:T(8,128)(2,1)S(1)}, bf16[640,128]{1,0:T(8,128)(2,1)S(1)}, u32[]{:S(2)}, u32[]{:S(2)}) collective-permute-start(bf16[640,128]{1,0:T(8,128)(2,1)S(1)} %copy-done.7), channel_id=1, source_target_pairs={{0,16},{16,0},{1,17},{17,1},{2,18},{18,2},{3,19},{19,3},{4,20},{20... | collective-permute-start | bytes 491528 | tf_op jit(solution)/shard_map/ppermute | solution.py:336
  55.3 14.6 %collective-permute-done.3.refs_2_ = bf16[128,2688]{1,0:T(8,128)(2,1)S(1)} collective-permute-done((bf16[128,2688]{1,0:T(8,128)(2,1)S(1)}, bf16[128,2688]{1,0:T(8,128)(2,1)S(1)}, u32[]{:S(2)}, u32[]{:S(2)}) %collective-permute-start.3) | collective-permute-done | bytes 688160 | tf_op jit(solution)/shard_map/ppermute | solution.py:340
  69.9 2.9 %collective-permute-start.4 = (bf16[128,2688]{1,0:T(8,128)(2,1)S(1)}, bf16[128,2688]{1,0:T(8,128)(2,1)S(1)}, u32[]{:S(2)}, u32[]{:S(2)}) collective-permute-start(bf16[128,2688]{1,0:T(8,128)(2,1)S(1)} %collective-permute-done.3.refs_2_), channel_id=1, source_target_pairs={{0,16},{16,0},{1,17},{17,1},{2,18},{18,2},{3,19},{19,3},{4,20},{20... | collective-permute-start | bytes 2064392 | tf_op jit(solution)/shard_map/ppermute | solution.py:336
  73.7 1.9 collective-permute-start.2
  75.6 10.3 %all-to-all-start.2 = ((bf16[16,8,640]{2,1,0:T(8,128)(2,1)}), bf16[16,8,640]{2,1,0:T(8,128)(2,1)S(1)}, u32[]{:S(2)}, u32[]{:S(2)}) async-start(bf16[16,8,640]{2,1,0:T(8,128)(2,1)} %shard_map.258), calls=%async_computation.2 | async-start | bytes 327680 | tf_op jit(solution)/shard_map/all_to_all | solution.py:332
  85.9 12.3 %all-to-all-done.2.hidden = bf16[16,8,640]{2,1,0:T(8,128)(2,1)S(1)} async-done(((bf16[16,8,640]{2,1,0:T(8,128)(2,1)}), bf16[16,8,640]{2,1,0:T(8,128)(2,1)S(1)}, u32[]{:S(2)}, u32[]{:S(2)}) %all-to-all-start.2) | async-done | bytes 163872 | tf_op jit(solution)/shard_map/all_to_all | solution.py:332
  98.5 9.5 %all_to_all.60.parts = bf16[16,8,256]{2,1,0:T(8,128)(2,1)S(1)} all-to-all(bf16[16,8,256]{2,1,0:T(8,128)(2,1)S(1)} %shard_map.259), channel_id=1, replica_groups=mesh['zh'=8,'za'=2,'c'=2,'tp'=16] {'tp'}, dimensions={0} | all-to-all | bytes 131072 | tf_op jit(solution)/shard_map/all_to_all | solution.py:332
  108.5 14.1 %all_to_all.61 = bf16[32,8,256]{2,1,0:T(8,128)(2,1)S(1)} all-to-all(bf16[32,8,256]{2,1,0:T(8,128)(2,1)S(1)} %shard_map.260), channel_id=1, replica_groups=mesh['zh'=8,'za'=2,'c'=2,'tp'=16] {'za','tp'}, dimensions={0} | all-to-all | bytes 262144 | tf_op jit(solution)/shard_map/all_to_all | solution.py:332
  123.5 16.6 %all_to_all.62.parts = bf16[8,8,640]{2,1,0:T(8,128)(2,1)S(1)} all-to-all(bf16[8,8,640]{2,1,0:T(8,128)(2,1)S(1)} %shard_map.261), channel_id=1, replica_groups=mesh['zh'=8,'za'=2,'c'=2,'tp'=16] {'zh'}, dimensions={0} | all-to-all | bytes 163840 | tf_op jit(solution)/shard_map/all_to_all | solution.py:332
  140.1 1.3 shard_map.262
  141.4 13.8 %all_to_all.63.mixed = bf16[8,8,128]{2,1,0:T(8,128)(2,1)S(1)} all-to-all(bf16[8,8,128]{2,1,0:T(8,128)(2,1)S(1)} %shard_map.262), channel_id=1, replica_groups=mesh['zh'=8,'za'=2,'c'=2,'tp'=16] {'zh'}, dimensions={0} | all-to-all | bytes 32768 | tf_op jit(solution)/shard_map/all_to_all | solution.py:332
  155.9 9.5 %all_to_all.64.parts = bf16[16,8,256]{2,1,0:T(8,128)(2,1)S(1)} all-to-all(bf16[16,8,256]{2,1,0:T(8,128)(2,1)S(1)} %bitcast.34), channel_id=1, replica_groups=mesh['zh'=8,'za'=2,'c'=2,'tp'=16] {'tp'}, dimensions={0} | all-to-all | bytes 131072 | tf_op jit(solution)/shard_map/all_to_all | solution.py:332
  166.0 9.4 %all_to_all.65 = bf16[16,8,256]{2,1,0:T(8,128)(2,1)S(1)} all-to-all(bf16[16,8,256]{2,1,0:T(8,128)(2,1)S(1)} %shard_map.264), channel_id=1, replica_groups=mesh['zh'=8,'za'=2,'c'=2,'tp'=16] {'tp'}, dimensions={0} | all-to-all | bytes 131072 | tf_op jit(solution)/shard_map/all_to_all | solution.py:332
  176.3 16.5 %all_to_all.66.parts = bf16[8,8,1408]{2,1,0:T(8,128)(2,1)S(1)} all-to-all(bf16[8,8,1408]{2,1,0:T(8,128)(2,1)S(1)} %shard_map.265), channel_id=1, replica_groups=mesh['zh'=8,'za'=2,'c'=2,'tp'=16] {'zh'}, dimensions={0} | all-to-all | bytes 360448 | tf_op jit(solution)/shard_map/all_to_all | solution.py:332
  193.0 14.9 %all_to_all.67.hidden = bf16[8,8,640]{2,1,0:T(8,128)(2,1)S(1)} all-to-all(bf16[8,8,640]{2,1,0:T(8,128)(2,1)S(1)} %shard_map.266), channel_id=1, replica_groups=mesh['zh'=8,'za'=2,'c'=2,'tp'=16] {'zh'}, dimensions={0} | all-to-all | bytes 163840 | tf_op jit(solution)/shard_map/all_to_all | solution.py:332
  208.7 25.6 %all_to_all.68 = bf16[64,8,256]{2,1,0:T(8,128)(2,1)S(1)} all-to-all(bf16[64,8,256]{2,1,0:T(8,128)(2,1)S(1)} %bitcast.31), channel_id=1, replica_groups=mesh['zh'=8,'za'=2,'c'=2,'tp'=16] {'za','c','tp'}, dimensions={0} | all-to-all | bytes 524288 | tf_op jit(solution)/shard_map/all_to_all | solution.py:332
  234.3 1.2 shard_map.268
  (76 shorter events, 11.8 us)
Async XLA Ops:
  1.8 8.8 %copy-start.13 = (bf16[16,128]{1,0:T(8,128)(2,1)S(1)}, bf16[16,128]{1,0:T(8,128)(2,1)}, u32[]{:S(2)}) copy-start(bf16[16,128]{1,0:T(8,128)(2,1)} %tokens.1) | copy-start | bytes 12292
  1.9 8.8 %copy-start.14 = (f32[128]{0:T(128)S(1)}, f32[128]{0:T(128)}, u32[]{:S(2)}) copy-start(f32[128]{0:T(128)} %param.28) | copy-start | bytes 1540
  1.9 20.6 %collective-permute-start = (bf16[128,1280]{1,0:T(8,128)(2,1)S(1)}, bf16[128,1280]{1,0:T(8,128)(2,1)S(1)}, u32[]{:S(2)}, u32[]{:S(2)}) collective-permute-start(bf16[128,1280]{1,0:T(8,128)(2,1)S(1)} %shard_map.254.weights), channel_id=1, source_target_pairs={{0,16},{16,0},{1,17},{17,1},{2,18},{18,2},{3,19},{19,3},{4,20},{20... | collective-permute-start | bytes 983048 | tf_op jit(solution)/shard_map/ppermute | solution.py:336
  11.3 11.2 %all-to-all-start = ((bf16[32,8,256]{2,1,0:T(8,128)(2,1)}), bf16[32,8,256]{2,1,0:T(8,128)(2,1)S(1)}, u32[]{:S(2)}, u32[]{:S(2)}) async-start(bf16[32,8,256]{2,1,0:T(8,128)(2,1)} %bitcast.6), calls=%async_computation | async-start | bytes 262144 | tf_op jit(solution)/shard_map/all_to_all | solution.py:332
  24.1 15.4 %copy-start.4 = (bf16[128,640]{1,0:T(8,128)(2,1)S(1)}, bf16[128,640]{1,0:T(8,128)(2,1)}, u32[]{:S(2)}) copy-start(bf16[128,640]{1,0:T(8,128)(2,1)} %gate.2) | copy-start | bytes 491524
  24.1 15.4 %copy-start.5 = (bf16[128,640]{1,0:T(8,128)(2,1)S(1)}, bf16[128,640]{1,0:T(8,128)(2,1)}, u32[]{:S(2)}) copy-start(bf16[128,640]{1,0:T(8,128)(2,1)} %up.2) | copy-start | bytes 491524
  24.1 15.4 %copy-start.6 = (bf16[640,128]{1,0:T(8,128)(2,1)S(1)}, bf16[640,128]{1,0:T(8,128)(2,1)}, u32[]{:S(2)}) copy-start(bf16[640,128]{1,0:T(8,128)(2,1)} %down) | copy-start | bytes 491524
  24.1 15.4 %copy-start.8 = (bf16[128,128]{1,0:T(8,128)(2,1)S(1)}, bf16[128,128]{1,0:T(8,128)(2,1)}, u32[]{:S(2)}) copy-start(bf16[128,128]{1,0:T(8,128)(2,1)} %query) | copy-start | bytes 98308
  24.1 15.4 %copy-start.9 = (bf16[128,128]{1,0:T(8,128)(2,1)S(1)}, bf16[128,128]{1,0:T(8,128)(2,1)}, u32[]{:S(2)}) copy-start(bf16[128,128]{1,0:T(8,128)(2,1)} %key) | copy-start | bytes 98308
  24.1 15.4 %copy-start.10 = (bf16[128,128]{1,0:T(8,128)(2,1)S(1)}, bf16[128,128]{1,0:T(8,128)(2,1)}, u32[]{:S(2)}) copy-start(bf16[128,128]{1,0:T(8,128)(2,1)} %value) | copy-start | bytes 98308
  24.1 15.4 %copy-start.11 = (bf16[128,128]{1,0:T(8,128)(2,1)S(1)}, bf16[128,128]{1,0:T(8,128)(2,1)}, u32[]{:S(2)}) copy-start(bf16[128,128]{1,0:T(8,128)(2,1)} %outer) | copy-start | bytes 98308
  24.1 15.4 %copy-start.12 = (bf16[128,128]{1,0:T(8,128)(2,1)S(1)}, bf16[128,128]{1,0:T(8,128)(2,1)}, u32[]{:S(2)}) copy-start(bf16[128,128]{1,0:T(8,128)(2,1)} %mixer_out) | copy-start | bytes 98308
  24.1 48.7 %all-to-all-start.1 = ((bf16[16,8,1408]{2,1,0:T(8,128)(2,1)}), bf16[16,8,1408]{2,1,0:T(8,128)(2,1)S(1)}, u32[]{:S(2)}, u32[]{:S(2)}) async-start(bf16[16,8,1408]{2,1,0:T(8,128)(2,1)} %shard_map.255), calls=%async_computation.1 | async-start | bytes 720896 | tf_op jit(solution)/shard_map/all_to_all | solution.py:332
  39.6 1.0 copy-start.15
  39.6 1.1 copy-start.16
  39.6 1.1 copy-start.17
  39.6 1.1 copy-start.20
  40.7 10.5 %copy-start.7 = (bf16[640,128]{1,0:T(8,128)(2,1)S(1)}, bf16[640,128]{1,0:T(8,128)(2,1)}, u32[]{:S(2)}) copy-start(bf16[640,128]{1,0:T(8,128)(2,1)} %weight) | copy-start | bytes 491524
  47.9 22.0 %collective-permute-start.3 = (bf16[128,2688]{1,0:T(8,128)(2,1)S(1)}, bf16[128,2688]{1,0:T(8,128)(2,1)S(1)}, u32[]{:S(2)}, u32[]{:S(2)}) collective-permute-start(bf16[128,2688]{1,0:T(8,128)(2,1)S(1)} %shard_map.257.refs_0_), channel_id=1, source_target_pairs={{0,32},{32,0},{1,33},{33,1},{2,34},{34,2},{3,35},{35,3},{4,36},{36... | collective-permute-start | bytes 2064392 | tf_op jit(solution)/shard_map/ppermute | solution.py:340
  51.2 21.6 %collective-permute-start.1 = (bf16[640,128]{1,0:T(8,128)(2,1)S(1)}, bf16[640,128]{1,0:T(8,128)(2,1)S(1)}, u32[]{:S(2)}, u32[]{:S(2)}) collective-permute-start(bf16[640,128]{1,0:T(8,128)(2,1)S(1)} %copy-done.7), channel_id=1, source_target_pairs={{0,16},{16,0},{1,17},{17,1},{2,18},{18,2},{3,19},{19,3},{4,20},{20... | collective-permute-start | bytes 491528 | tf_op jit(solution)/shard_map/ppermute | solution.py:336
  69.9 16.1 %collective-permute-start.4 = (bf16[128,2688]{1,0:T(8,128)(2,1)S(1)}, bf16[128,2688]{1,0:T(8,128)(2,1)S(1)}, u32[]{:S(2)}, u32[]{:S(2)}) collective-permute-start(bf16[128,2688]{1,0:T(8,128)(2,1)S(1)} %collective-permute-done.3.refs_2_), channel_id=1, source_target_pairs={{0,16},{16,0},{1,17},{17,1},{2,18},{18,2},{3,19},{19,3},{4,20},{20... | collective-permute-start | bytes 2064392 | tf_op jit(solution)/shard_map/ppermute | solution.py:336
  73.7 24.6 %collective-permute-start.2 = (bf16[128,2688]{1,0:T(8,128)(2,1)S(1)}, bf16[128,2688]{1,0:T(8,128)(2,1)S(1)}, u32[]{:S(2)}, u32[]{:S(2)}) collective-permute-start(bf16[128,2688]{1,0:T(8,128)(2,1)S(1)} %shard_map.257.refs_0_), channel_id=1, source_target_pairs={{0,16},{16,0},{1,17},{17,1},{2,18},{18,2},{3,19},{19,3},{4,20},{20... | collective-permute-start | bytes 2064392 | tf_op jit(solution)/shard_map/ppermute | solution.py:336
  75.6 22.6 %all-to-all-start.2 = ((bf16[16,8,640]{2,1,0:T(8,128)(2,1)}), bf16[16,8,640]{2,1,0:T(8,128)(2,1)S(1)}, u32[]{:S(2)}, u32[]{:S(2)}) async-start(bf16[16,8,640]{2,1,0:T(8,128)(2,1)} %shard_map.258), calls=%async_computation.2 | async-start | bytes 327680 | tf_op jit(solution)/shard_map/all_to_all | solution.py:332
  122.6 17.5 %copy-start.1 = (f32[8,128,128]{2,1,0:T(8,128)S(1)}, f32[8,128,128]{2,1,0:T(8,128)}, u32[]{:S(2)}) copy-start(f32[8,128,128]{2,1,0:T(8,128)} %copy-done) | copy-start | bytes 1572868
  (9 other events, 7.7 us)

commit v8 on v7

--- a/solution.py
+++ b/solution.py
@@ -91,9 +91,9 @@
     out[:, n:] = up[...]
 
 
-def pack(gate, up, down, query, key, value, outer, mixer_out, gains, out):
+def pack(gate, up, down, first, query, key, value, outer, mixer_out, gains, out):
     n = gate.shape[1]
-    down = [down[i : i + LANES] for i in range(0, n, LANES)]
+    down = [w[i : i + LANES] for w in (down, first) for i in range(0, n, LANES)]
     at = 0
     for part in (gate, up, *down, query, key, value, outer, mixer_out):
         out[:, at : at + part.shape[1]] = part[...]
@@ -165,11 +165,21 @@
     out[...] = jnp.broadcast_to(hidden[None], out.shape).astype(bf16)
 
 
-def first_down(hidden, weight, weight_x, out):
+def down_product(rows, packed, at):
+    n = rows.shape[1]
+    return sum(
+        dot(rows[:, j : j + LANES], packed[:, at + j : at + j + LANES])
+        for j in range(0, n, LANES)
+    )
+
+
+def first_down(ids, hidden, *refs):
+    out = refs[-1]
     rows = flat(hidden[...]).astype(bf16)
-    half = weight.shape[1]
-    out[:, :, :half] = blocked(dot(rows, weight[...]), out.shape[0]).astype(bf16)
-    out[:, :, half:] = blocked(dot(rows, weight_x[...]), out.shape[0]).astype(bf16)
+    for i, ((chip, _), packed) in enumerate(zip(order(ids), refs[:-1])):
+        at = i % 2 * LANES
+        part = down_product(rows, packed, 3 * rows.shape[1])
+        out[:, chip, :, at : at + LANES] = blocked(part, out.shape[0]).astype(bf16)
 
 
 def last_down(ids, hidden, second, *refs):
@@ -178,10 +188,7 @@
     rows = flat(hidden[...]).astype(bf16)
     n = rows.shape[1]
     for i, ((chip, half), packed) in enumerate(zip(order(ids), refs[:-1])):
-        part = sum(
-            dot(rows[:, j : j + LANES], packed[:, 2 * n + j : 2 * n + j + LANES])
-            for j in range(0, n, LANES)
-        )
+        part = down_product(rows, packed, 2 * n)
         out[chip, half, :, side, :, :LANES] = blocked(part, out.shape[2]).astype(bf16)
         at = i % 2 * LANES
         out[chip, half, :, side, :, LANES:] = second[:, chip, :, at : at + LANES]
@@ -197,25 +204,28 @@
         out[:, chip, :, at : at + LANES] = blocked(dot(rows, weight), out.shape[0]).astype(bf16)
 
 
-def add_first(ids, parts, got, out):
+def add_first(ids, parts, got, got_z, out):
     sums = jnp.sum(parts[...].astype(f32), axis=0)
-    core, block = ids[0], ids[1]
-    own, other = got[core, block].astype(f32), got[1 - core, block].astype(f32)
-    rows = jnp.concatenate([own[:, :LANES], other[:, :LANES]], 1) + 0.5 * sums
+    core, side, chip = ids[0], ids[2], ids[3]
+    block = 2 * ids[4] + side
+    halves = []
+    for c in (core, 1 - core):
+        mine, theirs = got[c, block].astype(f32), got_z[c, block].astype(f32)
+        halves.append(jnp.where(chip == side, mine, theirs)[:, :LANES])
+    rows = jnp.concatenate(halves, 1) + 0.5 * sums
     out[...] = jnp.broadcast_to(rows[None], out.shape).astype(bf16)
 
 
 def add_mixer(ids, parts, middle, out):
     sums = jnp.sum(parts[...].astype(f32), axis=0)
-    rows = middle[ids[3], ids[4], ids[2]].astype(f32) + sums
+    rows = middle[ids[4], ids[3]].astype(f32) + sums
     out[...] = jnp.broadcast_to(rows[None], out.shape).astype(bf16)
 
 
 def project(ids, middle, logits, *refs):
     out, packs = refs[-1], refs[:-1]
-    side = ids[2]
     n, count = out.shape[2] - LANES, out.shape[0]
-    raw = slices(ids, lambda chip: middle[chip, :, side])
+    raw = slices(ids, lambda chip: middle[:, chip])
     scaled = [(x * packed_gain(p, 0)).astype(bf16) for x, p in zip(raw, packs)]
     at = packs[0].shape[1] - 2 * LANES - n
     part = sum(dot(x, p[:, at : at + n]) for x, p in zip(scaled, packs))
@@ -417,7 +427,6 @@
     )
     down, branch, heads, outer, logits, decays, caches, histories, others = later
     parts = exchange(sent, Z)
-    down_x = swap(down)
     gains = jnp.stack(outer[1:])
     head = jnp.concatenate(decays)
     lengths, head_norm_gain = others
@@ -440,33 +449,41 @@
     )
     packed = kernel(
         pack,
-        ((width, 3 * hidden_units + 4 * dk + width + LANES), bf16),
+        ((width, 4 * hidden_units + 4 * dk + width + LANES), bf16),
         *branch,
+        down,
         *heads,
         outer[0],
         gains,
     )
     state, packed = together(state, packed)
     packed_z = swap_chips(packed)
+    got_z = swap_chips(got)
     start = lax.axis_index("zh") * 4 * width
     logits = [lax.dynamic_slice_in_dim(w.T, start, 4 * width, 1) for w in logits]
     logits = jnp.stack(logits).reshape(2, -1, 4, width).transpose(0, 2, 1, 3)
-    parts, down_x, logits, state, new_extra, norm_gain, packed = together(
-        parts, down_x, logits, state, new_extra, norm_gain, packed
-    )
-
-    hidden = kernel(activate, ((ring, rows, hidden_units), bf16), parts, features=features)
+    parts, logits, state, new_extra, norm_gain, packed = together(
+        parts, logits, state, new_extra, norm_gain, packed
+    )
+
+    hidden = kernel(activate, ((half, rows, hidden_units), bf16), parts, features=features)
     hidden, packed = together(hidden, packed)
-    hidden = exchange(hidden, Z)
+    hidden = exchange(hidden, "zh")
     packed_x = swap(packed)
     packed_zx = swap(packed_z)
-    hidden, packed_x, packed_z, packed_zx = together(hidden, packed_x, packed_z, packed_zx)
+    hidden, packed_x, packed_z, packed_zx, got_z = together(
+        hidden, packed_x, packed_z, packed_zx, got_z
+    )
     packs = (packed, packed_x, packed_z, packed_zx)
 
-    parts = kernel(first_down, ((plane, rows, 2 * width), bf16), hidden, down, down_x)
-    parts = exchange(parts, "tp")
-    middle = kernel(add_first, ((2 * plane, rows, 2 * width), bf16), ids, parts, got, scalars=1)
-    middle = exchange(middle, ("za", "tp")).reshape(2, plane // 2, 2, rows, 2 * width)
+    parts = kernel(
+        first_down, ((plane // 2, 2, rows, 2 * width), bf16), ids, hidden, *packs, scalars=1
+    )
+    parts = exchange(parts.reshape(plane, rows, 2 * width), "tp")
+    middle = kernel(
+        add_first, ((plane, rows, 2 * width), bf16), ids, parts, got, got_z, scalars=1
+    )
+    middle = exchange(middle, "tp").reshape(plane // 2, 2, rows, 2 * width)
 
     parts = kernel(
         project,

time: 236 us -> 240 us (1.017)
  waiting for transfers between devices: 34.3 us -> 37.2 us
    ppermute x1 -> x2, waiting for transfers between devices: 14.6 us -> 25.9 us  [swap_chips(): return lax.ppermute(x, 'za', [(0, 1), (1, 0)])]
    all_to_all x3, waiting for transfers between devices: 19.7 us -> 11.4 us  [exchange(): return lax.all_to_all(x, axis, 0, 0, tiled=True)]
    ppermute x4 -> x3, starting transfers between devices: 16.9 us -> 13.6 us  [swap(): return lax.ppermute(x, 'c', [(0, 1), (1, 0)])]
    ppermute x1 -> x2, starting transfers between devices: 3.27 us -> 6.34 us  [swap_chips(): return lax.ppermute(x, 'za', [(0, 1), (1, 0)])]
    unnamed x50 -> x58, local copies, waits for them, and re-layouts: 4.29 us -> 5.53 us
  transfers between devices with their start and end apart: 8 -> 8, of which waited for: 3 -> 4; matrix products, arithmetic and copies ran while one was open for 0% -> 1% of each run, Pallas kernels for 3% -> 3%
where the time goes in v8:
time: 240 us; the launch traced here: 239 us
  blocking collectives  128 us (53%)
  starting transfers between devices  47.1 us (20%)
  waiting for transfers between devices  37.2 us (16%)
  Pallas kernels  17.3 us (7%)
  local copies, waits for them, and re-layouts  6.4 us (3%)
    all_to_all x9, blocking collectives, exchange(): return lax.all_to_all(x, axis, 0, 0, tiled=True)  128 us
    all_to_all x3, starting transfers between devices, exchange(): return lax.all_to_all(x, axis, 0, 0, tiled=True)  27.2 us
    ppermute x2, waiting for transfers between devices, swap_chips(): return lax.ppermute(x, 'za', [(0, 1), (1, 0)])  25.9 us
    pallas_call x16, Pallas kernels, kernel(): pl.pallas_call(functools.partial(fn, **static), out_shape=shapes, in_spec...  17.3 us
    ppermute x3, starting transfers between devices, swap(): return lax.ppermute(x, 'c', [(0, 1), (1, 0)])  13.6 us
    all_to_all x3, waiting for transfers between devices, exchange(): return lax.all_to_all(x, axis, 0, 0, tiled=True)  11.4 us
    ppermute x2, starting transfers between devices, swap_chips(): return lax.ppermute(x, 'za', [(0, 1), (1, 0)])  6.34 us
    unnamed x58, local copies, waits for them, and re-layouts  5.53 us
  transfers between devices with their start and end apart: 8, of which 4 were waited for; matrix products, arithmetic and copies ran while one was open for 1% of the time, Pallas kernels for 3%

profile of v8, /device:TPU:1, one launch (start us, length us, event | category | flops | bytes accessed | tf_op | source)
XLA Modules:
  0.0 238.5 jit_solution(11036776104391507767)
XLA Ops:
  1.9 8.7 %collective-permute-start = (bf16[128,1280]{1,0:T(8,128)(2,1)S(1)}, bf16[128,1280]{1,0:T(8,128)(2,1)S(1)}, u32[]{:S(2)}, u32[]{:S(2)}) collective-permute-start(bf16[128,1280]{1,0:T(8,128)(2,1)S(1)} %shard_map.254.weights), channel_id=1, source_target_pairs={{0,16},{16,0},{1,17},{17,1},{2,18},{18,2},{3,19},{19,3},{4,20},{20... | collective-permute-start | bytes 983048 | tf_op jit(solution)/shard_map/ppermute | solution.py:346
  11.3 3.6 %all-to-all-start = ((bf16[32,8,256]{2,1,0:T(8,128)(2,1)}), bf16[32,8,256]{2,1,0:T(8,128)(2,1)S(1)}, u32[]{:S(2)}, u32[]{:S(2)}) async-start(bf16[32,8,256]{2,1,0:T(8,128)(2,1)} %bitcast.6), calls=%async_computation | async-start | bytes 262144 | tf_op jit(solution)/shard_map/all_to_all | solution.py:342
  15.0 7.4 %all-to-all-done = bf16[32,8,256]{2,1,0:T(8,128)(2,1)S(1)} async-done(((bf16[32,8,256]{2,1,0:T(8,128)(2,1)}), bf16[32,8,256]{2,1,0:T(8,128)(2,1)S(1)}, u32[]{:S(2)}, u32[]{:S(2)}) %all-to-all-start) | async-done | bytes 131104 | tf_op jit(solution)/shard_map/all_to_all | solution.py:342
  22.5 1.6 shard_map.255
  24.1 13.3 %all-to-all-start.1 = ((bf16[16,8,1408]{2,1,0:T(8,128)(2,1)}), bf16[16,8,1408]{2,1,0:T(8,128)(2,1)S(1)}, u32[]{:S(2)}, u32[]{:S(2)}) async-start(bf16[16,8,1408]{2,1,0:T(8,128)(2,1)} %shard_map.255), calls=%async_computation.1 | async-start | bytes 720896 | tf_op jit(solution)/shard_map/all_to_all | solution.py:342
  40.7 6.4 %shard_map.256 = (f32[8,128,128]{2,1,0:T(8,128)S(1)}, f32[8,128]{1,0:T(8,128)S(1)}, f32[8,128]{1,0:T(8,128)S(1)}) custom-call(s32[8]{0:T(128)S(1)} %copy-done.25, f32[2]{0:T(128)S(1)} %pad_maximum_fusion.1.head, f32[8,128,128]{2,1,0:T(8,128)S(1)} %bitcast.39, bf16[8,64,128]{2,1,0:T(8,128)(2,1)S(1)} %copy-done.20, bf16[8,64,128]{2,1,0:T(8,128)(2,1)S(1)} %copy-done.21, ...), custom_call_target="tpu_custom_call" | custom-call | flops 268435456 | bytes 793128 | tf_op jit(solution)/shard_map/pallas_call | solution.py:24
  47.9 3.3 %collective-permute-start.2 = (bf16[128,3328]{1,0:T(8,128)(2,1)S(1)}, bf16[128,3328]{1,0:T(8,128)(2,1)S(1)}, u32[]{:S(2)}, u32[]{:S(2)}) collective-permute-start(bf16[128,3328]{1,0:T(8,128)(2,1)S(1)} %shard_map.257.refs_0_), channel_id=1, source_target_pairs={{0,32},{32,0},{1,33},{33,1},{2,34},{34,2},{3,35},{35,3},{4,36},{36... | collective-permute-start | bytes 2555912 | tf_op jit(solution)/shard_map/ppermute | solution.py:350
  52.6 20.8 %collective-permute-done.2.refs_2_ = bf16[128,3328]{1,0:T(8,128)(2,1)S(1)} collective-permute-done((bf16[128,3328]{1,0:T(8,128)(2,1)S(1)}, bf16[128,3328]{1,0:T(8,128)(2,1)S(1)}, u32[]{:S(2)}, u32[]{:S(2)}) %collective-permute-start.2) | collective-permute-done | bytes 852000 | tf_op jit(solution)/shard_map/ppermute | solution.py:350
  73.4 2.9 %collective-permute-start.3 = (bf16[128,3328]{1,0:T(8,128)(2,1)S(1)}, bf16[128,3328]{1,0:T(8,128)(2,1)S(1)}, u32[]{:S(2)}, u32[]{:S(2)}) collective-permute-start(bf16[128,3328]{1,0:T(8,128)(2,1)S(1)} %collective-permute-done.2.refs_2_), channel_id=1, source_target_pairs={{0,16},{16,0},{1,17},{17,1},{2,18},{18,2},{3,19},{19,3},{4,20},{20... | collective-permute-start | bytes 2555912 | tf_op jit(solution)/shard_map/ppermute | solution.py:346
  77.1 1.9 collective-permute-start.1
  79.1 10.2 %all-to-all-start.2 = ((bf16[8,8,640]{2,1,0:T(8,128)(2,1)}), bf16[8,8,640]{2,1,0:T(8,128)(2,1)}, u32[]{:S(2)}, u32[]{:S(2)}) async-start(bf16[8,8,640]{2,1,0:T(8,128)(2,1)} %copy-done.2), calls=%async_computation.2 | async-start | bytes 163840 | tf_op jit(solution)/shard_map/all_to_all | solution.py:342
  89.3 3.1 %collective-permute-start.4 = (bf16[2,16,8,256]{3,2,1,0:T(8,128)(2,1)S(1)}, bf16[2,16,8,256]{3,2,1,0:T(8,128)(2,1)S(1)}, u32[]{:S(2)}, u32[]{:S(2)}) collective-permute-start(bf16[2,16,8,256]{3,2,1,0:T(8,128)(2,1)S(1)} %bitcast.28), channel_id=1, source_target_pairs={{0,32},{32,0},{1,33},{33,1},{2,34},{34,2},{3,35},{35,3},{4,36},{36... | collective-permute-start | bytes 393224 | tf_op jit(solution)/shard_map/ppermute | solution.py:350
  92.4 5.0 %collective-permute-done.4.got_z = bf16[2,16,8,256]{3,2,1,0:T(8,128)(2,1)S(1)} collective-permute-done((bf16[2,16,8,256]{3,2,1,0:T(8,128)(2,1)S(1)}, bf16[2,16,8,256]{3,2,1,0:T(8,128)(2,1)S(1)}, u32[]{:S(2)}, u32[]{:S(2)}) %collective-permute-start.4) | collective-permute-done | bytes 131104 | tf_op jit(solution)/shard_map/ppermute | solution.py:350
  98.1 3.9 %all-to-all-done.2.hidden = bf16[8,8,640]{2,1,0:T(8,128)(2,1)} async-done(((bf16[8,8,640]{2,1,0:T(8,128)(2,1)}), bf16[8,8,640]{2,1,0:T(8,128)(2,1)}, u32[]{:S(2)}, u32[]{:S(2)}) %all-to-all-start.2) | async-done | bytes 81952 | tf_op jit(solution)/shard_map/all_to_all | solution.py:342
  103.2 9.6 %all_to_all.60.parts = bf16[16,8,256]{2,1,0:T(8,128)(2,1)S(1)} all-to-all(bf16[16,8,256]{2,1,0:T(8,128)(2,1)S(1)} %bitcast.37), channel_id=1, replica_groups=mesh['zh'=8,'za'=2,'c'=2,'tp'=16] {'tp'}, dimensions={0} | all-to-all | bytes 131072 | tf_op jit(solution)/shard_map/all_to_all | solution.py:342
  113.4 9.4 %all_to_all.61 = bf16[16,8,256]{2,1,0:T(8,128)(2,1)S(1)} all-to-all(bf16[16,8,256]{2,1,0:T(8,128)(2,1)S(1)} %shard_map.260), channel_id=1, replica_groups=mesh['zh'=8,'za'=2,'c'=2,'tp'=16] {'tp'}, dimensions={0} | all-to-all | bytes 131072 | tf_op jit(solution)/shard_map/all_to_all | solution.py:342
  123.7 19.7 %all_to_all.62.parts = bf16[8,8,640]{2,1,0:T(8,128)(2,1)S(1)} all-to-all(bf16[8,8,640]{2,1,0:T(8,128)(2,1)S(1)} %shard_map.261), channel_id=1, replica_groups=mesh['zh'=8,'za'=2,'c'=2,'tp'=16] {'zh'}, dimensions={0} | all-to-all | bytes 163840 | tf_op jit(solution)/shard_map/all_to_all | solution.py:342
  143.4 1.3 shard_map.262
  144.8 13.8 %all_to_all.63.mixed = bf16[8,8,128]{2,1,0:T(8,128)(2,1)S(1)} all-to-all(bf16[8,8,128]{2,1,0:T(8,128)(2,1)S(1)} %shard_map.262), channel_id=1, replica_groups=mesh['zh'=8,'za'=2,'c'=2,'tp'=16] {'zh'}, dimensions={0} | all-to-all | bytes 32768 | tf_op jit(solution)/shard_map/all_to_all | solution.py:342
  159.2 9.6 %all_to_all.64.parts = bf16[16,8,256]{2,1,0:T(8,128)(2,1)S(1)} all-to-all(bf16[16,8,256]{2,1,0:T(8,128)(2,1)S(1)} %bitcast.36), channel_id=1, replica_groups=mesh['zh'=8,'za'=2,'c'=2,'tp'=16] {'tp'}, dimensions={0} | all-to-all | bytes 131072 | tf_op jit(solution)/shard_map/all_to_all | solution.py:342
  169.4 9.4 %all_to_all.65 = bf16[16,8,256]{2,1,0:T(8,128)(2,1)S(1)} all-to-all(bf16[16,8,256]{2,1,0:T(8,128)(2,1)S(1)} %shard_map.264), channel_id=1, replica_groups=mesh['zh'=8,'za'=2,'c'=2,'tp'=16] {'tp'}, dimensions={0} | all-to-all | bytes 131072 | tf_op jit(solution)/shard_map/all_to_all | solution.py:342
  179.7 16.5 %all_to_all.66.parts = bf16[8,8,1408]{2,1,0:T(8,128)(2,1)S(1)} all-to-all(bf16[8,8,1408]{2,1,0:T(8,128)(2,1)S(1)} %shard_map.265), channel_id=1, replica_groups=mesh['zh'=8,'za'=2,'c'=2,'tp'=16] {'zh'}, dimensions={0} | all-to-all | bytes 360448 | tf_op jit(solution)/shard_map/all_to_all | solution.py:342
  196.4 14.8 %all_to_all.67.hidden = bf16[8,8,640]{2,1,0:T(8,128)(2,1)S(1)} all-to-all(bf16[8,8,640]{2,1,0:T(8,128)(2,1)S(1)} %shard_map.266), channel_id=1, replica_groups=mesh['zh'=8,'za'=2,'c'=2,'tp'=16] {'zh'}, dimensions={0} | all-to-all | bytes 163840 | tf_op jit(solution)/shard_map/all_to_all | solution.py:342
  212.1 25.3 %all_to_all.68 = bf16[64,8,256]{2,1,0:T(8,128)(2,1)S(1)} all-to-all(bf16[64,8,256]{2,1,0:T(8,128)(2,1)S(1)} %bitcast.30), channel_id=1, replica_groups=mesh['zh'=8,'za'=2,'c'=2,'tp'=16] {'za','c','tp'}, dimensions={0} | all-to-all | bytes 524288 | tf_op jit(solution)/shard_map/all_to_all | solution.py:342
  (84 shorter events, 15.1 us)
Async XLA Ops:
  1.8 8.8 %copy-start.17 = (bf16[16,128]{1,0:T(8,128)(2,1)S(1)}, bf16[16,128]{1,0:T(8,128)(2,1)}, u32[]{:S(2)}) copy-start(bf16[16,128]{1,0:T(8,128)(2,1)} %tokens.1) | copy-start | bytes 12292
  1.9 8.8 %copy-start.18 = (f32[128]{0:T(128)S(1)}, f32[128]{0:T(128)}, u32[]{:S(2)}) copy-start(f32[128]{0:T(128)} %param.28) | copy-start | bytes 1540
  1.9 20.6 %collective-permute-start = (bf16[128,1280]{1,0:T(8,128)(2,1)S(1)}, bf16[128,1280]{1,0:T(8,128)(2,1)S(1)}, u32[]{:S(2)}, u32[]{:S(2)}) collective-permute-start(bf16[128,1280]{1,0:T(8,128)(2,1)S(1)} %shard_map.254.weights), channel_id=1, source_target_pairs={{0,16},{16,0},{1,17},{17,1},{2,18},{18,2},{3,19},{19,3},{4,20},{20... | collective-permute-start | bytes 983048 | tf_op jit(solution)/shard_map/ppermute | solution.py:346
  11.3 11.2 %all-to-all-start = ((bf16[32,8,256]{2,1,0:T(8,128)(2,1)}), bf16[32,8,256]{2,1,0:T(8,128)(2,1)S(1)}, u32[]{:S(2)}, u32[]{:S(2)}) async-start(bf16[32,8,256]{2,1,0:T(8,128)(2,1)} %bitcast.6), calls=%async_computation | async-start | bytes 262144 | tf_op jit(solution)/shard_map/all_to_all | solution.py:342
  22.5 17.0 %copy-start.14 = (bf16[128,128]{1,0:T(8,128)(2,1)S(1)}, bf16[128,128]{1,0:T(8,128)(2,1)}, u32[]{:S(2)}) copy-start(bf16[128,128]{1,0:T(8,128)(2,1)} %value) | copy-start | bytes 98308
  22.5 17.0 %copy-start.15 = (bf16[128,128]{1,0:T(8,128)(2,1)S(1)}, bf16[128,128]{1,0:T(8,128)(2,1)}, u32[]{:S(2)}) copy-start(bf16[128,128]{1,0:T(8,128)(2,1)} %outer) | copy-start | bytes 98308
  22.5 17.0 %copy-start.16 = (bf16[128,128]{1,0:T(8,128)(2,1)S(1)}, bf16[128,128]{1,0:T(8,128)(2,1)}, u32[]{:S(2)}) copy-start(bf16[128,128]{1,0:T(8,128)(2,1)} %mixer_out) | copy-start | bytes 98308
  24.1 15.4 %copy-start.5 = (bf16[128,640]{1,0:T(8,128)(2,1)S(1)}, bf16[128,640]{1,0:T(8,128)(2,1)}, u32[]{:S(2)}) copy-start(bf16[128,640]{1,0:T(8,128)(2,1)} %gate.2) | copy-start | bytes 491524
  24.1 15.4 %copy-start.6 = (bf16[128,640]{1,0:T(8,128)(2,1)S(1)}, bf16[128,640]{1,0:T(8,128)(2,1)}, u32[]{:S(2)}) copy-start(bf16[128,640]{1,0:T(8,128)(2,1)} %up.2) | copy-start | bytes 491524
  24.1 15.4 %copy-start.7 = (bf16[640,128]{1,0:T(8,128)(2,1)S(1)}, bf16[640,128]{1,0:T(8,128)(2,1)}, u32[]{:S(2)}) copy-start(bf16[640,128]{1,0:T(8,128)(2,1)} %down) | copy-start | bytes 491524
  24.1 15.4 %copy-start.8 = (bf16[640,128]{1,0:T(8,128)(2,1)S(1)}, bf16[640,128]{1,0:T(8,128)(2,1)}, u32[]{:S(2)}) copy-start(bf16[640,128]{1,0:T(8,128)(2,1)} %first) | copy-start | bytes 491524
  24.1 15.4 %copy-start.12 = (bf16[128,128]{1,0:T(8,128)(2,1)S(1)}, bf16[128,128]{1,0:T(8,128)(2,1)}, u32[]{:S(2)}) copy-start(bf16[128,128]{1,0:T(8,128)(2,1)} %query) | copy-start | bytes 98308
  24.1 15.4 %copy-start.13 = (bf16[128,128]{1,0:T(8,128)(2,1)S(1)}, bf16[128,128]{1,0:T(8,128)(2,1)}, u32[]{:S(2)}) copy-start(bf16[128,128]{1,0:T(8,128)(2,1)} %key) | copy-start | bytes 98308
  24.1 52.2 %all-to-all-start.1 = ((bf16[16,8,1408]{2,1,0:T(8,128)(2,1)}), bf16[16,8,1408]{2,1,0:T(8,128)(2,1)S(1)}, u32[]{:S(2)}, u32[]{:S(2)}) async-start(bf16[16,8,1408]{2,1,0:T(8,128)(2,1)} %shard_map.255), calls=%async_computation.1 | async-start | bytes 720896 | tf_op jit(solution)/shard_map/all_to_all | solution.py:342
  39.6 1.1 copy-start.21
  39.6 1.1 copy-start.24
  47.9 25.5 %collective-permute-start.2 = (bf16[128,3328]{1,0:T(8,128)(2,1)S(1)}, bf16[128,3328]{1,0:T(8,128)(2,1)S(1)}, u32[]{:S(2)}, u32[]{:S(2)}) collective-permute-start(bf16[128,3328]{1,0:T(8,128)(2,1)S(1)} %shard_map.257.refs_0_), channel_id=1, source_target_pairs={{0,32},{32,0},{1,33},{33,1},{2,34},{34,2},{3,35},{35,3},{4,36},{36... | collective-permute-start | bytes 2555912 | tf_op jit(solution)/shard_map/ppermute | solution.py:350
  73.4 28.6 %collective-permute-start.3 = (bf16[128,3328]{1,0:T(8,128)(2,1)S(1)}, bf16[128,3328]{1,0:T(8,128)(2,1)S(1)}, u32[]{:S(2)}, u32[]{:S(2)}) collective-permute-start(bf16[128,3328]{1,0:T(8,128)(2,1)S(1)} %collective-permute-done.2.refs_2_), channel_id=1, source_target_pairs={{0,16},{16,0},{1,17},{17,1},{2,18},{18,2},{3,19},{19,3},{4,20},{20... | collective-permute-start | bytes 2555912 | tf_op jit(solution)/shard_map/ppermute | solution.py:346
  77.1 24.9 %collective-permute-start.1 = (bf16[128,3328]{1,0:T(8,128)(2,1)S(1)}, bf16[128,3328]{1,0:T(8,128)(2,1)S(1)}, u32[]{:S(2)}, u32[]{:S(2)}) collective-permute-start(bf16[128,3328]{1,0:T(8,128)(2,1)S(1)} %shard_map.257.refs_0_), channel_id=1, source_target_pairs={{0,16},{16,0},{1,17},{17,1},{2,18},{18,2},{3,19},{19,3},{4,20},{20... | collective-permute-start | bytes 2555912 | tf_op jit(solution)/shard_map/ppermute | solution.py:346
  79.1 23.0 %all-to-all-start.2 = ((bf16[8,8,640]{2,1,0:T(8,128)(2,1)}), bf16[8,8,640]{2,1,0:T(8,128)(2,1)}, u32[]{:S(2)}, u32[]{:S(2)}) async-start(bf16[8,8,640]{2,1,0:T(8,128)(2,1)} %copy-done.2), calls=%async_computation.2 | async-start | bytes 163840 | tf_op jit(solution)/shard_map/all_to_all | solution.py:342
  89.3 8.1 %collective-permute-start.4 = (bf16[2,16,8,256]{3,2,1,0:T(8,128)(2,1)S(1)}, bf16[2,16,8,256]{3,2,1,0:T(8,128)(2,1)S(1)}, u32[]{:S(2)}, u32[]{:S(2)}) collective-permute-start(bf16[2,16,8,256]{3,2,1,0:T(8,128)(2,1)S(1)} %bitcast.28), channel_id=1, source_target_pairs={{0,32},{32,0},{1,33},{33,1},{2,34},{34,2},{3,35},{35,3},{4,36},{36... | collective-permute-start | bytes 393224 | tf_op jit(solution)/shard_map/ppermute | solution.py:350
  103.2 9.6 %copy-start.11 = (bf16[2,16,8,256]{3,2,1,0:T(8,128)(2,1)S(1)}, bf16[2,16,8,256]{3,2,1,0:T(8,128)(2,1)}, u32[]{:S(2)}) copy-start(bf16[2,16,8,256]{3,2,1,0:T(8,128)(2,1)} %copy-done.10) | copy-start | bytes 393220
  113.4 9.4 %copy-start.9 = (bf16[2,4,16,128]{3,2,1,0:T(8,128)(2,1)S(1)}, bf16[2,4,16,128]{3,2,1,0:T(8,128)(2,1)}, u32[]{:S(2)}) copy-start(bf16[2,4,16,128]{3,2,1,0:T(8,128)(2,1)} %maximum_bitcast_fusion.logits) | copy-start | bytes 98308
  122.8 20.6 %copy-start.1 = (f32[8,128,128]{2,1,0:T(8,128)S(1)}, f32[8,128,128]{2,1,0:T(8,128)}, u32[]{:S(2)}) copy-start(f32[8,128,128]{2,1,0:T(8,128)} %copy-done) | copy-start | bytes 1572868
  (13 other events, 11.0 us)

commit v9 on v8

--- a/solution.py
+++ b/solution.py
@@ -91,13 +91,17 @@
     out[:, n:] = up[...]
 
 
-def pack(gate, up, down, first, query, key, value, outer, mixer_out, gains, out):
-    n = gate.shape[1]
-    down = [w[i : i + LANES] for w in (down, first) for i in range(0, n, LANES)]
-    at = 0
-    for part in (gate, up, *down, query, key, value, outer, mixer_out):
-        out[:, at : at + part.shape[1]] = part[...]
-        at += part.shape[1]
+def lay(parts, out):
+    rows, at = out.shape[0], 0
+    for part in parts:
+        for i in range(0, part.shape[0], rows):
+            out[:, at : at + part.shape[1]] = part[i : i + rows]
+            at += part.shape[1]
+    return at
+
+
+def pack(down, query, key, value, outer, mixer_out, gains, out):
+    at = lay((down, query, key, value, outer, mixer_out), out)
     row = lax.broadcasted_iota(jnp.int32, (out.shape[0], LANES), 0)
     tile = jnp.zeros(row.shape, f32)
     for which in range(2):
@@ -109,6 +113,10 @@
     out[:, at:] = tile.astype(bf16)
 
 
+def pack_second(gate, up, down, out):
+    lay((gate, up, down), out)
+
+
 def packed_gain(packed, which):
     tile = packed[0:16, packed.shape[1] - LANES :].astype(f32)
     at = 3 * which
@@ -151,10 +159,10 @@
 
 
 def second_products(ids, second, *refs):
-    out, packs = refs[-1], refs[:-1]
+    out, packs, weights = refs[-1], refs[:4], refs[4:8]
     raw = slices(ids, lambda chip: second[:, chip])
     scaled = [(x * packed_gain(p, 1)).astype(bf16) for x, p in zip(raw, packs)]
-    gate_up(scaled, packs, row_sum(raw), out)
+    gate_up(scaled, weights, row_sum(raw), out)
 
 
 def activate(parts, out, *, features):
@@ -178,7 +186,7 @@
     rows = flat(hidden[...]).astype(bf16)
     for i, ((chip, _), packed) in enumerate(zip(order(ids), refs[:-1])):
         at = i % 2 * LANES
-        part = down_product(rows, packed, 3 * rows.shape[1])
+        part = down_product(rows, packed, 0)
         out[:, chip, :, at : at + LANES] = blocked(part, out.shape[0]).astype(bf16)
 
 
@@ -449,8 +457,7 @@
     )
     packed = kernel(
         pack,
-        ((width, 4 * hidden_units + 4 * dk + width + LANES), bf16),
-        *branch,
+        ((width, hidden_units + 4 * dk + width + LANES), bf16),
         down,
         *heads,
         outer[0],
@@ -462,27 +469,29 @@
     start = lax.axis_index("zh") * 4 * width
     logits = [lax.dynamic_slice_in_dim(w.T, start, 4 * width, 1) for w in logits]
     logits = jnp.stack(logits).reshape(2, -1, 4, width).transpose(0, 2, 1, 3)
-    parts, logits, state, new_extra, norm_gain, packed = together(
-        parts, logits, state, new_extra, norm_gain, packed
+    parts, logits, state, new_extra, norm_gain, packed, branch = together(
+        parts, logits, state, new_extra, norm_gain, packed, branch
     )
 
     hidden = kernel(activate, ((half, rows, hidden_units), bf16), parts, features=features)
-    hidden, packed = together(hidden, packed)
+    hidden, packed, branch = together(hidden, packed, branch)
     hidden = exchange(hidden, "zh")
+    later = kernel(pack_second, ((width, 3 * hidden_units), bf16), *branch)
     packed_x = swap(packed)
     packed_zx = swap(packed_z)
-    hidden, packed_x, packed_z, packed_zx, got_z = together(
-        hidden, packed_x, packed_z, packed_zx, got_z
+    later_x = swap(later)
+    hidden, packed_x, packed_z, packed_zx, got_z, later, later_x = together(
+        hidden, packed_x, packed_z, packed_zx, got_z, later, later_x
     )
     packs = (packed, packed_x, packed_z, packed_zx)
 
     parts = kernel(
         first_down, ((plane // 2, 2, rows, 2 * width), bf16), ids, hidden, *packs, scalars=1
     )
+    parts, later = together(parts, later)
     parts = exchange(parts.reshape(plane, rows, 2 * width), "tp")
-    middle = kernel(
-        add_first, ((plane, rows, 2 * width), bf16), ids, parts, got, got_z, scalars=1
-    )
+    later_z = swap_chips(later)
+    middle = kernel(add_first, ((plane, rows, 2 * width), bf16), ids, parts, got, got_z, scalars=1)
     middle = exchange(middle, "tp").reshape(plane // 2, 2, rows, 2 * width)
 
     parts = kernel(
@@ -510,7 +519,11 @@
     parts = kernel(
         mixer_down, ((plane // 2, 2, rows, 2 * width), bf16), ids, mixed, *packs, scalars=1
     )
+    parts, later_z = together(parts, later_z)
     parts = exchange(parts.reshape(plane, rows, 2 * width), "tp")
+    later_zx = swap(later_z)
+    parts, later_zx = together(parts, later_zx)
+    laters = (later, later_x, later_z, later_zx)
     second = kernel(add_mixer, ((plane, rows, 2 * width), bf16), ids, parts, middle, scalars=1)
     second = exchange(second, "tp").reshape(plane // 2, 2, rows, 2 * width)
 
@@ -520,6 +533,7 @@
         ids,
         second,
         *packs,
+        *laters,
         scalars=1,
     )
     parts = exchange(sent, "zh")
@@ -531,7 +545,7 @@
         ids,
         hidden,
         second,
-        *packs,
+        *laters,
         scalars=1,
     )
     parts = exchange(parts.reshape(4 * plane, rows, 2 * width), ("za", "c", "tp"))

time: 240 us -> 233 us (0.971)
  starting transfers between devices: 47.1 us -> 66.5 us
  waiting for transfers between devices: 37.2 us -> 20.4 us
  blocking collectives: 128 us -> 122 us
  local copies, waits for them, and re-layouts: 6.4 us -> 3.72 us
    ppermute x2 -> x3, waiting for transfers between devices: 25.9 us -> 4.96 us  [swap_chips(): return lax.ppermute(x, 'za', [(0, 1), (1, 0)])]
    ppermute x3 -> x5, starting transfers between devices: 13.6 us -> 30.6 us  [swap(): return lax.ppermute(x, 'c', [(0, 1), (1, 0)])]
    all_to_all x9, blocking collectives: 128 us -> 122 us  [exchange(): return lax.all_to_all(x, axis, 0, 0, tiled=True)]
    all_to_all x3, waiting for transfers between devices: 11.4 us -> 15.4 us  [exchange(): return lax.all_to_all(x, axis, 0, 0, tiled=True)]
    ppermute x2 -> x3, starting transfers between devices: 6.34 us -> 9.27 us  [swap_chips(): return lax.ppermute(x, 'za', [(0, 1), (1, 0)])]
    unnamed x58 -> x46, local copies, waits for them, and re-layouts: 5.53 us -> 2.85 us
    pallas_call x16 -> x17, Pallas kernels: 17.3 us -> 17.6 us  [kernel(): pl.pallas_call(functools.partial(fn, **static), out_shape=shapes, in_spec...]
  transfers between devices with their start and end apart: 8 -> 11, of which waited for: 4 -> 4; matrix products, arithmetic and copies ran while one was open for 1% -> 0% of each run, Pallas kernels for 3% -> 5%
where the time goes in v9:
time: 233 us; the launch traced here: 232 us
  blocking collectives  122 us (52%)
  starting transfers between devices  66.5 us (29%)
  waiting for transfers between devices  20.4 us (9%)
  Pallas kernels  17.6 us (8%)
  local copies, waits for them, and re-layouts  3.72 us (2%)
    all_to_all x9, blocking collectives, exchange(): return lax.all_to_all(x, axis, 0, 0, tiled=True)  122 us
    ppermute x5, starting transfers between devices, swap(): return lax.ppermute(x, 'c', [(0, 1), (1, 0)])  30.6 us
    all_to_all x3, starting transfers between devices, exchange(): return lax.all_to_all(x, axis, 0, 0, tiled=True)  26.7 us
    pallas_call x17, Pallas kernels, kernel(): pl.pallas_call(functools.partial(fn, **static), out_shape=shapes, in_spec...  17.6 us
    all_to_all x3, waiting for transfers between devices, exchange(): return lax.all_to_all(x, axis, 0, 0, tiled=True)  15.4 us
    ppermute x3, starting transfers between devices, swap_chips(): return lax.ppermute(x, 'za', [(0, 1), (1, 0)])  9.27 us
    ppermute x3, waiting for transfers between devices, swap_chips(): return lax.ppermute(x, 'za', [(0, 1), (1, 0)])  4.96 us
  transfers between devices with their start and end apart: 11, of which 4 were waited for; matrix products, arithmetic and copies ran while one was open for 0% of the time, Pallas kernels for 5%

profile of v9, /device:TPU:1, one launch (start us, length us, event | category | flops | bytes accessed | tf_op | source)
XLA Modules:
  0.0 231.7 jit_solution(5805491340264630071)
XLA Ops:
  1.9 8.7 %collective-permute-start = (bf16[128,1280]{1,0:T(8,128)(2,1)S(1)}, bf16[128,1280]{1,0:T(8,128)(2,1)S(1)}, u32[]{:S(2)}, u32[]{:S(2)}) collective-permute-start(bf16[128,1280]{1,0:T(8,128)(2,1)S(1)} %shard_map.254.weights), channel_id=1, source_target_pairs={{0,16},{16,0},{1,17},{17,1},{2,18},{18,2},{3,19},{19,3},{4,20},{20... | collective-permute-start | bytes 983048 | tf_op jit(solution)/shard_map/ppermute | solution.py:354
  11.3 3.6 %all-to-all-start = ((bf16[32,8,256]{2,1,0:T(8,128)(2,1)}), bf16[32,8,256]{2,1,0:T(8,128)(2,1)S(1)}, u32[]{:S(2)}, u32[]{:S(2)}) async-start(bf16[32,8,256]{2,1,0:T(8,128)(2,1)} %bitcast.6), calls=%async_computation | async-start | bytes 262144 | tf_op jit(solution)/shard_map/all_to_all | solution.py:350
  15.1 7.4 %all-to-all-done = bf16[32,8,256]{2,1,0:T(8,128)(2,1)S(1)} async-done(((bf16[32,8,256]{2,1,0:T(8,128)(2,1)}), bf16[32,8,256]{2,1,0:T(8,128)(2,1)S(1)}, u32[]{:S(2)}, u32[]{:S(2)}) %all-to-all-start) | async-done | bytes 131104 | tf_op jit(solution)/shard_map/all_to_all | solution.py:350
  24.1 13.3 %all-to-all-start.1 = ((bf16[16,8,1408]{2,1,0:T(8,128)(2,1)}), bf16[16,8,1408]{2,1,0:T(8,128)(2,1)S(1)}, u32[]{:S(2)}, u32[]{:S(2)}) async-start(bf16[16,8,1408]{2,1,0:T(8,128)(2,1)} %shard_map.255), calls=%async_computation.1 | async-start | bytes 720896 | tf_op jit(solution)/shard_map/all_to_all | solution.py:350
  39.9 6.4 %shard_map.256 = (f32[8,128,128]{2,1,0:T(8,128)S(1)}, f32[8,128]{1,0:T(8,128)S(1)}, f32[8,128]{1,0:T(8,128)S(1)}) custom-call(s32[8]{0:T(128)S(1)} %copy-done.19, f32[2]{0:T(128)S(1)} %pad_maximum_fusion.1.head, f32[8,128,128]{2,1,0:T(8,128)S(1)} %bitcast.39, bf16[8,64,128]{2,1,0:T(8,128)(2,1)S(1)} %copy-done.14, bf16[8,64,128]{2,1,0:T(8,128)(2,1)S(1)} %copy-done.15, ...), custom_call_target="tpu_custom_call" | custom-call | flops 268435456 | bytes 793128 | tf_op jit(solution)/shard_map/pallas_call | solution.py:24
  46.3 3.3 %collective-permute-start.2 = (bf16[128,1408]{1,0:T(8,128)(2,1)S(1)}, bf16[128,1408]{1,0:T(8,128)(2,1)S(1)}, u32[]{:S(2)}, u32[]{:S(2)}) collective-permute-start(bf16[128,1408]{1,0:T(8,128)(2,1)S(1)} %shard_map.257.refs_0_), channel_id=1, source_target_pairs={{0,32},{32,0},{1,33},{33,1},{2,34},{34,2},{3,35},{35,3},{4,36},{36... | collective-permute-start | bytes 1081352 | tf_op jit(solution)/shard_map/ppermute | solution.py:358
  50.4 3.5 %all-to-all-done.1.parts = bf16[16,8,1408]{2,1,0:T(8,128)(2,1)S(1)} async-done(((bf16[16,8,1408]{2,1,0:T(8,128)(2,1)}), bf16[16,8,1408]{2,1,0:T(8,128)(2,1)S(1)}, u32[]{:S(2)}, u32[]{:S(2)}) %all-to-all-start.1) | async-done | bytes 360480 | tf_op jit(solution)/shard_map/all_to_all | solution.py:350
  54.9 9.0 %collective-permute-start.5 = (bf16[128,1920]{1,0:T(8,128)(2,1)S(1)}, bf16[128,1920]{1,0:T(8,128)(2,1)S(1)}, u32[]{:S(2)}, u32[]{:S(2)}) collective-permute-start(bf16[128,1920]{1,0:T(8,128)(2,1)S(1)} %shard_map.259.refs_4_.refs_0_), channel_id=1, source_target_pairs={{0,16},{16,0},{1,17},{17,1},{2,18},{18,2},{3,19},{19,3},{4,20},{20... | collective-permute-start | bytes 1474568 | tf_op jit(solution)/shard_map/ppermute | solution.py:354
  65.8 2.4 %collective-permute-start.1 = (bf16[128,1408]{1,0:T(8,128)(2,1)S(1)}, bf16[128,1408]{1,0:T(8,128)(2,1)S(1)}, u32[]{:S(2)}, u32[]{:S(2)}) collective-permute-start(bf16[128,1408]{1,0:T(8,128)(2,1)S(1)} %shard_map.257.refs_0_), channel_id=1, source_target_pairs={{0,16},{16,0},{1,17},{17,1},{2,18},{18,2},{3,19},{19,3},{4,20},{20... | collective-permute-start | bytes 1081352 | tf_op jit(solution)/shard_map/ppermute | solution.py:354
  68.2 9.7 %all-to-all-start.2 = ((bf16[8,8,640]{2,1,0:T(8,128)(2,1)}), bf16[8,8,640]{2,1,0:T(8,128)(2,1)S(1)}, u32[]{:S(2)}, u32[]{:S(2)}) async-start(bf16[8,8,640]{2,1,0:T(8,128)(2,1)} %shard_map.258), calls=%async_computation.2 | async-start | bytes 163840 | tf_op jit(solution)/shard_map/all_to_all | solution.py:350
  77.9 3.1 %collective-permute-start.4 = (bf16[2,16,8,256]{3,2,1,0:T(8,128)(2,1)S(1)}, bf16[2,16,8,256]{3,2,1,0:T(8,128)(2,1)S(1)}, u32[]{:S(2)}, u32[]{:S(2)}) collective-permute-start(bf16[2,16,8,256]{3,2,1,0:T(8,128)(2,1)S(1)} %bitcast.28), channel_id=1, source_target_pairs={{0,32},{32,0},{1,33},{33,1},{2,34},{34,2},{3,35},{35,3},{4,36},{36... | collective-permute-start | bytes 393224 | tf_op jit(solution)/shard_map/ppermute | solution.py:358
  81.0 4.9 %collective-permute-done.4.got_z = bf16[2,16,8,256]{3,2,1,0:T(8,128)(2,1)S(1)} collective-permute-done((bf16[2,16,8,256]{3,2,1,0:T(8,128)(2,1)S(1)}, bf16[2,16,8,256]{3,2,1,0:T(8,128)(2,1)S(1)}, u32[]{:S(2)}, u32[]{:S(2)}) %collective-permute-start.4) | collective-permute-done | bytes 131104 | tf_op jit(solution)/shard_map/ppermute | solution.py:358
  86.0 4.6 %all-to-all-done.2.hidden = bf16[8,8,640]{2,1,0:T(8,128)(2,1)S(1)} async-done(((bf16[8,8,640]{2,1,0:T(8,128)(2,1)}), bf16[8,8,640]{2,1,0:T(8,128)(2,1)S(1)}, u32[]{:S(2)}, u32[]{:S(2)}) %all-to-all-start.2) | async-done | bytes 81952 | tf_op jit(solution)/shard_map/all_to_all | solution.py:350
  91.4 2.9 %collective-permute-start.6 = (bf16[128,1920]{1,0:T(8,128)(2,1)S(1)}, bf16[128,1920]{1,0:T(8,128)(2,1)S(1)}, u32[]{:S(2)}, u32[]{:S(2)}) collective-permute-start(bf16[128,1920]{1,0:T(8,128)(2,1)S(1)} %shard_map.259.refs_4_.refs_0_), channel_id=1, source_target_pairs={{0,32},{32,0},{1,33},{33,1},{2,34},{34,2},{3,35},{35,3},{4,36},{36... | collective-permute-start | bytes 1474568 | tf_op jit(solution)/shard_map/ppermute | solution.py:358
  94.3 9.5 %all_to_all.60.parts = bf16[16,8,256]{2,1,0:T(8,128)(2,1)S(1)} all-to-all(bf16[16,8,256]{2,1,0:T(8,128)(2,1)S(1)} %bitcast.37), channel_id=1, replica_groups=mesh['zh'=8,'za'=2,'c'=2,'tp'=16] {'tp'}, dimensions={0} | all-to-all | bytes 131072 | tf_op jit(solution)/shard_map/all_to_all | solution.py:350
  104.4 9.4 %all_to_all.61 = bf16[16,8,256]{2,1,0:T(8,128)(2,1)S(1)} all-to-all(bf16[16,8,256]{2,1,0:T(8,128)(2,1)S(1)} %shard_map.261), channel_id=1, replica_groups=mesh['zh'=8,'za'=2,'c'=2,'tp'=16] {'tp'}, dimensions={0} | all-to-all | bytes 131072 | tf_op jit(solution)/shard_map/all_to_all | solution.py:350
  114.6 18.9 %all_to_all.62.parts = bf16[8,8,640]{2,1,0:T(8,128)(2,1)S(1)} all-to-all(bf16[8,8,640]{2,1,0:T(8,128)(2,1)S(1)} %shard_map.262), channel_id=1, replica_groups=mesh['zh'=8,'za'=2,'c'=2,'tp'=16] {'zh'}, dimensions={0} | all-to-all | bytes 163840 | tf_op jit(solution)/shard_map/all_to_all | solution.py:350
  134.8 13.8 %all_to_all.63.mixed = bf16[8,8,128]{2,1,0:T(8,128)(2,1)S(1)} all-to-all(bf16[8,8,128]{2,1,0:T(8,128)(2,1)S(1)} %shard_map.263), channel_id=1, replica_groups=mesh['zh'=8,'za'=2,'c'=2,'tp'=16] {'zh'}, dimensions={0} | all-to-all | bytes 32768 | tf_op jit(solution)/shard_map/all_to_all | solution.py:350
  149.3 8.5 %collective-permute-start.7 = (bf16[128,1920]{1,0:T(8,128)(2,1)S(1)}, bf16[128,1920]{1,0:T(8,128)(2,1)S(1)}, u32[]{:S(2)}, u32[]{:S(2)}) collective-permute-start(bf16[128,1920]{1,0:T(8,128)(2,1)S(1)} %collective-permute-done.6.refs_6_.refs_2_), channel_id=1, source_target_pairs={{0,16},{16,0},{1,17},{17,1},{2,18},{18,2},{3,19},{19,3},{4,20},{20... | collective-permute-start | bytes 1474568 | tf_op jit(solution)/shard_map/ppermute | solution.py:354
  157.9 9.4 %all_to_all.64.parts = bf16[16,8,256]{2,1,0:T(8,128)(2,1)S(1)} all-to-all(bf16[16,8,256]{2,1,0:T(8,128)(2,1)S(1)} %bitcast.36), channel_id=1, replica_groups=mesh['zh'=8,'za'=2,'c'=2,'tp'=16] {'tp'}, dimensions={0} | all-to-all | bytes 131072 | tf_op jit(solution)/shard_map/all_to_all | solution.py:350
  167.8 9.7 %all_to_all.65 = bf16[16,8,256]{2,1,0:T(8,128)(2,1)S(1)} all-to-all(bf16[16,8,256]{2,1,0:T(8,128)(2,1)S(1)} %shard_map.265), channel_id=1, replica_groups=mesh['zh'=8,'za'=2,'c'=2,'tp'=16] {'tp'}, dimensions={0} | all-to-all | bytes 131072 | tf_op jit(solution)/shard_map/all_to_all | solution.py:350
  178.4 16.7 %all_to_all.66.parts = bf16[8,8,1408]{2,1,0:T(8,128)(2,1)S(1)} all-to-all(bf16[8,8,1408]{2,1,0:T(8,128)(2,1)S(1)} %shard_map.266), channel_id=1, replica_groups=mesh['zh'=8,'za'=2,'c'=2,'tp'=16] {'zh'}, dimensions={0} | all-to-all | bytes 360448 | tf_op jit(solution)/shard_map/all_to_all | solution.py:350
  195.2 16.6 %all_to_all.67.hidden = bf16[8,8,640]{2,1,0:T(8,128)(2,1)S(1)} all-to-all(bf16[8,8,640]{2,1,0:T(8,128)(2,1)S(1)} %shard_map.267), channel_id=1, replica_groups=mesh['zh'=8,'za'=2,'c'=2,'tp'=16] {'zh'}, dimensions={0} | all-to-all | bytes 163840 | tf_op jit(solution)/shard_map/all_to_all | solution.py:350
  212.7 17.8 %all_to_all.68 = bf16[64,8,256]{2,1,0:T(8,128)(2,1)S(1)} all-to-all(bf16[64,8,256]{2,1,0:T(8,128)(2,1)S(1)} %bitcast.31), channel_id=1, replica_groups=mesh['zh'=8,'za'=2,'c'=2,'tp'=16] {'za','c','tp'}, dimensions={0} | all-to-all | bytes 524288 | tf_op jit(solution)/shard_map/all_to_all | solution.py:350
  (79 shorter events, 16.9 us)
Async XLA Ops:
  1.8 8.8 %copy-start.11 = (bf16[16,128]{1,0:T(8,128)(2,1)S(1)}, bf16[16,128]{1,0:T(8,128)(2,1)}, u32[]{:S(2)}) copy-start(bf16[16,128]{1,0:T(8,128)(2,1)} %tokens.1) | copy-start | bytes 12292
  1.9 8.8 %copy-start.12 = (f32[128]{0:T(128)S(1)}, f32[128]{0:T(128)}, u32[]{:S(2)}) copy-start(f32[128]{0:T(128)} %param.28) | copy-start | bytes 1540
  1.9 20.6 %collective-permute-start = (bf16[128,1280]{1,0:T(8,128)(2,1)S(1)}, bf16[128,1280]{1,0:T(8,128)(2,1)S(1)}, u32[]{:S(2)}, u32[]{:S(2)}) collective-permute-start(bf16[128,1280]{1,0:T(8,128)(2,1)S(1)} %shard_map.254.weights), channel_id=1, source_target_pairs={{0,16},{16,0},{1,17},{17,1},{2,18},{18,2},{3,19},{19,3},{4,20},{20... | collective-permute-start | bytes 983048 | tf_op jit(solution)/shard_map/ppermute | solution.py:354
  11.3 11.2 %all-to-all-start = ((bf16[32,8,256]{2,1,0:T(8,128)(2,1)}), bf16[32,8,256]{2,1,0:T(8,128)(2,1)S(1)}, u32[]{:S(2)}, u32[]{:S(2)}) async-start(bf16[32,8,256]{2,1,0:T(8,128)(2,1)} %bitcast.6), calls=%async_computation | async-start | bytes 262144 | tf_op jit(solution)/shard_map/all_to_all | solution.py:350
  24.1 14.8 %copy-start.21 = (f32[128]{0:T(128)S(1)}, f32[128]{0:T(128)}, u32[]{:S(2)}) copy-start(f32[128]{0:T(128)} %param.43) | copy-start | bytes 1540
  24.1 14.8 %copy-start.22 = (f32[128]{0:T(128)S(1)}, f32[128]{0:T(128)}, u32[]{:S(2)}) copy-start(f32[128]{0:T(128)} %param.32) | copy-start | bytes 1540
  24.1 14.8 %copy-start.2 = (bf16[640,128]{1,0:T(8,128)(2,1)S(1)}, bf16[640,128]{1,0:T(8,128)(2,1)}, u32[]{:S(2)}) copy-start(bf16[640,128]{1,0:T(8,128)(2,1)} %down) | copy-start | bytes 491524
  24.1 14.8 %copy-start.6 = (bf16[128,128]{1,0:T(8,128)(2,1)S(1)}, bf16[128,128]{1,0:T(8,128)(2,1)}, u32[]{:S(2)}) copy-start(bf16[128,128]{1,0:T(8,128)(2,1)} %query) | copy-start | bytes 98308
  24.1 14.8 %copy-start.7 = (bf16[128,128]{1,0:T(8,128)(2,1)S(1)}, bf16[128,128]{1,0:T(8,128)(2,1)}, u32[]{:S(2)}) copy-start(bf16[128,128]{1,0:T(8,128)(2,1)} %key) | copy-start | bytes 98308
  24.1 14.8 %copy-start.8 = (bf16[128,128]{1,0:T(8,128)(2,1)S(1)}, bf16[128,128]{1,0:T(8,128)(2,1)}, u32[]{:S(2)}) copy-start(bf16[128,128]{1,0:T(8,128)(2,1)} %value) | copy-start | bytes 98308
  24.1 14.8 %copy-start.9 = (bf16[128,128]{1,0:T(8,128)(2,1)S(1)}, bf16[128,128]{1,0:T(8,128)(2,1)}, u32[]{:S(2)}) copy-start(bf16[128,128]{1,0:T(8,128)(2,1)} %outer) | copy-start | bytes 98308
  24.1 14.8 %copy-start.10 = (bf16[128,128]{1,0:T(8,128)(2,1)S(1)}, bf16[128,128]{1,0:T(8,128)(2,1)}, u32[]{:S(2)}) copy-start(bf16[128,128]{1,0:T(8,128)(2,1)} %mixer_out) | copy-start | bytes 98308
  24.1 15.0 %copy-start.15 = (bf16[8,64,128]{2,1,0:T(8,128)(2,1)S(1)}, bf16[8,64,128]{2,1,0:T(8,128)(2,1)}, u32[]{:S(2)}) copy-start(bf16[8,64,128]{2,1,0:T(8,128)(2,1)} %values) | copy-start | bytes 393220
  24.1 29.7 %all-to-all-start.1 = ((bf16[16,8,1408]{2,1,0:T(8,128)(2,1)}), bf16[16,8,1408]{2,1,0:T(8,128)(2,1)S(1)}, u32[]{:S(2)}, u32[]{:S(2)}) async-start(bf16[16,8,1408]{2,1,0:T(8,128)(2,1)} %shard_map.255), calls=%async_computation.1 | async-start | bytes 720896 | tf_op jit(solution)/shard_map/all_to_all | solution.py:350
  37.4 1.7 copy-start.13
  46.3 17.6 %collective-permute-start.2 = (bf16[128,1408]{1,0:T(8,128)(2,1)S(1)}, bf16[128,1408]{1,0:T(8,128)(2,1)S(1)}, u32[]{:S(2)}, u32[]{:S(2)}) collective-permute-start(bf16[128,1408]{1,0:T(8,128)(2,1)S(1)} %shard_map.257.refs_0_), channel_id=1, source_target_pairs={{0,32},{32,0},{1,33},{33,1},{2,34},{34,2},{3,35},{35,3},{4,36},{36... | collective-permute-start | bytes 1081352 | tf_op jit(solution)/shard_map/ppermute | solution.py:358
  50.4 4.3 %copy-start.5 = (bf16[640,128]{1,0:T(8,128)(2,1)S(1)}, bf16[640,128]{1,0:T(8,128)(2,1)}, u32[]{:S(2)}) copy-start(bf16[640,128]{1,0:T(8,128)(2,1)} %down.1) | copy-start | bytes 491524
  54.9 35.7 %collective-permute-start.5 = (bf16[128,1920]{1,0:T(8,128)(2,1)S(1)}, bf16[128,1920]{1,0:T(8,128)(2,1)S(1)}, u32[]{:S(2)}, u32[]{:S(2)}) collective-permute-start(bf16[128,1920]{1,0:T(8,128)(2,1)S(1)} %shard_map.259.refs_4_.refs_0_), channel_id=1, source_target_pairs={{0,16},{16,0},{1,17},{17,1},{2,18},{18,2},{3,19},{19,3},{4,20},{20... | collective-permute-start | bytes 1474568 | tf_op jit(solution)/shard_map/ppermute | solution.py:354
  63.9 22.1 %collective-permute-start.3 = (bf16[128,1408]{1,0:T(8,128)(2,1)S(1)}, bf16[128,1408]{1,0:T(8,128)(2,1)S(1)}, u32[]{:S(2)}, u32[]{:S(2)}) collective-permute-start(bf16[128,1408]{1,0:T(8,128)(2,1)S(1)} %collective-permute-done.2.refs_2_), channel_id=1, source_target_pairs={{0,16},{16,0},{1,17},{17,1},{2,18},{18,2},{3,19},{19,3},{4,20},{20... | collective-permute-start | bytes 1081352 | tf_op jit(solution)/shard_map/ppermute | solution.py:354
  65.8 24.8 %collective-permute-start.1 = (bf16[128,1408]{1,0:T(8,128)(2,1)S(1)}, bf16[128,1408]{1,0:T(8,128)(2,1)S(1)}, u32[]{:S(2)}, u32[]{:S(2)}) collective-permute-start(bf16[128,1408]{1,0:T(8,128)(2,1)S(1)} %shard_map.257.refs_0_), channel_id=1, source_target_pairs={{0,16},{16,0},{1,17},{17,1},{2,18},{18,2},{3,19},{19,3},{4,20},{20... | collective-permute-start | bytes 1081352 | tf_op jit(solution)/shard_map/ppermute | solution.py:354
  68.2 22.3 %all-to-all-start.2 = ((bf16[8,8,640]{2,1,0:T(8,128)(2,1)}), bf16[8,8,640]{2,1,0:T(8,128)(2,1)S(1)}, u32[]{:S(2)}, u32[]{:S(2)}) async-start(bf16[8,8,640]{2,1,0:T(8,128)(2,1)} %shard_map.258), calls=%async_computation.2 | async-start | bytes 163840 | tf_op jit(solution)/shard_map/all_to_all | solution.py:350
  77.9 8.0 %collective-permute-start.4 = (bf16[2,16,8,256]{3,2,1,0:T(8,128)(2,1)S(1)}, bf16[2,16,8,256]{3,2,1,0:T(8,128)(2,1)S(1)}, u32[]{:S(2)}, u32[]{:S(2)}) collective-permute-start(bf16[2,16,8,256]{3,2,1,0:T(8,128)(2,1)S(1)} %bitcast.28), channel_id=1, source_target_pairs={{0,32},{32,0},{1,33},{33,1},{2,34},{34,2},{3,35},{35,3},{4,36},{36... | collective-permute-start | bytes 393224 | tf_op jit(solution)/shard_map/ppermute | solution.py:358
  91.4 57.9 %collective-permute-start.6 = (bf16[128,1920]{1,0:T(8,128)(2,1)S(1)}, bf16[128,1920]{1,0:T(8,128)(2,1)S(1)}, u32[]{:S(2)}, u32[]{:S(2)}) collective-permute-start(bf16[128,1920]{1,0:T(8,128)(2,1)S(1)} %shard_map.259.refs_4_.refs_0_), channel_id=1, source_target_pairs={{0,32},{32,0},{1,33},{33,1},{2,34},{34,2},{3,35},{35,3},{4,36},{36... | collective-permute-start | bytes 1474568 | tf_op jit(solution)/shard_map/ppermute | solution.py:358
  149.3 17.9 %collective-permute-start.7 = (bf16[128,1920]{1,0:T(8,128)(2,1)S(1)}, bf16[128,1920]{1,0:T(8,128)(2,1)S(1)}, u32[]{:S(2)}, u32[]{:S(2)}) collective-permute-start(bf16[128,1920]{1,0:T(8,128)(2,1)S(1)} %collective-permute-done.6.refs_6_.refs_2_), channel_id=1, source_target_pairs={{0,16},{16,0},{1,17},{17,1},{2,18},{18,2},{3,19},{19,3},{4,20},{20... | collective-permute-start | bytes 1474568 | tf_op jit(solution)/shard_map/ppermute | solution.py:354
  (10 other events, 8.7 us)

commit v10 on v9

--- a/solution.py
+++ b/solution.py
@@ -409,6 +409,18 @@
         pack_first, ((width, 2 * hidden_units), bf16), first_gate_weight, first_up_weight
     )
     first_x = swap(first)
+    packed = kernel(
+        pack,
+        ((width, hidden_units + 4 * dk + width + LANES), bf16),
+        first_down_weight,
+        query_weight_matrix,
+        key_weight_matrix,
+        value_weight_matrix,
+        output_gate_weight,
+        mixer_out_weight,
+        jnp.stack([mixer_norm_gain, second_norm_gain]),
+    )
+    packed_z = swap_chips(packed)
     sent = kernel(
         first_products,
         ((ring, rows, 2 * hidden_units + LANES), bf16),
@@ -422,10 +434,7 @@
     sent, later = together(
         sent,
         (
-            first_down_weight,
             (second_gate_weight, second_up_weight, second_down_weight),
-            (query_weight_matrix, key_weight_matrix, value_weight_matrix, output_gate_weight),
-            (mixer_out_weight, mixer_norm_gain, second_norm_gain),
             (strength_weight, decay_weight),
             (head_decay_speed, head_decay_offset),
             (recurrent, earlier_key_cache, earlier_value_cache),
@@ -433,9 +442,8 @@
             (lengths, head_norm_gain),
         ),
     )
-    down, branch, heads, outer, logits, decays, caches, histories, others = later
+    branch, logits, decays, caches, histories, others = later
     parts = exchange(sent, Z)
-    gains = jnp.stack(outer[1:])
     head = jnp.concatenate(decays)
     lengths, head_norm_gain = others
     local = lengths.shape[0]
@@ -455,16 +463,6 @@
         scalars=2,
         flops=1 << 28,
     )
-    packed = kernel(
-        pack,
-        ((width, hidden_units + 4 * dk + width + LANES), bf16),
-        down,
-        *heads,
-        outer[0],
-        gains,
-    )
-    state, packed = together(state, packed)
-    packed_z = swap_chips(packed)
     got_z = swap_chips(got)
     start = lax.axis_index("zh") * 4 * width
     logits = [lax.dynamic_slice_in_dim(w.T, start, 4 * width, 1) for w in logits]

time: 233 us -> 233 us (level)
  no operation moved by 1% of the time
where the time goes in v10:
time: 233 us; the launch traced here: 232 us
  blocking collectives  122 us (52%)
  starting transfers between devices  66.6 us (29%)
  waiting for transfers between devices  20.4 us (9%)
  Pallas kernels  17.6 us (8%)
  local copies, waits for them, and re-layouts  3.6 us (2%)
    all_to_all x9, blocking collectives, exchange(): return lax.all_to_all(x, axis, 0, 0, tiled=True)  122 us
    ppermute x5, starting transfers between devices, swap(): return lax.ppermute(x, 'c', [(0, 1), (1, 0)])  31.1 us
    all_to_all x3, starting transfers between devices, exchange(): return lax.all_to_all(x, axis, 0, 0, tiled=True)  26.1 us
    pallas_call x17, Pallas kernels, kernel(): pl.pallas_call(functools.partial(fn, **static), out_shape=shapes, in_spec...  17.6 us
    all_to_all x3, waiting for transfers between devices, exchange(): return lax.all_to_all(x, axis, 0, 0, tiled=True)  15.5 us
    ppermute x3, starting transfers between devices, swap_chips(): return lax.ppermute(x, 'za', [(0, 1), (1, 0)])  9.4 us
    ppermute x3, waiting for transfers between devices, swap_chips(): return lax.ppermute(x, 'za', [(0, 1), (1, 0)])  4.96 us
  transfers between devices with their start and end apart: 11, of which 4 were waited for; matrix products, arithmetic and copies ran while one was open for 0% of the time, Pallas kernels for 5%

profile of v10, /device:TPU:1, one launch (start us, length us, event | category | flops | bytes accessed | tf_op | source)
XLA Modules:
  0.0 231.6 jit_solution(7871091754452578730)
XLA Ops:
  1.9 8.7 %collective-permute-start = (bf16[128,1280]{1,0:T(8,128)(2,1)S(1)}, bf16[128,1280]{1,0:T(8,128)(2,1)S(1)}, u32[]{:S(2)}, u32[]{:S(2)}) collective-permute-start(bf16[128,1280]{1,0:T(8,128)(2,1)S(1)} %shard_map.254.weights), channel_id=1, source_target_pairs={{0,16},{16,0},{1,17},{17,1},{2,18},{18,2},{3,19},{19,3},{4,20},{20... | collective-permute-start | bytes 983048 | tf_op jit(solution)/shard_map/ppermute | solution.py:354
  11.3 3.6 %all-to-all-start = ((bf16[32,8,256]{2,1,0:T(8,128)(2,1)}), bf16[32,8,256]{2,1,0:T(8,128)(2,1)S(1)}, u32[]{:S(2)}, u32[]{:S(2)}) async-start(bf16[32,8,256]{2,1,0:T(8,128)(2,1)} %bitcast.6), calls=%async_computation | async-start | bytes 262144 | tf_op jit(solution)/shard_map/all_to_all | solution.py:350
  15.1 7.4 %all-to-all-done = bf16[32,8,256]{2,1,0:T(8,128)(2,1)S(1)} async-done(((bf16[32,8,256]{2,1,0:T(8,128)(2,1)}), bf16[32,8,256]{2,1,0:T(8,128)(2,1)S(1)}, u32[]{:S(2)}, u32[]{:S(2)}) %all-to-all-start) | async-done | bytes 131104 | tf_op jit(solution)/shard_map/all_to_all | solution.py:350
  24.1 13.3 %all-to-all-start.1 = ((bf16[16,8,1408]{2,1,0:T(8,128)(2,1)}), bf16[16,8,1408]{2,1,0:T(8,128)(2,1)S(1)}, u32[]{:S(2)}, u32[]{:S(2)}) async-start(bf16[16,8,1408]{2,1,0:T(8,128)(2,1)} %shard_map.255), calls=%async_computation.1 | async-start | bytes 720896 | tf_op jit(solution)/shard_map/all_to_all | solution.py:350
  37.6 3.4 %collective-permute-start.2 = (bf16[128,1408]{1,0:T(8,128)(2,1)S(1)}, bf16[128,1408]{1,0:T(8,128)(2,1)S(1)}, u32[]{:S(2)}, u32[]{:S(2)}) collective-permute-start(bf16[128,1408]{1,0:T(8,128)(2,1)S(1)} %shard_map.257.refs_0_), channel_id=1, source_target_pairs={{0,32},{32,0},{1,33},{33,1},{2,34},{34,2},{3,35},{35,3},{4,36},{36... | collective-permute-start | bytes 1081352 | tf_op jit(solution)/shard_map/ppermute | solution.py:358
  43.9 6.4 %shard_map.256 = (f32[8,128,128]{2,1,0:T(8,128)S(1)}, f32[8,128]{1,0:T(8,128)S(1)}, f32[8,128]{1,0:T(8,128)S(1)}) custom-call(s32[8]{0:T(128)S(1)} %copy-done.19, f32[2]{0:T(128)S(1)} %pad_maximum_fusion.1.head, f32[8,128,128]{2,1,0:T(8,128)S(1)} %bitcast.39, bf16[8,64,128]{2,1,0:T(8,128)(2,1)S(1)} %copy-done.14, bf16[8,64,128]{2,1,0:T(8,128)(2,1)S(1)} %copy-done.15, ...), custom_call_target="tpu_custom_call" | custom-call | flops 268435456 | bytes 793128 | tf_op jit(solution)/shard_map/pallas_call | solution.py:24
  50.4 3.5 %all-to-all-done.1.parts = bf16[16,8,1408]{2,1,0:T(8,128)(2,1)S(1)} async-done(((bf16[16,8,1408]{2,1,0:T(8,128)(2,1)}), bf16[16,8,1408]{2,1,0:T(8,128)(2,1)S(1)}, u32[]{:S(2)}, u32[]{:S(2)}) %all-to-all-start.1) | async-done | bytes 360480 | tf_op jit(solution)/shard_map/all_to_all | solution.py:350
  54.9 9.5 %collective-permute-start.5 = (bf16[128,1920]{1,0:T(8,128)(2,1)S(1)}, bf16[128,1920]{1,0:T(8,128)(2,1)S(1)}, u32[]{:S(2)}, u32[]{:S(2)}) collective-permute-start(bf16[128,1920]{1,0:T(8,128)(2,1)S(1)} %shard_map.259.refs_4_.refs_0_), channel_id=1, source_target_pairs={{0,16},{16,0},{1,17},{17,1},{2,18},{18,2},{3,19},{19,3},{4,20},{20... | collective-permute-start | bytes 1474568 | tf_op jit(solution)/shard_map/ppermute | solution.py:354
  66.3 2.4 %collective-permute-start.1 = (bf16[128,1408]{1,0:T(8,128)(2,1)S(1)}, bf16[128,1408]{1,0:T(8,128)(2,1)S(1)}, u32[]{:S(2)}, u32[]{:S(2)}) collective-permute-start(bf16[128,1408]{1,0:T(8,128)(2,1)S(1)} %shard_map.257.refs_0_), channel_id=1, source_target_pairs={{0,16},{16,0},{1,17},{17,1},{2,18},{18,2},{3,19},{19,3},{4,20},{20... | collective-permute-start | bytes 1081352 | tf_op jit(solution)/shard_map/ppermute | solution.py:354
  68.7 9.2 %all-to-all-start.2 = ((bf16[8,8,640]{2,1,0:T(8,128)(2,1)}), bf16[8,8,640]{2,1,0:T(8,128)(2,1)S(1)}, u32[]{:S(2)}, u32[]{:S(2)}) async-start(bf16[8,8,640]{2,1,0:T(8,128)(2,1)} %shard_map.258), calls=%async_computation.2 | async-start | bytes 163840 | tf_op jit(solution)/shard_map/all_to_all | solution.py:350
  77.9 3.1 %collective-permute-start.4 = (bf16[2,16,8,256]{3,2,1,0:T(8,128)(2,1)S(1)}, bf16[2,16,8,256]{3,2,1,0:T(8,128)(2,1)S(1)}, u32[]{:S(2)}, u32[]{:S(2)}) collective-permute-start(bf16[2,16,8,256]{3,2,1,0:T(8,128)(2,1)S(1)} %bitcast.28), channel_id=1, source_target_pairs={{0,32},{32,0},{1,33},{33,1},{2,34},{34,2},{3,35},{35,3},{4,36},{36... | collective-permute-start | bytes 393224 | tf_op jit(solution)/shard_map/ppermute | solution.py:358
  81.0 4.9 %collective-permute-done.4.got_z = bf16[2,16,8,256]{3,2,1,0:T(8,128)(2,1)S(1)} collective-permute-done((bf16[2,16,8,256]{3,2,1,0:T(8,128)(2,1)S(1)}, bf16[2,16,8,256]{3,2,1,0:T(8,128)(2,1)S(1)}, u32[]{:S(2)}, u32[]{:S(2)}) %collective-permute-start.4) | collective-permute-done | bytes 131104 | tf_op jit(solution)/shard_map/ppermute | solution.py:358
  86.0 4.6 %all-to-all-done.2.hidden = bf16[8,8,640]{2,1,0:T(8,128)(2,1)S(1)} async-done(((bf16[8,8,640]{2,1,0:T(8,128)(2,1)}), bf16[8,8,640]{2,1,0:T(8,128)(2,1)S(1)}, u32[]{:S(2)}, u32[]{:S(2)}) %all-to-all-start.2) | async-done | bytes 81952 | tf_op jit(solution)/shard_map/all_to_all | solution.py:350
  91.4 2.9 %collective-permute-start.6 = (bf16[128,1920]{1,0:T(8,128)(2,1)S(1)}, bf16[128,1920]{1,0:T(8,128)(2,1)S(1)}, u32[]{:S(2)}, u32[]{:S(2)}) collective-permute-start(bf16[128,1920]{1,0:T(8,128)(2,1)S(1)} %shard_map.259.refs_4_.refs_0_), channel_id=1, source_target_pairs={{0,32},{32,0},{1,33},{33,1},{2,34},{34,2},{3,35},{35,3},{4,36},{36... | collective-permute-start | bytes 1474568 | tf_op jit(solution)/shard_map/ppermute | solution.py:358
  94.3 9.5 %all_to_all.60.parts = bf16[16,8,256]{2,1,0:T(8,128)(2,1)S(1)} all-to-all(bf16[16,8,256]{2,1,0:T(8,128)(2,1)S(1)} %bitcast.37), channel_id=1, replica_groups=mesh['zh'=8,'za'=2,'c'=2,'tp'=16] {'tp'}, dimensions={0} | all-to-all | bytes 131072 | tf_op jit(solution)/shard_map/all_to_all | solution.py:350
  104.4 9.4 %all_to_all.61 = bf16[16,8,256]{2,1,0:T(8,128)(2,1)S(1)} all-to-all(bf16[16,8,256]{2,1,0:T(8,128)(2,1)S(1)} %shard_map.261), channel_id=1, replica_groups=mesh['zh'=8,'za'=2,'c'=2,'tp'=16] {'tp'}, dimensions={0} | all-to-all | bytes 131072 | tf_op jit(solution)/shard_map/all_to_all | solution.py:350
  114.6 18.9 %all_to_all.62.parts = bf16[8,8,640]{2,1,0:T(8,128)(2,1)S(1)} all-to-all(bf16[8,8,640]{2,1,0:T(8,128)(2,1)S(1)} %shard_map.262), channel_id=1, replica_groups=mesh['zh'=8,'za'=2,'c'=2,'tp'=16] {'zh'}, dimensions={0} | all-to-all | bytes 163840 | tf_op jit(solution)/shard_map/all_to_all | solution.py:350
  134.8 13.8 %all_to_all.63.mixed = bf16[8,8,128]{2,1,0:T(8,128)(2,1)S(1)} all-to-all(bf16[8,8,128]{2,1,0:T(8,128)(2,1)S(1)} %shard_map.263), channel_id=1, replica_groups=mesh['zh'=8,'za'=2,'c'=2,'tp'=16] {'zh'}, dimensions={0} | all-to-all | bytes 32768 | tf_op jit(solution)/shard_map/all_to_all | solution.py:350
  149.3 8.5 %collective-permute-start.7 = (bf16[128,1920]{1,0:T(8,128)(2,1)S(1)}, bf16[128,1920]{1,0:T(8,128)(2,1)S(1)}, u32[]{:S(2)}, u32[]{:S(2)}) collective-permute-start(bf16[128,1920]{1,0:T(8,128)(2,1)S(1)} %collective-permute-done.6.refs_6_.refs_2_), channel_id=1, source_target_pairs={{0,16},{16,0},{1,17},{17,1},{2,18},{18,2},{3,19},{19,3},{4,20},{20... | collective-permute-start | bytes 1474568 | tf_op jit(solution)/shard_map/ppermute | solution.py:354
  157.8 9.4 %all_to_all.64.parts = bf16[16,8,256]{2,1,0:T(8,128)(2,1)S(1)} all-to-all(bf16[16,8,256]{2,1,0:T(8,128)(2,1)S(1)} %bitcast.36), channel_id=1, replica_groups=mesh['zh'=8,'za'=2,'c'=2,'tp'=16] {'tp'}, dimensions={0} | all-to-all | bytes 131072 | tf_op jit(solution)/shard_map/all_to_all | solution.py:350
  167.8 9.7 %all_to_all.65 = bf16[16,8,256]{2,1,0:T(8,128)(2,1)S(1)} all-to-all(bf16[16,8,256]{2,1,0:T(8,128)(2,1)S(1)} %shard_map.265), channel_id=1, replica_groups=mesh['zh'=8,'za'=2,'c'=2,'tp'=16] {'tp'}, dimensions={0} | all-to-all | bytes 131072 | tf_op jit(solution)/shard_map/all_to_all | solution.py:350
  178.4 16.7 %all_to_all.66.parts = bf16[8,8,1408]{2,1,0:T(8,128)(2,1)S(1)} all-to-all(bf16[8,8,1408]{2,1,0:T(8,128)(2,1)S(1)} %shard_map.266), channel_id=1, replica_groups=mesh['zh'=8,'za'=2,'c'=2,'tp'=16] {'zh'}, dimensions={0} | all-to-all | bytes 360448 | tf_op jit(solution)/shard_map/all_to_all | solution.py:350
  195.2 16.6 %all_to_all.67.hidden = bf16[8,8,640]{2,1,0:T(8,128)(2,1)S(1)} all-to-all(bf16[8,8,640]{2,1,0:T(8,128)(2,1)S(1)} %shard_map.267), channel_id=1, replica_groups=mesh['zh'=8,'za'=2,'c'=2,'tp'=16] {'zh'}, dimensions={0} | all-to-all | bytes 163840 | tf_op jit(solution)/shard_map/all_to_all | solution.py:350
  212.7 17.8 %all_to_all.68 = bf16[64,8,256]{2,1,0:T(8,128)(2,1)S(1)} all-to-all(bf16[64,8,256]{2,1,0:T(8,128)(2,1)S(1)} %bitcast.31), channel_id=1, replica_groups=mesh['zh'=8,'za'=2,'c'=2,'tp'=16] {'za','c','tp'}, dimensions={0} | all-to-all | bytes 524288 | tf_op jit(solution)/shard_map/all_to_all | solution.py:350
  (79 shorter events, 16.8 us)
Async XLA Ops:
  1.8 8.8 %copy-start.11 = (bf16[16,128]{1,0:T(8,128)(2,1)S(1)}, bf16[16,128]{1,0:T(8,128)(2,1)}, u32[]{:S(2)}) copy-start(bf16[16,128]{1,0:T(8,128)(2,1)} %tokens.1) | copy-start | bytes 12292
  1.9 8.8 %copy-start.12 = (f32[128]{0:T(128)S(1)}, f32[128]{0:T(128)}, u32[]{:S(2)}) copy-start(f32[128]{0:T(128)} %param.28) | copy-start | bytes 1540
  1.9 20.6 %collective-permute-start = (bf16[128,1280]{1,0:T(8,128)(2,1)S(1)}, bf16[128,1280]{1,0:T(8,128)(2,1)S(1)}, u32[]{:S(2)}, u32[]{:S(2)}) collective-permute-start(bf16[128,1280]{1,0:T(8,128)(2,1)S(1)} %shard_map.254.weights), channel_id=1, source_target_pairs={{0,16},{16,0},{1,17},{17,1},{2,18},{18,2},{3,19},{19,3},{4,20},{20... | collective-permute-start | bytes 983048 | tf_op jit(solution)/shard_map/ppermute | solution.py:354
  11.3 11.2 %all-to-all-start = ((bf16[32,8,256]{2,1,0:T(8,128)(2,1)}), bf16[32,8,256]{2,1,0:T(8,128)(2,1)S(1)}, u32[]{:S(2)}, u32[]{:S(2)}) async-start(bf16[32,8,256]{2,1,0:T(8,128)(2,1)} %bitcast.6), calls=%async_computation | async-start | bytes 262144 | tf_op jit(solution)/shard_map/all_to_all | solution.py:350
  24.1 13.4 %copy-start.21 = (f32[128]{0:T(128)S(1)}, f32[128]{0:T(128)}, u32[]{:S(2)}) copy-start(f32[128]{0:T(128)} %param.43) | copy-start | bytes 1540
  24.1 13.4 %copy-start.22 = (f32[128]{0:T(128)S(1)}, f32[128]{0:T(128)}, u32[]{:S(2)}) copy-start(f32[128]{0:T(128)} %param.32) | copy-start | bytes 1540
  24.1 13.4 %copy-start.2 = (bf16[640,128]{1,0:T(8,128)(2,1)S(1)}, bf16[640,128]{1,0:T(8,128)(2,1)}, u32[]{:S(2)}) copy-start(bf16[640,128]{1,0:T(8,128)(2,1)} %down.1) | copy-start | bytes 491524
  24.1 13.4 %copy-start.6 = (bf16[128,128]{1,0:T(8,128)(2,1)S(1)}, bf16[128,128]{1,0:T(8,128)(2,1)}, u32[]{:S(2)}) copy-start(bf16[128,128]{1,0:T(8,128)(2,1)} %query.1) | copy-start | bytes 98308
  24.1 13.4 %copy-start.7 = (bf16[128,128]{1,0:T(8,128)(2,1)S(1)}, bf16[128,128]{1,0:T(8,128)(2,1)}, u32[]{:S(2)}) copy-start(bf16[128,128]{1,0:T(8,128)(2,1)} %key.1) | copy-start | bytes 98308
  24.1 13.4 %copy-start.8 = (bf16[128,128]{1,0:T(8,128)(2,1)S(1)}, bf16[128,128]{1,0:T(8,128)(2,1)}, u32[]{:S(2)}) copy-start(bf16[128,128]{1,0:T(8,128)(2,1)} %value.1) | copy-start | bytes 98308
  24.1 13.4 %copy-start.9 = (bf16[128,128]{1,0:T(8,128)(2,1)S(1)}, bf16[128,128]{1,0:T(8,128)(2,1)}, u32[]{:S(2)}) copy-start(bf16[128,128]{1,0:T(8,128)(2,1)} %outer.1) | copy-start | bytes 98308
  24.1 13.4 %copy-start.10 = (bf16[128,128]{1,0:T(8,128)(2,1)S(1)}, bf16[128,128]{1,0:T(8,128)(2,1)}, u32[]{:S(2)}) copy-start(bf16[128,128]{1,0:T(8,128)(2,1)} %mixer_out.1) | copy-start | bytes 98308
  24.1 29.7 %all-to-all-start.1 = ((bf16[16,8,1408]{2,1,0:T(8,128)(2,1)}), bf16[16,8,1408]{2,1,0:T(8,128)(2,1)S(1)}, u32[]{:S(2)}, u32[]{:S(2)}) async-start(bf16[16,8,1408]{2,1,0:T(8,128)(2,1)} %shard_map.255), calls=%async_computation.1 | async-start | bytes 720896 | tf_op jit(solution)/shard_map/all_to_all | solution.py:350
  37.4 5.9 %copy-start.13 = (f32[8,1,128,128]{3,2,1,0:T(8,128)S(1)}, f32[8,1,128,128]{3,2,1,0:T(8,128)}, u32[]{:S(2)}) copy-start(f32[8,1,128,128]{3,2,1,0:T(8,128)} %param.47) | copy-start | bytes 1572868
  37.5 5.8 %copy-start.15 = (bf16[8,64,128]{2,1,0:T(8,128)(2,1)S(1)}, bf16[8,64,128]{2,1,0:T(8,128)(2,1)}, u32[]{:S(2)}) copy-start(bf16[8,64,128]{2,1,0:T(8,128)(2,1)} %values) | copy-start | bytes 393220
  37.6 5.7 %copy-start.14 = (bf16[8,64,128]{2,1,0:T(8,128)(2,1)S(1)}, bf16[8,64,128]{2,1,0:T(8,128)(2,1)}, u32[]{:S(2)}) copy-start(bf16[8,64,128]{2,1,0:T(8,128)(2,1)} %keys) | copy-start | bytes 393220
  37.6 26.7 %collective-permute-start.2 = (bf16[128,1408]{1,0:T(8,128)(2,1)S(1)}, bf16[128,1408]{1,0:T(8,128)(2,1)S(1)}, u32[]{:S(2)}, u32[]{:S(2)}) collective-permute-start(bf16[128,1408]{1,0:T(8,128)(2,1)S(1)} %shard_map.257.refs_0_), channel_id=1, source_target_pairs={{0,32},{32,0},{1,33},{33,1},{2,34},{34,2},{3,35},{35,3},{4,36},{36... | collective-permute-start | bytes 1081352 | tf_op jit(solution)/shard_map/ppermute | solution.py:358
  54.9 35.7 %collective-permute-start.5 = (bf16[128,1920]{1,0:T(8,128)(2,1)S(1)}, bf16[128,1920]{1,0:T(8,128)(2,1)S(1)}, u32[]{:S(2)}, u32[]{:S(2)}) collective-permute-start(bf16[128,1920]{1,0:T(8,128)(2,1)S(1)} %shard_map.259.refs_4_.refs_0_), channel_id=1, source_target_pairs={{0,16},{16,0},{1,17},{17,1},{2,18},{18,2},{3,19},{19,3},{4,20},{20... | collective-permute-start | bytes 1474568 | tf_op jit(solution)/shard_map/ppermute | solution.py:354
  64.4 21.6 %collective-permute-start.3 = (bf16[128,1408]{1,0:T(8,128)(2,1)S(1)}, bf16[128,1408]{1,0:T(8,128)(2,1)S(1)}, u32[]{:S(2)}, u32[]{:S(2)}) collective-permute-start(bf16[128,1408]{1,0:T(8,128)(2,1)S(1)} %collective-permute-done.2.refs_2_), channel_id=1, source_target_pairs={{0,16},{16,0},{1,17},{17,1},{2,18},{18,2},{3,19},{19,3},{4,20},{20... | collective-permute-start | bytes 1081352 | tf_op jit(solution)/shard_map/ppermute | solution.py:354
  66.3 24.2 %collective-permute-start.1 = (bf16[128,1408]{1,0:T(8,128)(2,1)S(1)}, bf16[128,1408]{1,0:T(8,128)(2,1)S(1)}, u32[]{:S(2)}, u32[]{:S(2)}) collective-permute-start(bf16[128,1408]{1,0:T(8,128)(2,1)S(1)} %shard_map.257.refs_0_), channel_id=1, source_target_pairs={{0,16},{16,0},{1,17},{17,1},{2,18},{18,2},{3,19},{19,3},{4,20},{20... | collective-permute-start | bytes 1081352 | tf_op jit(solution)/shard_map/ppermute | solution.py:354
  68.7 21.8 %all-to-all-start.2 = ((bf16[8,8,640]{2,1,0:T(8,128)(2,1)}), bf16[8,8,640]{2,1,0:T(8,128)(2,1)S(1)}, u32[]{:S(2)}, u32[]{:S(2)}) async-start(bf16[8,8,640]{2,1,0:T(8,128)(2,1)} %shard_map.258), calls=%async_computation.2 | async-start | bytes 163840 | tf_op jit(solution)/shard_map/all_to_all | solution.py:350
  77.9 8.0 %collective-permute-start.4 = (bf16[2,16,8,256]{3,2,1,0:T(8,128)(2,1)S(1)}, bf16[2,16,8,256]{3,2,1,0:T(8,128)(2,1)S(1)}, u32[]{:S(2)}, u32[]{:S(2)}) collective-permute-start(bf16[2,16,8,256]{3,2,1,0:T(8,128)(2,1)S(1)} %bitcast.28), channel_id=1, source_target_pairs={{0,32},{32,0},{1,33},{33,1},{2,34},{34,2},{3,35},{35,3},{4,36},{36... | collective-permute-start | bytes 393224 | tf_op jit(solution)/shard_map/ppermute | solution.py:358
  91.4 57.9 %collective-permute-start.6 = (bf16[128,1920]{1,0:T(8,128)(2,1)S(1)}, bf16[128,1920]{1,0:T(8,128)(2,1)S(1)}, u32[]{:S(2)}, u32[]{:S(2)}) collective-permute-start(bf16[128,1920]{1,0:T(8,128)(2,1)S(1)} %shard_map.259.refs_4_.refs_0_), channel_id=1, source_target_pairs={{0,32},{32,0},{1,33},{33,1},{2,34},{34,2},{3,35},{35,3},{4,36},{36... | collective-permute-start | bytes 1474568 | tf_op jit(solution)/shard_map/ppermute | solution.py:358
  149.3 17.9 %collective-permute-start.7 = (bf16[128,1920]{1,0:T(8,128)(2,1)S(1)}, bf16[128,1920]{1,0:T(8,128)(2,1)S(1)}, u32[]{:S(2)}, u32[]{:S(2)}) collective-permute-start(bf16[128,1920]{1,0:T(8,128)(2,1)S(1)} %collective-permute-done.6.refs_6_.refs_2_), channel_id=1, source_target_pairs={{0,16},{16,0},{1,17},{17,1},{2,18},{18,2},{3,19},{19,3},{4,20},{20... | collective-permute-start | bytes 1474568 | tf_op jit(solution)/shard_map/ppermute | solution.py:354
  (10 other events, 11.5 us)
